TPU v7x, 128 devices: a 2x2x16 block of a 8x8x16 slice. The times are simulated.
128 devices in a mesh: grp: 4 (over y, x), ep: 32 (over z, core).
Axes of the slice: x: 2, y: 2, z: 16, core: 2. Of those that a mesh axis runs over, the one named last changes fastest.
The devices are a block of a 8x8x16 slice.
Arguments:
- tokens: bfloat16 [4096, 2048], P(('grp', 'ep')), parts along dimension 0, may hold values from -6 to 6
- norm_gain: float32 [2048], replicated, may hold values from 0.5 to 4
- routes: int32 [4096, 4], P(('grp', 'ep')), parts along dimension 0, may hold values from 0 to 31, all different within a row; in each aligned block of 32 rows (0 to 31, 32 to 63, ...) at most 8 rows name the same one
- route_logits: float32 [4096, 4], P(('grp', 'ep')), parts along dimension 0, may hold values from -6 to 6
- w_gate: bfloat16 [32, 2048, 1792], P('ep'), may hold values from -0.125 to 0.125
- w_up: bfloat16 [32, 2048, 1792], P('ep'), may hold values from -0.125 to 0.125
- w_down: bfloat16 [32, 1792, 2048], P('ep'), may hold values from -0.125 to 0.125
Outputs:
- mixed: bfloat16 [4096, 2048], P(('grp', 'ep')), parts along dimension 0
There are 4 independent parts, one for each index of `grp`. A program takes and returns all parts, laid end to end along the dimension named above; an argument that names none is the same for every part. Nothing has to cross between parts.
Inputs may be any that keep to these rules, and one draw needn't show every extreme that they name: `routes`: each token names 4 different experts. Among the 32 tokens of one device no expert is named by more than 8 of them, and in every draw some expert is named by exactly 8 tokens of some device.
All inputs are finite; a program needn't handle non-finite values.
Results may differ from a plain program's by a relative error of at most 0.012.
Values may be sent and summed in bfloat16 or wider, within the bound.
No kernel may reach another device: no remote copies, remote signals or barrier semaphores. Data moves between devices by JAX's collectives and lax.ppermute only.
A program may use at most 64 MiB of HBM per device.

v0:
```python
import jax
import jax.numpy as jnp
from jax import lax
from jax.sharding import Mesh
from jax.sharding import PartitionSpec as P

TOP_K = 4
EP = ("ep_0", "ep_1")
GRP_EP = ("grp", "ep_0", "ep_1")


def cut_along(x, dim, devices):
    lengths = x.shape
    pieces = x.reshape(*lengths[:dim], devices, lengths[dim] // devices, *lengths[dim + 1 :])
    return jnp.moveaxis(pieces, dim, 0)


def in_order(pieces, dim):
    lengths = list(pieces.shape[1:])
    lengths[dim] *= pieces.shape[0]
    return jnp.moveaxis(pieces, 0, dim).reshape(lengths)


def turned_blocks(pieces, axes, order):
    inside = pieces.shape[1:]
    out = pieces.reshape(*(lax.axis_size(a) for a in axes), *inside)
    for k in order:
        out = lax.all_to_all(out, axes[k], k, k, tiled=True)
    return out.reshape(-1, *inside)


def exchange_by_chip(x, groups, order, split_dim, concat_dim):
    devices = lax.axis_size(groups[0]) * lax.axis_size(groups[1])
    pieces = cut_along(x, split_dim, devices)
    return in_order(turned_blocks(pieces, groups, order), concat_dim)


def rmsnorm(values, gain):
    floats = values.astype(jnp.float32)
    scaled = floats * lax.rsqrt(jnp.mean(floats * floats, axis=-1, keepdims=True) + 1e-06)
    return (scaled * gain).astype(jnp.bfloat16)


def expert(rows, gate_weight, up_weight, down_weight):
    gate = jnp.minimum(jnp.dot(rows, gate_weight, preferred_element_type=jnp.float32), 7.0)
    upper = jnp.clip(jnp.dot(rows, up_weight, preferred_element_type=jnp.float32), -7.0, 7.0)
    active = (gate * jax.nn.sigmoid(1.702 * gate) * (upper + 1.0)).astype(jnp.bfloat16)
    return jnp.dot(active, down_weight, preferred_element_type=jnp.float32).astype(jnp.bfloat16)


def shards(tokens, norm_gain, routes, route_logits, w_gate, w_up, w_down):
    tok_rows = tokens.shape[0]
    width = tokens.shape[1]
    n_experts = lax.axis_size(EP)
    capacity = max(2, 2 * tok_rows * TOP_K // n_experts)
    slot_count = n_experts * capacity
    normed = rmsnorm(tokens, norm_gain)
    route_weights = jax.nn.softmax(route_logits, axis=-1)
    slot_ids = jnp.arange(slot_count, dtype=jnp.int32)
    chosen = routes.reshape(-1)
    onehot = (chosen[:, None] == jnp.arange(n_experts, dtype=jnp.int32)[None, :]).astype(jnp.int32)
    within = jnp.sum(jnp.cumsum(onehot, axis=0) * onehot, axis=1) - 1
    slot_of = chosen * capacity + within
    placing = (slot_of[:, None] == slot_ids[None, :]).astype(jnp.bfloat16)
    repeated = jnp.repeat(normed, TOP_K, axis=0)
    outgoing = jnp.einsum("ps,pd->sd", placing, repeated, preferred_element_type=jnp.float32)
    outgoing = outgoing.astype(jnp.bfloat16).reshape(n_experts, capacity, width)
    arrived = lax.all_to_all(outgoing, EP, split_axis=0, concat_axis=0, tiled=True)
    count = arrived.shape[1]
    rows_in = arrived.reshape(n_experts * count, width)
    result = expert(rows_in, w_gate[0], w_up[0], w_down[0]).reshape(n_experts, count, width)
    returned_rows = exchange_by_chip(result, ("ep_0", "ep_1"), (0, 1), 0, 0)
    returned_rows = returned_rows.reshape(slot_count, width)
    picked = jnp.dot(placing, returned_rows, preferred_element_type=jnp.float32)
    total = jnp.sum(picked.reshape(tok_rows, TOP_K, width) * route_weights[:, :, None], axis=1)
    return total.astype(jnp.bfloat16)


def solution(mesh):
    split = Mesh(mesh.devices.reshape(mesh.shape["grp"], 16, 2), ("grp", "ep_0", "ep_1"))
    placed = (
        P(GRP_EP, None),
        P(),
        P(GRP_EP, None),
        P(GRP_EP, None),
        P(EP, None, None),
        P(EP, None, None),
        P(EP, None, None),
    )
    return jax.shard_map(
        shards, mesh=split, in_specs=placed, out_specs=P(GRP_EP, None), check_vma=False
    )
```

profile of v0, /device:TPU:86, one launch (start us, length us, event | category | flops | bytes accessed | tf_op | source)
XLA Modules:
  0.0 153.2 jit_solution(4344165232778566368)
XLA Ops:
  0.0 0.8 copy.23
  0.8 0.1 eq.50
  0.9 0.1 fusion.43
  1.0 0.2 reduce_window_sum.11
  1.1 0.2 select_reduce_fusion
  1.3 1.0 fusion.36
  2.4 1.0 fusion.38
  3.4 0.2 broadcast_in_dim.2
  3.6 0.1 reshape.59
  3.8 0.5 fusion.24
  4.3 72.9 %all_to_all.15 = bf16[32,8,2048]{2,1,0:T(8,128)(2,1)S(1)} all-to-all(bf16[32,8,2048]{2,1,0:T(8,128)(2,1)S(1)} %fusion.24), channel_id=1, replica_groups=mesh['grp'=4,'ep_0'=16,'ep_1'=2] {'ep_0','ep_1'}, dimensions={0} | all-to-all | bytes 2097152 | tf_op jit(solution)/shard_map/all_to_all | solution.py:68
  77.2 5.2 %fusion.9 = f32[256,1792]{1,0:T(8,128)S(1)} fusion(bf16[1,2048,1792]{2,1,0:T(8,128)(2,1)} %param.11, bf16[32,8,2048]{2,1,0:T(8,128)(2,1)S(1)} %all_to_all.15), kind=kOutput, calls=%fused_computation.7 | convolution fusion | flops 1879506944 | bytes 10223616 | tf_op jit(solution)/shard_map/dot_general | solution.py:45
  82.4 10.8 %fusion.21 = bf16[256,2048]{1,0:T(8,128)(2,1)} fusion(bf16[1,1792,2048]{2,1,0:T(8,128)(2,1)} %param.13, bf16[1,2048,1792]{2,1,0:T(8,128)(2,1)} %param.12, f32[256,1792]{1,0:T(8,128)S(1)} %fusion.9, bf16[32,8,2048]{2,1,0:T(8,128)(2,1)S(1)} %all_to_all.15), kind=kOutput, calls=%fused_computation.11 | convolution fusion | flops 3762749440 | bytes 18612224 | tf_op jit(solution)/shard_map/dot_general | solution.py:48
  93.2 0.0 copy-start
  93.2 0.0 copy-start.1
  93.2 4.2 %all-to-all-start.1 = ((bf16[16,2,1,8,2048]{4,3,1,2,0:T(8,128)(2,1)}), bf16[16,2,1,8,2048]{4,3,1,2,0:T(8,128)(2,1)S(1)}, u32[]{:S(2)}, u32[]{:S(2)}) async-start(bf16[16,2,1,8,2048]{4,3,1,2,0:T(8,128)(2,1)} %bitcast.7), calls=%async_computation.1 | async-start | bytes 2097152 | tf_op jit(solution)/shard_map/all_to_all | solution.py:28
  97.4 0.1 sub.15
  97.5 0.1 copy.24
  97.6 0.0 copy-done
  97.7 0.0 copy-done.1
  97.7 49.7 %all-to-all-done.1 = bf16[16,2,1,8,2048]{4,3,1,2,0:T(8,128)(2,1)S(1)} async-done(((bf16[16,2,1,8,2048]{4,3,1,2,0:T(8,128)(2,1)}), bf16[16,2,1,8,2048]{4,3,1,2,0:T(8,128)(2,1)S(1)}, u32[]{:S(2)}, u32[]{:S(2)}) %all-to-all-start.1) | async-done | bytes 1048608 | tf_op jit(solution)/shard_map/all_to_all | solution.py:28
  147.4 0.1 copy.26
  147.5 4.6 %all_to_all.16 = bf16[16,2,1,8,2048]{4,3,0,2,1:T(8,128)(2,1)S(1)} all-to-all(bf16[16,2,1,8,2048]{4,3,0,2,1:T(8,128)(2,1)S(1)} %copy.26), channel_id=1, replica_groups=mesh['grp'=4,'ep_0'=16,'ep_1'=2] {'ep_1'}, dimensions={1} | all-to-all | bytes 2097152 | tf_op jit(solution)/shard_map/all_to_all | solution.py:28
  152.1 0.1 copy.27
  152.2 1.0 fusion.25
  (6 shorter events, 0.1 us)
Async XLA Ops:
  93.2 4.4 %copy-start = (f32[32,4]{0,1:T(4,128)S(1)}, f32[32,4]{0,1:T(4,128)}, u32[]{:S(2)}) copy-start(f32[32,4]{0,1:T(4,128)} %param.10) | copy-start | bytes 1540
  93.2 4.5 %copy-start.1 = (s32[32,4]{0,1:T(4,128)S(1)}, s32[32,4]{0,1:T(4,128)}, u32[]{:S(2)}) copy-start(s32[32,4]{0,1:T(4,128)} %param.9) | copy-start | bytes 1540
  93.2 54.2 %all-to-all-start.1 = ((bf16[16,2,1,8,2048]{4,3,1,2,0:T(8,128)(2,1)}), bf16[16,2,1,8,2048]{4,3,1,2,0:T(8,128)(2,1)S(1)}, u32[]{:S(2)}, u32[]{:S(2)}) async-start(bf16[16,2,1,8,2048]{4,3,1,2,0:T(8,128)(2,1)} %bitcast.7), calls=%async_computation.1 | async-start | bytes 2097152 | tf_op jit(solution)/shard_map/all_to_all | solution.py:28
where the time goes:
time: 155 us; the launch traced here: 153 us
  blocking collectives  77.5 us (50%)
  waiting for transfers between devices  49.7 us (32%)
  matrix products  17.5 us (11%)
  starting transfers between devices  4.23 us (3%)
  other arithmetic  2.56 us (2%)
  local copies, waits for them, and re-layouts  1.56 us (1%)
    all_to_all x1, blocking collectives, shards(): lax.all_to_all(outgoing, EP, split_axis=0, concat_axis=0, tiled=True)  72.9 us
    all_to_all x1, waiting for transfers between devices, turned_blocks(): out = lax.all_to_all(out, axes[k], k, k, tiled=True)  49.7 us
    dot_general x1, matrix products, expert(): jnp.dot(active, down_weight, preferred_element_type=jnp.float32)  10.8 us
    dot_general x1, matrix products, expert(): jnp.dot(rows, gate_weight, preferred_element_type=jnp.float32)  5.15 us
    all_to_all x1, blocking collectives, turned_blocks(): out = lax.all_to_all(out, axes[k], k, k, tiled=True)  4.59 us
    all_to_all x1, starting transfers between devices, turned_blocks(): out = lax.all_to_all(out, axes[k], k, k, tiled=True)  4.23 us
  transfers between devices with their start and end apart: 1, of which 1 were waited for; matrix products, arithmetic and copies ran while one was open for 0% of the time, Pallas kernels for 0%

commit v1 on v0

--- a/solution.py
+++ b/solution.py
@@ -7,32 +7,6 @@
 TOP_K = 4
 EP = ("ep_0", "ep_1")
 GRP_EP = ("grp", "ep_0", "ep_1")
-
-
-def cut_along(x, dim, devices):
-    lengths = x.shape
-    pieces = x.reshape(*lengths[:dim], devices, lengths[dim] // devices, *lengths[dim + 1 :])
-    return jnp.moveaxis(pieces, dim, 0)
-
-
-def in_order(pieces, dim):
-    lengths = list(pieces.shape[1:])
-    lengths[dim] *= pieces.shape[0]
-    return jnp.moveaxis(pieces, 0, dim).reshape(lengths)
-
-
-def turned_blocks(pieces, axes, order):
-    inside = pieces.shape[1:]
-    out = pieces.reshape(*(lax.axis_size(a) for a in axes), *inside)
-    for k in order:
-        out = lax.all_to_all(out, axes[k], k, k, tiled=True)
-    return out.reshape(-1, *inside)
-
-
-def exchange_by_chip(x, groups, order, split_dim, concat_dim):
-    devices = lax.axis_size(groups[0]) * lax.axis_size(groups[1])
-    pieces = cut_along(x, split_dim, devices)
-    return in_order(turned_blocks(pieces, groups, order), concat_dim)
 
 
 def rmsnorm(values, gain):
@@ -69,7 +43,7 @@
     count = arrived.shape[1]
     rows_in = arrived.reshape(n_experts * count, width)
     result = expert(rows_in, w_gate[0], w_up[0], w_down[0]).reshape(n_experts, count, width)
-    returned_rows = exchange_by_chip(result, ("ep_0", "ep_1"), (0, 1), 0, 0)
+    returned_rows = lax.all_to_all(result, EP, split_axis=0, concat_axis=0, tiled=True)
     returned_rows = returned_rows.reshape(slot_count, width)
     picked = jnp.dot(placing, returned_rows, preferred_element_type=jnp.float32)
     total = jnp.sum(picked.reshape(tok_rows, TOP_K, width) * route_weights[:, :, None], axis=1)

time: 155 us -> 156 us (level)
  waiting for transfers between devices: 49.7 us -> 55.4 us
  blocking collectives: 77.5 us -> 72.9 us
    all_to_all x1, waiting for transfers between devices: 49.7 us -> 55.4 us  [shards(): lax.all_to_all(result, EP, split_axis=0, concat_axis=0, tiled=True)]
    all_to_all x1 -> x0, blocking collectives: 4.59 us -> none  [turned_blocks(): out = lax.all_to_all(out, axes[k], k, k, tiled=True)]
where the time goes in v1:
time: 156 us; the launch traced here: 155 us
  blocking collectives  72.9 us (47%)
  waiting for transfers between devices  55.4 us (36%)
  matrix products  17.5 us (11%)
  starting transfers between devices  4.98 us (3%)
  other arithmetic  2.56 us (2%)
    all_to_all x1, blocking collectives, shards(): lax.all_to_all(outgoing, EP, split_axis=0, concat_axis=0, tiled=True)  72.9 us
    all_to_all x1, waiting for transfers between devices, shards(): lax.all_to_all(result, EP, split_axis=0, concat_axis=0, tiled=True)  55.4 us
    dot_general x1, matrix products, expert(): jnp.dot(active, down_weight, preferred_element_type=jnp.float32)  10.8 us
    dot_general x1, matrix products, expert(): jnp.dot(rows, gate_weight, preferred_element_type=jnp.float32)  5.15 us
    all_to_all x1, starting transfers between devices, shards(): lax.all_to_all(result, EP, split_axis=0, concat_axis=0, tiled=True)  4.98 us
  transfers between devices with their start and end apart: 1, of which 1 were waited for; matrix products, arithmetic and copies ran while one was open for 0% of the time, Pallas kernels for 0%

profile of v1, /device:TPU:86, one launch (start us, length us, event | category | flops | bytes accessed | tf_op | source)
XLA Modules:
  0.0 154.9 jit_solution(13537507260134202245)
XLA Ops:
  0.0 0.8 copy.16
  0.8 0.1 eq.50
  0.9 0.1 fusion.46
  1.0 0.2 reduce_window_sum.11
  1.1 0.2 select_reduce_fusion
  1.3 1.0 fusion.39
  2.4 1.0 fusion.41
  3.4 0.2 broadcast_in_dim.2
  3.6 0.1 reshape.65
  3.8 0.5 fusion.24
  4.3 72.9 %all_to_all.10 = bf16[32,8,2048]{2,1,0:T(8,128)(2,1)S(1)} all-to-all(bf16[32,8,2048]{2,1,0:T(8,128)(2,1)S(1)} %fusion.24), channel_id=1, replica_groups=mesh['grp'=4,'ep_0'=16,'ep_1'=2] {'ep_0','ep_1'}, dimensions={0} | all-to-all | bytes 2097152 | tf_op jit(solution)/shard_map/all_to_all | solution.py:42
  77.2 5.2 %fusion.9 = f32[256,1792]{1,0:T(8,128)S(1)} fusion(bf16[1,2048,1792]{2,1,0:T(8,128)(2,1)} %param.11, bf16[32,8,2048]{2,1,0:T(8,128)(2,1)S(1)} %all_to_all.10), kind=kOutput, calls=%fused_computation.7 | convolution fusion | flops 1879506944 | bytes 10223616 | tf_op jit(solution)/shard_map/dot_general | solution.py:19
  82.4 10.8 %fusion.25 = bf16[32,8,2048]{2,1,0:T(8,128)(2,1)} fusion(bf16[1,1792,2048]{2,1,0:T(8,128)(2,1)} %param.13, bf16[1,2048,1792]{2,1,0:T(8,128)(2,1)} %param.12, f32[256,1792]{1,0:T(8,128)S(1)} %fusion.9, bf16[32,8,2048]{2,1,0:T(8,128)(2,1)S(1)} %all_to_all.10), kind=kOutput, calls=%fused_computation.14 | convolution fusion | flops 3762749440 | bytes 18612224 | tf_op jit(solution)/shard_map/dot_general | solution.py:22
  93.2 0.0 copy-start
  93.2 0.0 copy-start.1
  93.2 5.0 %all-to-all-start.1 = ((bf16[32,8,2048]{2,1,0:T(8,128)(2,1)}), bf16[32,8,2048]{2,1,0:T(8,128)(2,1)S(1)}, u32[]{:S(2)}, u32[]{:S(2)}) async-start(bf16[32,8,2048]{2,1,0:T(8,128)(2,1)} %fusion.25), calls=%async_computation.1 | async-start | bytes 2097152 | tf_op jit(solution)/shard_map/all_to_all | solution.py:46
  98.2 0.1 sub.15
  98.3 0.1 copy.17
  98.4 0.0 copy-done
  98.4 0.0 copy-done.1
  98.5 55.4 %all-to-all-done.1 = bf16[32,8,2048]{2,1,0:T(8,128)(2,1)S(1)} async-done(((bf16[32,8,2048]{2,1,0:T(8,128)(2,1)}), bf16[32,8,2048]{2,1,0:T(8,128)(2,1)S(1)}, u32[]{:S(2)}, u32[]{:S(2)}) %all-to-all-start.1) | async-done | bytes 1048608 | tf_op jit(solution)/shard_map/all_to_all | solution.py:46
  153.9 1.0 fusion.28
  (6 shorter events, 0.1 us)
Async XLA Ops:
  93.2 5.2 %copy-start = (f32[32,4]{0,1:T(4,128)S(1)}, f32[32,4]{0,1:T(4,128)}, u32[]{:S(2)}) copy-start(f32[32,4]{0,1:T(4,128)} %param.10) | copy-start | bytes 1540
  93.2 5.2 %copy-start.1 = (s32[32,4]{0,1:T(4,128)S(1)}, s32[32,4]{0,1:T(4,128)}, u32[]{:S(2)}) copy-start(s32[32,4]{0,1:T(4,128)} %param.9) | copy-start | bytes 1540
  93.2 60.7 %all-to-all-start.1 = ((bf16[32,8,2048]{2,1,0:T(8,128)(2,1)}), bf16[32,8,2048]{2,1,0:T(8,128)(2,1)S(1)}, u32[]{:S(2)}, u32[]{:S(2)}) async-start(bf16[32,8,2048]{2,1,0:T(8,128)(2,1)} %fusion.25), calls=%async_computation.1 | async-start | bytes 2097152 | tf_op jit(solution)/shard_map/all_to_all | solution.py:46

commit v2 on v1

v2 whole, which is shorter than its diff:
```python
import functools

import jax
import jax.numpy as jnp
from jax import lax
from jax.experimental import pallas as pl
from jax.experimental.pallas import tpu as pltpu
from jax.sharding import Mesh
from jax.sharding import PartitionSpec as P

HOP = 5
NEAR = (-2, -1, 0, 1, 2)
GRP_EP = ("grp", "z", "c")
META = 128
LIMIT = 16 << 20
VMEM = pl.BlockSpec(memory_space=pltpu.VMEM)
SMEM = pl.BlockSpec(memory_space=pltpu.SMEM)


def call(body, out_shape, n_in, smem=0, limit=LIMIT, scratch=(), flops=1 << 20):
    return pl.pallas_call(
        body,
        out_shape=out_shape,
        in_specs=[SMEM] * smem + [VMEM] * (n_in - smem),
        scratch_shapes=scratch,
        compiler_params=pltpu.CompilerParams(vmem_limit_bytes=limit),
        cost_estimate=pl.CostEstimate(flops=flops, bytes_accessed=1 << 20, transcendentals=0),
    )


def prepare(cap, tok_ref, gain_ref, routes_ref, logits_ref, out_ref):
    rows, width = tok_ref.shape
    top = routes_ref.shape[1]
    x = tok_ref[...].astype(jnp.float32)
    scale = lax.rsqrt(jnp.mean(x * x, axis=-1, keepdims=True) + 1e-06)
    out_ref[:, :width] = (x * scale * gain_ref[...]).astype(jnp.bfloat16)
    lane = lax.broadcasted_iota(jnp.int32, (rows, META), 1)
    routes = routes_ref[...]
    named = jnp.zeros((rows, META), jnp.float32)
    for k in range(top):
        named += jnp.where(lane == routes[:, k : k + 1], 1.0, 0.0)
    before = lax.broadcasted_iota(jnp.int32, (rows, rows), 0) > lax.broadcasted_iota(
        jnp.int32, (rows, rows), 1
    )
    earlier = jnp.dot(
        before.astype(jnp.float32).astype(jnp.bfloat16),
        named.astype(jnp.bfloat16),
        preferred_element_type=jnp.float32,
    )
    logits = logits_ref[...]
    powers = jnp.exp(logits - jnp.max(logits, axis=-1, keepdims=True))
    weights = powers / jnp.sum(powers, axis=-1, keepdims=True)
    high = weights.astype(jnp.bfloat16).astype(jnp.float32)
    low = weights - high
    meta = jnp.zeros((rows, META), jnp.float32)
    for k in range(top):
        hit = lane == routes[:, k : k + 1]
        rank = jnp.sum(jnp.where(hit, earlier, 0.0), axis=-1, keepdims=True)
        key = routes[:, k : k + 1].astype(jnp.float32) * cap + rank
        meta = jnp.where(lane == k, key, meta)
        meta = jnp.where(lane == top + k, high[:, k : k + 1], meta)
        meta = jnp.where(lane == 2 * top + k, low[:, k : k + 1], meta)
    out_ref[:, width:] = meta.astype(jnp.bfloat16)


def hand_on(chips, cap, top, place_ref, *refs):
    sources, refs = refs[:6], refs[6:]
    blocks, (high_ref, low_ref, all_ref) = refs[:6], refs[6:]
    rows = sources[0].shape[0]
    width = blocks[0].shape[1]
    z, c = place_ref[0], place_ref[1]
    near = 6 * cap
    slots = len(NEAR) * near + 2 * cap
    col = lax.broadcasted_iota(jnp.int32, (1, slots), 1)
    block = sum((col >= near * i).astype(jnp.int32) for i in range(1, len(NEAR) + 1))
    inside = col - block * near
    source = sum((inside >= cap * i).astype(jnp.int32) for i in range(1, 6))
    slot = inside - source * cap
    across = block == len(NEAR)
    source = jnp.where(across, source + jnp.where(c == 0, 2, 4), source)
    step = jnp.where(across, jnp.where(c == 0, 3, -3), block + NEAR[0])
    chip = z + step
    chip = jnp.where(chip < 0, chip + chips, chip)
    chip = jnp.where(chip >= chips, chip - chips, chip)
    target = ((2 * chip + c) * cap + slot + source * 2 * chips * cap).astype(jnp.float32)
    for s in range(6):
        all_ref[s * rows : (s + 1) * rows, :] = sources[s][...]
    meta = all_ref[:, width:].astype(jnp.float32)
    offset = (lax.broadcasted_iota(jnp.int32, (6 * rows, 1), 0) // rows * (2 * chips * cap)).astype(
        jnp.float32
    )
    pick = jnp.zeros((6 * rows, slots), jnp.float32)
    high, low = pick, pick
    for k in range(top):
        hit = meta[:, k : k + 1] + offset == target
        pick = jnp.where(hit, 1.0, pick)
        high = jnp.where(hit, meta[:, top + k : top + k + 1], high)
        low = jnp.where(hit, meta[:, 2 * top + k : 2 * top + k + 1], low)
    high_ref[...] = high.astype(jnp.bfloat16)
    low_ref[...] = low.astype(jnp.bfloat16)
    taken = lax.dot_general(
        pick.astype(jnp.bfloat16),
        all_ref[:, :width],
        (((0,), (0,)), ((), ())),
        preferred_element_type=jnp.float32,
    ).astype(jnp.bfloat16)
    for i in range(len(NEAR)):
        blocks[i][...] = taken[i * near : (i + 1) * near]
    blocks[5][...] = taken[len(NEAR) * near :]


def experts(tile, *refs):
    blocks, (gate_ref, up_ref, down_ref), refs = refs[:6], refs[6:9], refs[9:]
    outs, (x_ref, total_ref) = refs[:6], refs[6:]
    at = 0
    for b in blocks:
        x_ref[at : at + b.shape[0], :] = b[...]
        at += b.shape[0]
    hidden = gate_ref.shape[1]
    total_ref[...] = jnp.zeros_like(total_ref)

    @pl.loop(0, hidden // tile)
    def _(i):
        cols = pl.ds(pl.multiple_of(i * tile, tile), tile)
        x = x_ref[...]
        gate = jnp.minimum(jnp.dot(x, gate_ref[:, cols], preferred_element_type=jnp.float32), 7.0)
        upper = jnp.clip(
            jnp.dot(x, up_ref[:, cols], preferred_element_type=jnp.float32), -7.0, 7.0
        )
        active = (gate * jax.nn.sigmoid(1.702 * gate) * (upper + 1.0)).astype(jnp.bfloat16)
        total_ref[...] += jnp.dot(active, down_ref[cols, :], preferred_element_type=jnp.float32)

    at = 0
    for o in outs:
        o[...] = total_ref[at : at + o.shape[0], :].astype(jnp.bfloat16)
        at += o.shape[0]


def weigh(*refs):
    blocks, (high_ref, low_ref), refs = refs[:6], refs[6:8], refs[8:]
    far_mine, far_other, mine, other, x_ref = refs
    at = 0
    for b in blocks:
        x_ref[at : at + b.shape[0], :] = b[...]
        at += b.shape[0]
    x = x_ref[...]
    total = jnp.dot(high_ref[...], x, preferred_element_type=jnp.float32)
    total += jnp.dot(low_ref[...], x, preferred_element_type=jnp.float32)
    rows = mine.shape[0]
    mine[...] = total[:rows]
    other[...] = total[rows : 2 * rows].astype(jnp.bfloat16)
    for i in range(2):
        far_mine[i * rows : (i + 1) * rows, :] = total[(2 + 2 * i) * rows : (3 + 2 * i) * rows]
        far_other[i * rows : (i + 1) * rows, :] = total[
            (3 + 2 * i) * rows : (4 + 2 * i) * rows
        ].astype(jnp.bfloat16)


def join(mine, other, one, two):
    rows = one.shape[0]
    total = mine[...] + other[...].astype(jnp.float32)
    one[...] = total[:rows].astype(jnp.bfloat16)
    two[...] = total[rows:].astype(jnp.bfloat16)


def finish(mine, other, one, two, out):
    total = mine[...] + other[...].astype(jnp.float32)
    total += one[...].astype(jnp.float32) + two[...].astype(jnp.float32)
    out[...] = total.astype(jnp.bfloat16)


def shards(tokens, norm_gain, routes, route_logits, w_gate, w_up, w_down):
    rows, width = tokens.shape
    top = routes.shape[1]
    chips = lax.axis_size("z")
    cap = max(2, 2 * rows * top // (2 * chips))
    hidden = w_gate.shape[2]
    bf16 = lambda *shape: jax.ShapeDtypeStruct(shape, jnp.bfloat16)
    f32 = lambda *shape: jax.ShapeDtypeStruct(shape, jnp.float32)

    def shift(x, by):
        return lax.ppermute(x, "z", [(i, (i + by) % chips) for i in range(chips)])

    def across(x, sign):
        pairs = []
        for i in range(chips):
            pairs.append((2 * i, (i + 3 * sign) % chips * 2))
            pairs.append((2 * i + 1, (i - 3 * sign) % chips * 2 + 1))
        return lax.ppermute(x, ("z", "c"), pairs)

    def swap(x):
        return lax.ppermute(x, "c", [(0, 1), (1, 0)])

    place = jnp.stack([lax.axis_index("z"), lax.axis_index("c")]).astype(jnp.int32)
    own = call(functools.partial(prepare, cap), bf16(rows, width + META), 4)(
        tokens, norm_gain[None, :], routes, route_logits
    )
    low, high = shift(own, HOP), shift(own, -HOP)
    own2, low2, high2 = swap(own), swap(low), swap(high)
    near = 6 * cap
    slots = len(NEAR) * near + 2 * cap
    shapes = [bf16(near, width)] * len(NEAR) + [bf16(2 * cap, width)]
    weight = bf16(6 * rows, slots)
    *blocks, w_high, w_low = call(
        functools.partial(hand_on, chips, cap, top),
        shapes + [weight, weight],
        7,
        smem=1,
        scratch=[pltpu.VMEM((6 * rows, width + META), jnp.bfloat16)],
    )(place, own, own2, low, low2, high, high2)
    given = [shift(b, d) if d else b for b, d in zip(blocks, NEAR)] + [across(blocks[5], 1)]
    results = call(
        functools.partial(experts, 256),
        shapes,
        9,
        limit=56 << 20,
        scratch=[pltpu.VMEM((slots, width), jnp.bfloat16), pltpu.VMEM((slots, width), jnp.float32)],
        flops=6 * slots * width * hidden,
    )(*given, w_gate[0], w_up[0], w_down[0])
    back = [shift(b, -d) if d else b for b, d in zip(results, NEAR)] + [across(results[5], -1)]
    far_mine, far_other, mine, other = call(
        weigh,
        [f32(2 * rows, width), bf16(2 * rows, width), f32(rows, width), bf16(rows, width)],
        8,
        scratch=[pltpu.VMEM((slots, width), jnp.bfloat16)],
    )(*back, w_high, w_low)
    one, two = call(join, [bf16(rows, width)] * 2, 2)(far_mine, swap(far_other))
    return call(finish, bf16(rows, width), 4)(mine, swap(other), shift(one, -HOP), shift(two, HOP))


def solution(mesh):
    chips = mesh.shape["ep"] // 2
    split = Mesh(mesh.devices.reshape(mesh.shape["grp"], chips, 2), GRP_EP)
    ep = ("z", "c")
    placed = (
        P(GRP_EP, None),
        P(),
        P(GRP_EP, None),
        P(GRP_EP, None),
        P(ep, None, None),
        P(ep, None, None),
        P(ep, None, None),
    )
    return jax.shard_map(
        shards, mesh=split, in_specs=placed, out_specs=P(GRP_EP, None), check_vma=False
    )
```

time: 156 us -> 125 us (0.80)
  blocking collectives: 72.9 us -> 0 us
  starting transfers between devices: 4.98 us -> 37.9 us
  Pallas kernels: 0 us -> 19.7 us
  matrix products: 17.5 us -> 0 us
  waiting for transfers between devices: 55.4 us -> 59.7 us
  local copies, waits for them, and re-layouts: 1.39 us -> 5.55 us
  other arithmetic: 2.56 us -> 0.07 us
    all_to_all x1 -> x0, blocking collectives: 72.9 us -> none  [shards(): lax.all_to_all(outgoing, EP, split_axis=0, concat_axis=0, tiled=True)]
    ppermute x0 -> x19, waiting for transfers between devices: none -> 59.7 us  [the longest x12 37.6 us: shift(): return lax.ppermute(x, 'z', [(i, (i + by) % chips) for i in range(chips)])]
    all_to_all x1 -> x0, waiting for transfers between devices: 55.4 us -> none  [shards(): lax.all_to_all(result, EP, split_axis=0, concat_axis=0, tiled=True)]
    ppermute x0 -> x19, starting transfers between devices: none -> 37.9 us  [the longest x12 33.2 us: shift(): return lax.ppermute(x, 'z', [(i, (i + by) % chips) for i in range(chips)])]
    pallas_call x0 -> x6, Pallas kernels: none -> 19.7 us  [the longest x1 16.6 us: shards(): call(functools.partial(experts, 256), shapes, 9, limit=56 << 20, scratch=...]
    dot_general x4 -> x0, matrix products: 17.5 us -> none  [the longest x1 10.8 us: expert(): jnp.dot(active, down_weight, preferred_element_type=jnp.float32)]
    all_to_all x1 -> x0, starting transfers between devices: 4.98 us -> none  [shards(): lax.all_to_all(result, EP, split_axis=0, concat_axis=0, tiled=True)]
    unnamed x5 -> x20, local copies, waits for them, and re-layouts: 0.77 us -> 5.55 us
  transfers between devices with their start and end apart: 1 -> 19, of which waited for: 1 -> 9; matrix products, arithmetic and copies ran while one was open for 0% -> 0% of each run, Pallas kernels for 0% -> 0%
where the time goes in v2:
time: 125 us; the launch traced here: 123 us
  waiting for transfers between devices  59.7 us (48%)
  starting transfers between devices  37.9 us (30%)
  Pallas kernels  19.7 us (16%)
  local copies, waits for them, and re-layouts  5.55 us (4%)
    ppermute x12, waiting for transfers between devices, shift(): return lax.ppermute(x, 'z', [(i, (i + by) % chips) for i in range(chips)])  37.6 us
    ppermute x12, starting transfers between devices, shift(): return lax.ppermute(x, 'z', [(i, (i + by) % chips) for i in range(chips)])  33.2 us
    ppermute x2, waiting for transfers between devices, across(): return lax.ppermute(x, ('z', 'c'), pairs)  19.8 us
    pallas_call x1, Pallas kernels, shards(): call(functools.partial(experts, 256), shapes, 9, limit=56 << 20, scratch=...  16.6 us
    unnamed x20, local copies, waits for them, and re-layouts  5.55 us
    ppermute x2, starting transfers between devices, across(): return lax.ppermute(x, ('z', 'c'), pairs)  4.07 us
  transfers between devices with their start and end apart: 19, of which 9 were waited for; matrix products, arithmetic and copies ran while one was open for 0% of the time, Pallas kernels for 0%

profile of v2, /device:TPU:86, one launch (start us, length us, event | category | flops | bytes accessed | tf_op | source)
XLA Modules:
  0.0 123.1 jit_solution(18434309106133736785)
XLA Ops:
  0.0 0.8 copy.8.routes_ref
  0.8 0.8 copy.9.logits_ref
  1.5 0.0 copy-start.2
  1.5 0.9 copy-done.2
  2.4 0.0 copy-start.3
  2.4 0.7 copy-done.3
  3.1 0.5 shard_map.73.refs_0_
  3.6 14.8 %collective-permute-start.3 = (bf16[32,2176]{1,0:T(8,128)(2,1)S(1)}, bf16[32,2176]{1,0:T(8,128)(2,1)S(1)}, u32[]{:S(2)}, u32[]{:S(2)}) collective-permute-start(bf16[32,2176]{1,0:T(8,128)(2,1)S(1)} %shard_map.73.refs_0_), channel_id=1, source_target_pairs={{0,22},{2,24},{4,26},{6,28},{8,30},{10,0},{12,2},{14,4},{16,6},{18... | collective-permute-start | bytes 417800 | tf_op jit(solution)/shard_map/ppermute | solution.py:182
  18.4 0.0 collective-permute-start.1
  18.4 0.0 collective-permute-start
  18.4 14.5 %collective-permute-done.3.refs_4_ = bf16[32,2176]{1,0:T(8,128)(2,1)S(1)} collective-permute-done((bf16[32,2176]{1,0:T(8,128)(2,1)S(1)}, bf16[32,2176]{1,0:T(8,128)(2,1)S(1)}, u32[]{:S(2)}, u32[]{:S(2)}) %collective-permute-start.3) | collective-permute-done | bytes 139296 | tf_op jit(solution)/shard_map/ppermute | solution.py:182
  32.9 0.0 collective-permute-start.4
  33.0 7.6 %collective-permute-done.1.refs_2_ = bf16[32,2176]{1,0:T(8,128)(2,1)S(1)} collective-permute-done((bf16[32,2176]{1,0:T(8,128)(2,1)S(1)}, bf16[32,2176]{1,0:T(8,128)(2,1)S(1)}, u32[]{:S(2)}, u32[]{:S(2)}) %collective-permute-start.1) | collective-permute-done | bytes 139296 | tf_op jit(solution)/shard_map/ppermute | solution.py:182
  40.6 0.0 collective-permute-start.2
  40.6 0.1 pad_add_fusion.place_ref
  40.7 0.0 collective-permute-done.refs_1_
  40.7 0.0 collective-permute-done.4.refs_5_
  40.7 1.3 %collective-permute-done.2.refs_3_ = bf16[32,2176]{1,0:T(8,128)(2,1)S(1)} collective-permute-done((bf16[32,2176]{1,0:T(8,128)(2,1)S(1)}, bf16[32,2176]{1,0:T(8,128)(2,1)S(1)}, u32[]{:S(2)}, u32[]{:S(2)}) %collective-permute-start.2) | collective-permute-done | bytes 139296 | tf_op jit(solution)/shard_map/ppermute | solution.py:192
  42.0 1.3 %shard_map.74 = (bf16[48,2048]{1,0:T(8,128)(2,1)S(1)}, bf16[48,2048]{1,0:T(8,128)(2,1)S(1)}, bf16[48,2048]{1,0:T(8,128)(2,1)S(1)}, bf16[48,2048]{1,0:T(8,128)(2,...) custom-call(s32[2]{0:T(128)S(1)} %pad_add_fusion.place_ref, ...), custom_call_target="tpu_custom_call" | custom-call | flops 1048576 | bytes 1048576 | tf_op jit(solution)/shard_map/pallas_call | solution.py:204
  43.3 0.0 copy-start
  43.3 0.7 copy-done
  43.9 0.3 collective-permute-start.5
  44.3 0.0 collective-permute-start.6
  44.3 2.0 %collective-permute-start.7 = (bf16[48,2048]{1,0:T(8,128)(2,1)S(1)}, bf16[48,2048]{1,0:T(8,128)(2,1)S(1)}, u32[]{:S(2)}, u32[]{:S(2)}) collective-permute-start(bf16[48,2048]{1,0:T(8,128)(2,1)S(1)} %get-tuple-element.28), channel_id=1, source_target_pairs={{0,2},{2,4},{4,6},{6,8},{8,10},{10,12},{12,14},{14,16},{16,18},{18... | collective-permute-start | bytes 589832 | tf_op jit(solution)/shard_map/ppermute | solution.py:182
  46.3 2.6 %collective-permute-start.8 = (bf16[48,2048]{1,0:T(8,128)(2,1)S(1)}, bf16[48,2048]{1,0:T(8,128)(2,1)S(1)}, u32[]{:S(2)}, u32[]{:S(2)}) collective-permute-start(bf16[48,2048]{1,0:T(8,128)(2,1)S(1)} %get-tuple-element.29), channel_id=1, source_target_pairs={{0,4},{2,6},{4,8},{6,10},{8,12},{10,14},{12,16},{14,18},{16,20},{1... | collective-permute-start | bytes 589832 | tf_op jit(solution)/shard_map/ppermute | solution.py:182
  48.9 2.0 %collective-permute-start.9 = (bf16[16,2048]{1,0:T(8,128)(2,1)S(1)}, bf16[16,2048]{1,0:T(8,128)(2,1)S(1)}, u32[]{:S(2)}, u32[]{:S(2)}) collective-permute-start(bf16[16,2048]{1,0:T(8,128)(2,1)S(1)} %get-tuple-element.30), channel_id=1, source_target_pairs={{0,6},{1,27},{2,8},{3,29},{4,10},{5,31},{6,12},{7,1},{8,14},{9,3},... | collective-permute-start | bytes 196616 | tf_op jit(solution)/shard_map/ppermute | solution.py:189
  50.9 11.3 %collective-permute-done.9.refs_5_ = bf16[16,2048]{1,0:T(8,128)(2,1)S(1)} collective-permute-done((bf16[16,2048]{1,0:T(8,128)(2,1)S(1)}, bf16[16,2048]{1,0:T(8,128)(2,1)S(1)}, u32[]{:S(2)}, u32[]{:S(2)}) %collective-permute-start.9) | collective-permute-done | bytes 65568 | tf_op jit(solution)/shard_map/ppermute | solution.py:189
  62.2 0.0 copy-start.8
  62.2 0.0 collective-permute-done.5.refs_0_
  62.2 0.0 copy-start.4
  62.2 0.0 collective-permute-done.6.refs_1_
  62.2 0.0 copy-start.5
  62.2 0.0 collective-permute-done.7.refs_3_
  62.2 0.0 copy-start.6
  62.2 0.0 collective-permute-done.8.refs_4_
  62.2 0.0 copy-start.7
  62.3 0.6 copy-done.8
  62.8 0.1 copy-done.4
  62.9 0.1 copy-done.5
  63.0 0.1 copy-done.6
  63.0 0.1 copy-done.7
  63.1 16.6 %shard_map.75 = (bf16[48,2048]{1,0:T(8,128)(2,1)}, bf16[48,2048]{1,0:T(8,128)(2,1)}, bf16[48,2048]{1,0:T(8,128)(2,1)}, bf16[48,2048]{1,0:T(8,128)(2,1)}, bf16[48...) custom-call(bf16[48,2048]{1,0:T(8,128)(2,1)} %copy-done.4, bf16[48,2048]{1,0:T(8,128)(2,1)} %copy-done.5, ...), custom_call_target="tpu_custom_call" | custom-call | flops 5637144576 | bytes 1048576 | tf_op jit(solution)/shard_map/pallas_call | solution.py:212
  79.7 2.8 %collective-permute-start.10 = (bf16[48,2048]{1,0:T(8,128)(2,1)}, bf16[48,2048]{1,0:T(8,128)(2,1)S(1)}, u32[]{:S(2)}, u32[]{:S(2)}) collective-permute-start(bf16[48,2048]{1,0:T(8,128)(2,1)} %get-tuple-element.31), channel_id=1, source_target_pairs={{0,4},{2,6},{4,8},{6,10},{8,12},{10,14},{12,16},{14,18},{16,20},{1... | collective-permute-start | bytes 589832 | tf_op jit(solution)/shard_map/ppermute | solution.py:182
  82.6 0.0 collective-permute-start.11
  82.6 3.2 %collective-permute-start.12 = (bf16[48,2048]{1,0:T(8,128)(2,1)}, bf16[48,2048]{1,0:T(8,128)(2,1)S(1)}, u32[]{:S(2)}, u32[]{:S(2)}) collective-permute-start(bf16[48,2048]{1,0:T(8,128)(2,1)} %get-tuple-element.34), channel_id=1, source_target_pairs={{0,30},{2,0},{4,2},{6,4},{8,6},{10,8},{12,10},{14,12},{16,14},{18,... | collective-permute-start | bytes 589832 | tf_op jit(solution)/shard_map/ppermute | solution.py:182
  85.8 0.1 collective-permute-start.13
  85.9 2.0 %collective-permute-start.14 = (bf16[16,2048]{1,0:T(8,128)(2,1)}, bf16[16,2048]{1,0:T(8,128)(2,1)S(1)}, u32[]{:S(2)}, u32[]{:S(2)}) collective-permute-start(bf16[16,2048]{1,0:T(8,128)(2,1)} %get-tuple-element.36), channel_id=1, source_target_pairs={{0,26},{1,7},{2,28},{3,9},{4,30},{5,11},{6,0},{7,13},{8,2},{9,15},... | collective-permute-start | bytes 196616 | tf_op jit(solution)/shard_map/ppermute | solution.py:189
  87.9 8.5 %collective-permute-done.14.refs_5_ = bf16[16,2048]{1,0:T(8,128)(2,1)S(1)} collective-permute-done((bf16[16,2048]{1,0:T(8,128)(2,1)}, bf16[16,2048]{1,0:T(8,128)(2,1)S(1)}, u32[]{:S(2)}, u32[]{:S(2)}) %collective-permute-start.14) | collective-permute-done | bytes 65568 | tf_op jit(solution)/shard_map/ppermute | solution.py:189
  96.5 0.0 collective-permute-done.10.refs_0_
  96.5 0.0 collective-permute-done.11.refs_1_
  96.5 0.0 collective-permute-done.12.refs_3_
  96.5 0.5 collective-permute-done.13.refs_4_
  97.0 0.0 copy-start.1
  97.0 0.9 copy-done.1
  97.9 0.6 shard_map.76
  98.5 0.1 collective-permute-start.16
  98.7 0.5 collective-permute-start.15
  99.2 1.0 collective-permute-done.16.other
  100.2 6.1 %collective-permute-start.17 = (bf16[32,2048]{1,0:T(8,128)(2,1)S(1)}, bf16[32,2048]{1,0:T(8,128)(2,1)S(1)}, u32[]{:S(2)}, u32[]{:S(2)}) collective-permute-start(bf16[32,2048]{1,0:T(8,128)(2,1)S(1)} %get-tuple-element.43), channel_id=1, source_target_pairs={{0,22},{2,24},{4,26},{6,28},{8,30},{10,0},{12,2},{14,4},{16,6},{18... | collective-permute-start | bytes 393224 | tf_op jit(solution)/shard_map/ppermute | solution.py:182
  106.4 1.2 collective-permute-start.18
  107.5 0.0 collective-permute-done.15.other
  107.5 13.2 %collective-permute-done.17.one = bf16[32,2048]{1,0:T(8,128)(2,1)S(1)} collective-permute-done((bf16[32,2048]{1,0:T(8,128)(2,1)S(1)}, bf16[32,2048]{1,0:T(8,128)(2,1)S(1)}, u32[]{:S(2)}, u32[]{:S(2)}) %collective-permute-start.17) | collective-permute-done | bytes 131104 | tf_op jit(solution)/shard_map/ppermute | solution.py:182
  120.8 1.6 %collective-permute-done.18.two = bf16[32,2048]{1,0:T(8,128)(2,1)S(1)} collective-permute-done((bf16[32,2048]{1,0:T(8,128)(2,1)S(1)}, bf16[32,2048]{1,0:T(8,128)(2,1)S(1)}, u32[]{:S(2)}, u32[]{:S(2)}) %collective-permute-start.18) | collective-permute-done | bytes 131104 | tf_op jit(solution)/shard_map/ppermute | solution.py:182
  122.4 0.7 shard_map.78
  (1 shorter events, 0.0 us)
Async XLA Ops:
  1.5 0.9 copy-start.2
  2.4 0.7 copy-start.3
  3.6 29.3 %collective-permute-start.3 = (bf16[32,2176]{1,0:T(8,128)(2,1)S(1)}, bf16[32,2176]{1,0:T(8,128)(2,1)S(1)}, u32[]{:S(2)}, u32[]{:S(2)}) collective-permute-start(bf16[32,2176]{1,0:T(8,128)(2,1)S(1)} %shard_map.73.refs_0_), channel_id=1, source_target_pairs={{0,22},{2,24},{4,26},{6,28},{8,30},{10,0},{12,2},{14,4},{16,6},{18... | collective-permute-start | bytes 417800 | tf_op jit(solution)/shard_map/ppermute | solution.py:182
  18.4 22.2 %collective-permute-start.1 = (bf16[32,2176]{1,0:T(8,128)(2,1)S(1)}, bf16[32,2176]{1,0:T(8,128)(2,1)S(1)}, u32[]{:S(2)}, u32[]{:S(2)}) collective-permute-start(bf16[32,2176]{1,0:T(8,128)(2,1)S(1)} %shard_map.73.refs_0_), channel_id=1, source_target_pairs={{0,10},{2,12},{4,14},{6,16},{8,18},{10,20},{12,22},{14,24},{16,26}... | collective-permute-start | bytes 417800 | tf_op jit(solution)/shard_map/ppermute | solution.py:182
  18.4 22.3 %collective-permute-start = (bf16[32,2176]{1,0:T(8,128)(2,1)S(1)}, bf16[32,2176]{1,0:T(8,128)(2,1)S(1)}, u32[]{:S(2)}, u32[]{:S(2)}) collective-permute-start(bf16[32,2176]{1,0:T(8,128)(2,1)S(1)} %shard_map.73.refs_0_), channel_id=1, source_target_pairs={{0,1},{1,0},{2,3},{3,2},{4,5},{5,4},{6,7},{7,6},{8,9},{9,8},{10,11... | collective-permute-start | bytes 417800 | tf_op jit(solution)/shard_map/ppermute | solution.py:192
  32.9 7.7 %collective-permute-start.4 = (bf16[32,2176]{1,0:T(8,128)(2,1)S(1)}, bf16[32,2176]{1,0:T(8,128)(2,1)S(1)}, u32[]{:S(2)}, u32[]{:S(2)}) collective-permute-start(bf16[32,2176]{1,0:T(8,128)(2,1)S(1)} %collective-permute-done.3.refs_4_), channel_id=1, source_target_pairs={{0,1},{1,0},{2,3},{3,2},{4,5},{5,4},{6,7},{7,6},{8,9},{9,8},{10,11... | collective-permute-start | bytes 417800 | tf_op jit(solution)/shard_map/ppermute | solution.py:192
  40.6 1.4 %collective-permute-start.2 = (bf16[32,2176]{1,0:T(8,128)(2,1)S(1)}, bf16[32,2176]{1,0:T(8,128)(2,1)S(1)}, u32[]{:S(2)}, u32[]{:S(2)}) collective-permute-start(bf16[32,2176]{1,0:T(8,128)(2,1)S(1)} %collective-permute-done.1.refs_2_), channel_id=1, source_target_pairs={{0,1},{1,0},{2,3},{3,2},{4,5},{5,4},{6,7},{7,6},{8,9},{9,8},{10,11... | collective-permute-start | bytes 417800 | tf_op jit(solution)/shard_map/ppermute | solution.py:192
  43.3 0.7 copy-start
  43.9 18.3 %collective-permute-start.5 = (bf16[48,2048]{1,0:T(8,128)(2,1)S(1)}, bf16[48,2048]{1,0:T(8,128)(2,1)S(1)}, u32[]{:S(2)}, u32[]{:S(2)}) collective-permute-start(bf16[48,2048]{1,0:T(8,128)(2,1)S(1)} %get-tuple-element.25), channel_id=1, source_target_pairs={{0,28},{2,30},{4,0},{6,2},{8,4},{10,6},{12,8},{14,10},{16,12},{18,... | collective-permute-start | bytes 589832 | tf_op jit(solution)/shard_map/ppermute | solution.py:182
  44.3 17.9 %collective-permute-start.6 = (bf16[48,2048]{1,0:T(8,128)(2,1)S(1)}, bf16[48,2048]{1,0:T(8,128)(2,1)S(1)}, u32[]{:S(2)}, u32[]{:S(2)}) collective-permute-start(bf16[48,2048]{1,0:T(8,128)(2,1)S(1)} %get-tuple-element.26), channel_id=1, source_target_pairs={{0,30},{2,0},{4,2},{6,4},{8,6},{10,8},{12,10},{14,12},{16,14},{18,... | collective-permute-start | bytes 589832 | tf_op jit(solution)/shard_map/ppermute | solution.py:182
  44.3 18.0 %collective-permute-start.7 = (bf16[48,2048]{1,0:T(8,128)(2,1)S(1)}, bf16[48,2048]{1,0:T(8,128)(2,1)S(1)}, u32[]{:S(2)}, u32[]{:S(2)}) collective-permute-start(bf16[48,2048]{1,0:T(8,128)(2,1)S(1)} %get-tuple-element.28), channel_id=1, source_target_pairs={{0,2},{2,4},{4,6},{6,8},{8,10},{10,12},{12,14},{14,16},{16,18},{18... | collective-permute-start | bytes 589832 | tf_op jit(solution)/shard_map/ppermute | solution.py:182
  46.3 16.0 %collective-permute-start.8 = (bf16[48,2048]{1,0:T(8,128)(2,1)S(1)}, bf16[48,2048]{1,0:T(8,128)(2,1)S(1)}, u32[]{:S(2)}, u32[]{:S(2)}) collective-permute-start(bf16[48,2048]{1,0:T(8,128)(2,1)S(1)} %get-tuple-element.29), channel_id=1, source_target_pairs={{0,4},{2,6},{4,8},{6,10},{8,12},{10,14},{12,16},{14,18},{16,20},{1... | collective-permute-start | bytes 589832 | tf_op jit(solution)/shard_map/ppermute | solution.py:182
  48.9 13.3 %collective-permute-start.9 = (bf16[16,2048]{1,0:T(8,128)(2,1)S(1)}, bf16[16,2048]{1,0:T(8,128)(2,1)S(1)}, u32[]{:S(2)}, u32[]{:S(2)}) collective-permute-start(bf16[16,2048]{1,0:T(8,128)(2,1)S(1)} %get-tuple-element.30), channel_id=1, source_target_pairs={{0,6},{1,27},{2,8},{3,29},{4,10},{5,31},{6,12},{7,1},{8,14},{9,3},... | collective-permute-start | bytes 196616 | tf_op jit(solution)/shard_map/ppermute | solution.py:189
  62.2 0.6 copy-start.8
  62.2 0.7 copy-start.4
  62.2 0.7 copy-start.5
  62.2 0.8 copy-start.6
  62.2 0.8 copy-start.7
  79.7 16.7 %collective-permute-start.10 = (bf16[48,2048]{1,0:T(8,128)(2,1)}, bf16[48,2048]{1,0:T(8,128)(2,1)S(1)}, u32[]{:S(2)}, u32[]{:S(2)}) collective-permute-start(bf16[48,2048]{1,0:T(8,128)(2,1)} %get-tuple-element.31), channel_id=1, source_target_pairs={{0,4},{2,6},{4,8},{6,10},{8,12},{10,14},{12,16},{14,18},{16,20},{1... | collective-permute-start | bytes 589832 | tf_op jit(solution)/shard_map/ppermute | solution.py:182
  82.6 13.9 %collective-permute-start.11 = (bf16[48,2048]{1,0:T(8,128)(2,1)}, bf16[48,2048]{1,0:T(8,128)(2,1)S(1)}, u32[]{:S(2)}, u32[]{:S(2)}) collective-permute-start(bf16[48,2048]{1,0:T(8,128)(2,1)} %get-tuple-element.32), channel_id=1, source_target_pairs={{0,2},{2,4},{4,6},{6,8},{8,10},{10,12},{12,14},{14,16},{16,18},{18... | collective-permute-start | bytes 589832 | tf_op jit(solution)/shard_map/ppermute | solution.py:182
  82.6 13.9 %collective-permute-start.12 = (bf16[48,2048]{1,0:T(8,128)(2,1)}, bf16[48,2048]{1,0:T(8,128)(2,1)S(1)}, u32[]{:S(2)}, u32[]{:S(2)}) collective-permute-start(bf16[48,2048]{1,0:T(8,128)(2,1)} %get-tuple-element.34), channel_id=1, source_target_pairs={{0,30},{2,0},{4,2},{6,4},{8,6},{10,8},{12,10},{14,12},{16,14},{18,... | collective-permute-start | bytes 589832 | tf_op jit(solution)/shard_map/ppermute | solution.py:182
  85.8 11.2 %collective-permute-start.13 = (bf16[48,2048]{1,0:T(8,128)(2,1)}, bf16[48,2048]{1,0:T(8,128)(2,1)S(1)}, u32[]{:S(2)}, u32[]{:S(2)}) collective-permute-start(bf16[48,2048]{1,0:T(8,128)(2,1)} %get-tuple-element.35), channel_id=1, source_target_pairs={{0,28},{2,30},{4,0},{6,2},{8,4},{10,6},{12,8},{14,10},{16,12},{18,... | collective-permute-start | bytes 589832 | tf_op jit(solution)/shard_map/ppermute | solution.py:182
  85.9 10.6 %collective-permute-start.14 = (bf16[16,2048]{1,0:T(8,128)(2,1)}, bf16[16,2048]{1,0:T(8,128)(2,1)S(1)}, u32[]{:S(2)}, u32[]{:S(2)}) collective-permute-start(bf16[16,2048]{1,0:T(8,128)(2,1)} %get-tuple-element.36), channel_id=1, source_target_pairs={{0,26},{1,7},{2,28},{3,9},{4,30},{5,11},{6,0},{7,13},{8,2},{9,15},... | collective-permute-start | bytes 196616 | tf_op jit(solution)/shard_map/ppermute | solution.py:189
  97.0 0.9 copy-start.1
  98.5 1.7 %collective-permute-start.16 = (bf16[64,2048]{1,0:T(8,128)(2,1)S(1)}, bf16[64,2048]{1,0:T(8,128)(2,1)S(1)}, u32[]{:S(2)}, u32[]{:S(2)}) collective-permute-start(bf16[64,2048]{1,0:T(8,128)(2,1)S(1)} %get-tuple-element.42), channel_id=1, source_target_pairs={{0,1},{1,0},{2,3},{3,2},{4,5},{5,4},{6,7},{7,6},{8,9},{9,8},{10,11... | collective-permute-start | bytes 786440 | tf_op jit(solution)/shard_map/ppermute | solution.py:192
  98.7 8.9 %collective-permute-start.15 = (bf16[32,2048]{1,0:T(8,128)(2,1)S(1)}, bf16[32,2048]{1,0:T(8,128)(2,1)S(1)}, u32[]{:S(2)}, u32[]{:S(2)}) collective-permute-start(bf16[32,2048]{1,0:T(8,128)(2,1)S(1)} %get-tuple-element.40), channel_id=1, source_target_pairs={{0,1},{1,0},{2,3},{3,2},{4,5},{5,4},{6,7},{7,6},{8,9},{9,8},{10,11... | collective-permute-start | bytes 393224 | tf_op jit(solution)/shard_map/ppermute | solution.py:192
  100.2 20.5 %collective-permute-start.17 = (bf16[32,2048]{1,0:T(8,128)(2,1)S(1)}, bf16[32,2048]{1,0:T(8,128)(2,1)S(1)}, u32[]{:S(2)}, u32[]{:S(2)}) collective-permute-start(bf16[32,2048]{1,0:T(8,128)(2,1)S(1)} %get-tuple-element.43), channel_id=1, source_target_pairs={{0,22},{2,24},{4,26},{6,28},{8,30},{10,0},{12,2},{14,4},{16,6},{18... | collective-permute-start | bytes 393224 | tf_op jit(solution)/shard_map/ppermute | solution.py:182
  106.4 16.0 %collective-permute-start.18 = (bf16[32,2048]{1,0:T(8,128)(2,1)S(1)}, bf16[32,2048]{1,0:T(8,128)(2,1)S(1)}, u32[]{:S(2)}, u32[]{:S(2)}) collective-permute-start(bf16[32,2048]{1,0:T(8,128)(2,1)S(1)} %get-tuple-element.44), channel_id=1, source_target_pairs={{0,10},{2,12},{4,14},{6,16},{8,18},{10,20},{12,22},{14,24},{16,26}... | collective-permute-start | bytes 393224 | tf_op jit(solution)/shard_map/ppermute | solution.py:182

commit v3 on v2

--- a/solution.py
+++ b/solution.py
@@ -28,14 +28,25 @@
     )
 
 
-def prepare(cap, tok_ref, gain_ref, routes_ref, logits_ref, out_ref):
+def prepare(cap, tok_hbm, gain_hbm, routes_hbm, logits_hbm, out_ref, *scratch):
+    refs, sems = scratch[:4], scratch[4]
+    copies = [
+        pltpu.make_async_copy(source, ref, sems.at[i])
+        for i, (source, ref) in enumerate(zip((tok_hbm, gain_hbm, routes_hbm, logits_hbm), refs))
+    ]
+    for copy in copies:
+        copy.start()
+    for copy in copies:
+        copy.wait()
+    tok_ref, gain_ref, routes_ref, logits_ref = refs
     rows, width = tok_ref.shape
-    top = routes_ref.shape[1]
+    top = routes_ref.shape[0]
     x = tok_ref[...].astype(jnp.float32)
     scale = lax.rsqrt(jnp.mean(x * x, axis=-1, keepdims=True) + 1e-06)
     out_ref[:, :width] = (x * scale * gain_ref[...]).astype(jnp.bfloat16)
-    lane = lax.broadcasted_iota(jnp.int32, (rows, META), 1)
-    routes = routes_ref[...]
+    lane = lax.broadcasted_iota(jnp.int32, (rows, META), 1).astype(jnp.float32)
+    routes = jnp.transpose(routes_ref[...].astype(jnp.float32))
+    logits = jnp.transpose(logits_ref[...])
     named = jnp.zeros((rows, META), jnp.float32)
     for k in range(top):
         named += jnp.where(lane == routes[:, k : k + 1], 1.0, 0.0)
@@ -47,7 +58,6 @@
         named.astype(jnp.bfloat16),
         preferred_element_type=jnp.float32,
     )
-    logits = logits_ref[...]
     powers = jnp.exp(logits - jnp.max(logits, axis=-1, keepdims=True))
     weights = powers / jnp.sum(powers, axis=-1, keepdims=True)
     high = weights.astype(jnp.bfloat16).astype(jnp.float32)
@@ -56,7 +66,7 @@
     for k in range(top):
         hit = lane == routes[:, k : k + 1]
         rank = jnp.sum(jnp.where(hit, earlier, 0.0), axis=-1, keepdims=True)
-        key = routes[:, k : k + 1].astype(jnp.float32) * cap + rank
+        key = routes[:, k : k + 1] * cap + rank
         meta = jnp.where(lane == k, key, meta)
         meta = jnp.where(lane == top + k, high[:, k : k + 1], meta)
         meta = jnp.where(lane == 2 * top + k, low[:, k : k + 1], meta)
@@ -192,9 +202,21 @@
         return lax.ppermute(x, "c", [(0, 1), (1, 0)])
 
     place = jnp.stack([lax.axis_index("z"), lax.axis_index("c")]).astype(jnp.int32)
-    own = call(functools.partial(prepare, cap), bf16(rows, width + META), 4)(
-        tokens, norm_gain[None, :], routes, route_logits
-    )
+    own = pl.pallas_call(
+        functools.partial(prepare, cap),
+        out_shape=pltpu.VMEM((rows, width + META), jnp.bfloat16),
+        in_specs=[pl.BlockSpec(memory_space=pl.ANY)] * 4,
+        out_specs=VMEM,
+        scratch_shapes=[
+            pltpu.VMEM((rows, width), jnp.bfloat16),
+            pltpu.VMEM((1, width), jnp.float32),
+            pltpu.VMEM((top, rows), jnp.int32),
+            pltpu.VMEM((top, rows), jnp.float32),
+            pltpu.SemaphoreType.DMA((4,)),
+        ],
+        compiler_params=pltpu.CompilerParams(vmem_limit_bytes=60 << 20),
+        cost_estimate=pl.CostEstimate(flops=1 << 20, bytes_accessed=1 << 20, transcendentals=0),
+    )(tokens, norm_gain[None, :], routes.T, route_logits.T)
     low, high = shift(own, HOP), shift(own, -HOP)
     own2, low2, high2 = swap(own), swap(low), swap(high)
     near = 6 * cap
@@ -207,17 +229,20 @@
         7,
         smem=1,
         scratch=[pltpu.VMEM((6 * rows, width + META), jnp.bfloat16)],
+        flops=4 * 6 * slots * width * hidden,
     )(place, own, own2, low, low2, high, high2)
-    given = [shift(b, d) if d else b for b, d in zip(blocks, NEAR)] + [across(blocks[5], 1)]
+    last = across(blocks[5], 1)
+    given = [shift(b, d) if d else b for b, d in zip(blocks, NEAR)] + [last]
     results = call(
         functools.partial(experts, 256),
         shapes,
         9,
-        limit=56 << 20,
+        limit=LIMIT,
         scratch=[pltpu.VMEM((slots, width), jnp.bfloat16), pltpu.VMEM((slots, width), jnp.float32)],
         flops=6 * slots * width * hidden,
     )(*given, w_gate[0], w_up[0], w_down[0])
-    back = [shift(b, -d) if d else b for b, d in zip(results, NEAR)] + [across(results[5], -1)]
+    last = across(results[5], -1)
+    back = [shift(b, -d) if d else b for b, d in zip(results, NEAR)] + [last]
     far_mine, far_other, mine, other = call(
         weigh,
         [f32(2 * rows, width), bf16(2 * rows, width), f32(rows, width), bf16(rows, width)],

time: 125 us -> 114 us (0.912); the launches traced: 123 us -> 114 us
  Pallas kernels: 19.7 us -> 12.3 us
  local copies, waits for them, and re-layouts: 5.55 us -> 0.02 us
  waiting for transfers between devices: 59.7 us -> 63 us
    pallas_call x2, Pallas kernels: 17.1 us -> 9.68 us  [the longest x1 8.18 us: shards(): call(functools.partial(experts, 256), shapes, 9, limit=LIMIT, scratch=[pl...]
    unnamed x20 -> x12, local copies, waits for them, and re-layouts: 5.55 us -> 0.02 us
    ppermute x12, waiting for transfers between devices: 37.6 us -> 40.7 us  [shift(): return lax.ppermute(x, 'z', [(i, (i + by) % chips) for i in range(chips)])]
where the time goes in v3:
time: 114 us
  waiting for transfers between devices  63 us (55%)
  starting transfers between devices  38 us (33%)
  Pallas kernels  12.3 us (11%)
    ppermute x12, waiting for transfers between devices, shift(): return lax.ppermute(x, 'z', [(i, (i + by) % chips) for i in range(chips)])  40.7 us
    ppermute x12, starting transfers between devices, shift(): return lax.ppermute(x, 'z', [(i, (i + by) % chips) for i in range(chips)])  33.6 us
    ppermute x2, waiting for transfers between devices, across(): return lax.ppermute(x, ('z', 'c'), pairs)  20 us
    pallas_call x1, Pallas kernels, shards(): call(functools.partial(experts, 256), shapes, 9, limit=LIMIT, scratch=[pl...  8.18 us
    ppermute x2, starting transfers between devices, across(): return lax.ppermute(x, ('z', 'c'), pairs)  3.79 us
  transfers between devices with their start and end apart: 19, of which 9 were waited for; matrix products, arithmetic and copies ran while one was open for 0% of the time, Pallas kernels for 0%

profile of v3, /device:TPU:86, one launch (start us, length us, event | category | flops | bytes accessed | tf_op | source)
XLA Modules:
  0.0 113.6 jit_solution(8322958904975698916)
XLA Ops:
  0.0 1.5 %shard_map.73.refs_0_ = bf16[32,2176]{1,0:T(8,128)(2,1)S(1)} custom-call(bf16[32,2048]{1,0:T(8,128)(2,1)} %tok_hbm.1, f32[1,2048]{1,0:T(1,128)} %bitcast.17, s32[4,32]{1,0:T(4,128)} %bitcast.18, f32[4,32]{1,0:T(4,128)} %bitcast.19), custom_call_target="tpu_custom_call" | custom-call | flops 1048576 | bytes 1048576 | tf_op jit(solution)/shard_map/pallas_call | solution.py:205
  1.5 14.8 %collective-permute-start.3 = (bf16[32,2176]{1,0:T(8,128)(2,1)S(1)}, bf16[32,2176]{1,0:T(8,128)(2,1)S(1)}, u32[]{:S(2)}, u32[]{:S(2)}) collective-permute-start(bf16[32,2176]{1,0:T(8,128)(2,1)S(1)} %shard_map.73.refs_0_), channel_id=1, source_target_pairs={{0,22},{2,24},{4,26},{6,28},{8,30},{10,0},{12,2},{14,4},{16,6},{18... | collective-permute-start | bytes 417800 | tf_op jit(solution)/shard_map/ppermute | solution.py:192
  16.3 0.0 collective-permute-start.1
  16.3 0.0 collective-permute-start
  16.3 14.5 %collective-permute-done.3.refs_4_ = bf16[32,2176]{1,0:T(8,128)(2,1)S(1)} collective-permute-done((bf16[32,2176]{1,0:T(8,128)(2,1)S(1)}, bf16[32,2176]{1,0:T(8,128)(2,1)S(1)}, u32[]{:S(2)}, u32[]{:S(2)}) %collective-permute-start.3) | collective-permute-done | bytes 139296 | tf_op jit(solution)/shard_map/ppermute | solution.py:192
  30.9 0.0 collective-permute-start.4
  30.9 7.6 %collective-permute-done.1.refs_2_ = bf16[32,2176]{1,0:T(8,128)(2,1)S(1)} collective-permute-done((bf16[32,2176]{1,0:T(8,128)(2,1)S(1)}, bf16[32,2176]{1,0:T(8,128)(2,1)S(1)}, u32[]{:S(2)}, u32[]{:S(2)}) %collective-permute-start.1) | collective-permute-done | bytes 139296 | tf_op jit(solution)/shard_map/ppermute | solution.py:192
  38.5 0.0 collective-permute-start.2
  38.5 0.0 slice-start
  38.5 0.0 slice-start.2
  38.5 0.0 slice-start.4
  38.5 0.1 pad_add_fusion.place_ref
  38.6 0.0 slice-start.1
  38.6 0.0 slice-start.3
  38.6 0.0 slice-start.5
  38.6 0.0 collective-permute-done.refs_1_
  38.6 0.0 collective-permute-done.4.refs_5_
  38.6 1.2 %collective-permute-done.2.refs_3_ = bf16[32,2176]{1,0:T(8,128)(2,1)S(1)} collective-permute-done((bf16[32,2176]{1,0:T(8,128)(2,1)S(1)}, bf16[32,2176]{1,0:T(8,128)(2,1)S(1)}, u32[]{:S(2)}, u32[]{:S(2)}) %collective-permute-start.2) | collective-permute-done | bytes 139296 | tf_op jit(solution)/shard_map/ppermute | solution.py:202
  39.9 1.3 %shard_map.74 = (bf16[48,2048]{1,0:T(8,128)(2,1)S(1)}, bf16[48,2048]{1,0:T(8,128)(2,1)S(1)}, bf16[48,2048]{1,0:T(8,128)(2,1)S(1)}, bf16[48,2048]{1,0:T(8,128)(2,...) custom-call(s32[2]{0:T(128)S(1)} %pad_add_fusion.place_ref, ...), custom_call_target="tpu_custom_call" | custom-call | flops 22548578304 | bytes 1048576 | tf_op jit(solution)/shard_map/pallas_call | solution.py:226
  41.2 0.4 collective-permute-start.5
  41.6 0.0 collective-permute-start.6
  41.6 2.0 %collective-permute-start.7 = (bf16[48,2048]{1,0:T(8,128)(2,1)S(1)}, bf16[48,2048]{1,0:T(8,128)(2,1)S(1)}, u32[]{:S(2)}, u32[]{:S(2)}) collective-permute-start(bf16[48,2048]{1,0:T(8,128)(2,1)S(1)} %get-tuple-element.28), channel_id=1, source_target_pairs={{0,2},{2,4},{4,6},{6,8},{8,10},{10,12},{12,14},{14,16},{16,18},{18... | collective-permute-start | bytes 589832 | tf_op jit(solution)/shard_map/ppermute | solution.py:192
  43.6 2.6 %collective-permute-start.8 = (bf16[48,2048]{1,0:T(8,128)(2,1)S(1)}, bf16[48,2048]{1,0:T(8,128)(2,1)S(1)}, u32[]{:S(2)}, u32[]{:S(2)}) collective-permute-start(bf16[48,2048]{1,0:T(8,128)(2,1)S(1)} %get-tuple-element.29), channel_id=1, source_target_pairs={{0,4},{2,6},{4,8},{6,10},{8,12},{10,14},{12,16},{14,18},{16,20},{1... | collective-permute-start | bytes 589832 | tf_op jit(solution)/shard_map/ppermute | solution.py:192
  46.2 2.0 %collective-permute-start.9 = (bf16[16,2048]{1,0:T(8,128)(2,1)S(1)}, bf16[16,2048]{1,0:T(8,128)(2,1)S(1)}, u32[]{:S(2)}, u32[]{:S(2)}) collective-permute-start(bf16[16,2048]{1,0:T(8,128)(2,1)S(1)} %get-tuple-element.30), channel_id=1, source_target_pairs={{0,6},{1,27},{2,8},{3,29},{4,10},{5,31},{6,12},{7,1},{8,14},{9,3},... | collective-permute-start | bytes 196616 | tf_op jit(solution)/shard_map/ppermute | solution.py:199
  48.3 11.5 %collective-permute-done.9.refs_5_ = bf16[16,2048]{1,0:T(8,128)(2,1)S(1)} collective-permute-done((bf16[16,2048]{1,0:T(8,128)(2,1)S(1)}, bf16[16,2048]{1,0:T(8,128)(2,1)S(1)}, u32[]{:S(2)}, u32[]{:S(2)}) %collective-permute-start.9) | collective-permute-done | bytes 65568 | tf_op jit(solution)/shard_map/ppermute | solution.py:199
  59.8 0.0 collective-permute-done.5.refs_0_
  59.8 0.0 collective-permute-done.6.refs_1_
  59.8 0.0 collective-permute-done.7.refs_3_
  59.8 0.0 collective-permute-done.8.refs_4_
  59.8 0.0 slice-done
  59.9 0.0 slice-done.2
  59.9 0.0 slice-done.4
  59.9 0.0 slice-done.1
  59.9 0.0 slice-done.3
  59.9 0.0 slice-done.5
  59.9 8.2 %shard_map.75 = (bf16[48,2048]{1,0:T(8,128)(2,1)S(1)}, bf16[48,2048]{1,0:T(8,128)(2,1)S(1)}, bf16[48,2048]{1,0:T(8,128)(2,1)S(1)}, bf16[48,2048]{1,0:T(8,128)(2,...) custom-call(bf16[48,2048]{1,0:T(8,128)(2,1)S(1)} %collective-permute-done.5.refs_0_, ...), custom_call_target="tpu_custom_call" | custom-call | flops 5637144576 | bytes 1048576 | tf_op jit(solution)/shard_map/pallas_call | solution.py:236
  68.1 2.9 %collective-permute-start.10 = (bf16[48,2048]{1,0:T(8,128)(2,1)S(1)}, bf16[48,2048]{1,0:T(8,128)(2,1)S(1)}, u32[]{:S(2)}, u32[]{:S(2)}) collective-permute-start(bf16[48,2048]{1,0:T(8,128)(2,1)S(1)} %get-tuple-element.31), channel_id=1, source_target_pairs={{0,4},{2,6},{4,8},{6,10},{8,12},{10,14},{12,16},{14,18},{16,20},{1... | collective-permute-start | bytes 589832 | tf_op jit(solution)/shard_map/ppermute | solution.py:192
  71.0 0.0 collective-permute-start.11
  71.0 3.2 %collective-permute-start.12 = (bf16[48,2048]{1,0:T(8,128)(2,1)S(1)}, bf16[48,2048]{1,0:T(8,128)(2,1)S(1)}, u32[]{:S(2)}, u32[]{:S(2)}) collective-permute-start(bf16[48,2048]{1,0:T(8,128)(2,1)S(1)} %get-tuple-element.34), channel_id=1, source_target_pairs={{0,30},{2,0},{4,2},{6,4},{8,6},{10,8},{12,10},{14,12},{16,14},{18,... | collective-permute-start | bytes 589832 | tf_op jit(solution)/shard_map/ppermute | solution.py:192
  74.2 0.2 collective-permute-start.13
  74.4 1.7 %collective-permute-start.14 = (bf16[16,2048]{1,0:T(8,128)(2,1)S(1)}, bf16[16,2048]{1,0:T(8,128)(2,1)S(1)}, u32[]{:S(2)}, u32[]{:S(2)}) collective-permute-start(bf16[16,2048]{1,0:T(8,128)(2,1)S(1)} %get-tuple-element.36), channel_id=1, source_target_pairs={{0,26},{1,7},{2,28},{3,9},{4,30},{5,11},{6,0},{7,13},{8,2},{9,15},... | collective-permute-start | bytes 196616 | tf_op jit(solution)/shard_map/ppermute | solution.py:199
  76.1 8.4 %collective-permute-done.14.refs_5_ = bf16[16,2048]{1,0:T(8,128)(2,1)S(1)} collective-permute-done((bf16[16,2048]{1,0:T(8,128)(2,1)S(1)}, bf16[16,2048]{1,0:T(8,128)(2,1)S(1)}, u32[]{:S(2)}, u32[]{:S(2)}) %collective-permute-start.14) | collective-permute-done | bytes 65568 | tf_op jit(solution)/shard_map/ppermute | solution.py:199
  84.6 0.0 collective-permute-done.10.refs_0_
  84.6 0.0 collective-permute-done.11.refs_1_
  84.6 0.0 collective-permute-done.12.refs_3_
  84.6 0.3 collective-permute-done.13.refs_4_
  84.9 0.6 shard_map.76
  85.5 0.1 collective-permute-start.16
  85.6 0.5 collective-permute-start.15
  86.1 1.0 collective-permute-done.16.other
  87.2 6.2 %collective-permute-start.17 = (bf16[32,2048]{1,0:T(8,128)(2,1)S(1)}, bf16[32,2048]{1,0:T(8,128)(2,1)S(1)}, u32[]{:S(2)}, u32[]{:S(2)}) collective-permute-start(bf16[32,2048]{1,0:T(8,128)(2,1)S(1)} %get-tuple-element.43), channel_id=1, source_target_pairs={{0,22},{2,24},{4,26},{6,28},{8,30},{10,0},{12,2},{14,4},{16,6},{18... | collective-permute-start | bytes 393224 | tf_op jit(solution)/shard_map/ppermute | solution.py:192
  93.4 1.2 %collective-permute-start.18 = (bf16[32,2048]{1,0:T(8,128)(2,1)S(1)}, bf16[32,2048]{1,0:T(8,128)(2,1)S(1)}, u32[]{:S(2)}, u32[]{:S(2)}) collective-permute-start(bf16[32,2048]{1,0:T(8,128)(2,1)S(1)} %get-tuple-element.44), channel_id=1, source_target_pairs={{0,10},{2,12},{4,14},{6,16},{8,18},{10,20},{12,22},{14,24},{16,26}... | collective-permute-start | bytes 393224 | tf_op jit(solution)/shard_map/ppermute | solution.py:192
  94.6 0.0 collective-permute-done.15.other
  94.6 13.4 %collective-permute-done.17.one = bf16[32,2048]{1,0:T(8,128)(2,1)S(1)} collective-permute-done((bf16[32,2048]{1,0:T(8,128)(2,1)S(1)}, bf16[32,2048]{1,0:T(8,128)(2,1)S(1)}, u32[]{:S(2)}, u32[]{:S(2)}) %collective-permute-start.17) | collective-permute-done | bytes 131104 | tf_op jit(solution)/shard_map/ppermute | solution.py:192
  108.0 4.8 %collective-permute-done.18.two = bf16[32,2048]{1,0:T(8,128)(2,1)S(1)} collective-permute-done((bf16[32,2048]{1,0:T(8,128)(2,1)S(1)}, bf16[32,2048]{1,0:T(8,128)(2,1)S(1)}, u32[]{:S(2)}, u32[]{:S(2)}) %collective-permute-start.18) | collective-permute-done | bytes 131104 | tf_op jit(solution)/shard_map/ppermute | solution.py:192
  112.8 0.7 shard_map.78
  (4 shorter events, 0.0 us)
Async XLA Ops:
  1.5 29.3 %collective-permute-start.3 = (bf16[32,2176]{1,0:T(8,128)(2,1)S(1)}, bf16[32,2176]{1,0:T(8,128)(2,1)S(1)}, u32[]{:S(2)}, u32[]{:S(2)}) collective-permute-start(bf16[32,2176]{1,0:T(8,128)(2,1)S(1)} %shard_map.73.refs_0_), channel_id=1, source_target_pairs={{0,22},{2,24},{4,26},{6,28},{8,30},{10,0},{12,2},{14,4},{16,6},{18... | collective-permute-start | bytes 417800 | tf_op jit(solution)/shard_map/ppermute | solution.py:192
  16.3 22.2 %collective-permute-start.1 = (bf16[32,2176]{1,0:T(8,128)(2,1)S(1)}, bf16[32,2176]{1,0:T(8,128)(2,1)S(1)}, u32[]{:S(2)}, u32[]{:S(2)}) collective-permute-start(bf16[32,2176]{1,0:T(8,128)(2,1)S(1)} %shard_map.73.refs_0_), channel_id=1, source_target_pairs={{0,10},{2,12},{4,14},{6,16},{8,18},{10,20},{12,22},{14,24},{16,26}... | collective-permute-start | bytes 417800 | tf_op jit(solution)/shard_map/ppermute | solution.py:192
  16.3 22.3 %collective-permute-start = (bf16[32,2176]{1,0:T(8,128)(2,1)S(1)}, bf16[32,2176]{1,0:T(8,128)(2,1)S(1)}, u32[]{:S(2)}, u32[]{:S(2)}) collective-permute-start(bf16[32,2176]{1,0:T(8,128)(2,1)S(1)} %shard_map.73.refs_0_), channel_id=1, source_target_pairs={{0,1},{1,0},{2,3},{3,2},{4,5},{5,4},{6,7},{7,6},{8,9},{9,8},{10,11... | collective-permute-start | bytes 417800 | tf_op jit(solution)/shard_map/ppermute | solution.py:202
  30.9 7.8 %collective-permute-start.4 = (bf16[32,2176]{1,0:T(8,128)(2,1)S(1)}, bf16[32,2176]{1,0:T(8,128)(2,1)S(1)}, u32[]{:S(2)}, u32[]{:S(2)}) collective-permute-start(bf16[32,2176]{1,0:T(8,128)(2,1)S(1)} %collective-permute-done.3.refs_4_), channel_id=1, source_target_pairs={{0,1},{1,0},{2,3},{3,2},{4,5},{5,4},{6,7},{7,6},{8,9},{9,8},{10,11... | collective-permute-start | bytes 417800 | tf_op jit(solution)/shard_map/ppermute | solution.py:202
  38.5 1.4 %collective-permute-start.2 = (bf16[32,2176]{1,0:T(8,128)(2,1)S(1)}, bf16[32,2176]{1,0:T(8,128)(2,1)S(1)}, u32[]{:S(2)}, u32[]{:S(2)}) collective-permute-start(bf16[32,2176]{1,0:T(8,128)(2,1)S(1)} %collective-permute-done.1.refs_2_), channel_id=1, source_target_pairs={{0,1},{1,0},{2,3},{3,2},{4,5},{5,4},{6,7},{7,6},{8,9},{9,8},{10,11... | collective-permute-start | bytes 417800 | tf_op jit(solution)/shard_map/ppermute | solution.py:202
  38.5 21.3 %slice-start = ((s8[7340032]{0:T(1024)(128)(4,1)}), s8[4194304]{0:T(1024)(128)(4,1)S(1)}, s32[]{:S(2)}) async-start(s8[7340032]{0:T(1024)(128)(4,1)} %bitcast.8), calls=%async_computation | async-start | bytes 8388608
  38.5 21.3 %slice-start.2 = ((s8[7340032]{0:T(1024)(128)(4,1)}), s8[4194304]{0:T(1024)(128)(4,1)S(1)}, s32[]{:S(2)}) async-start(s8[7340032]{0:T(1024)(128)(4,1)} %bitcast.11), calls=%async_computation.2 | async-start | bytes 8388608
  38.5 21.3 %slice-start.4 = ((s8[7340032]{0:T(1024)(128)(4,1)}), s8[4194304]{0:T(1024)(128)(4,1)S(1)}, s32[]{:S(2)}) async-start(s8[7340032]{0:T(1024)(128)(4,1)} %bitcast.14), calls=%async_computation.4 | async-start | bytes 8388608
  38.6 21.3 %slice-start.1 = ((s8[7340032]{0:T(1024)(128)(4,1)}), s8[3145728]{0:T(1024)(128)(4,1)S(1)}, s32[]{:S(2)}) async-start(s8[7340032]{0:T(1024)(128)(4,1)} %bitcast.8), calls=%async_computation.1 | async-start | bytes 6291456
  38.6 21.3 %slice-start.3 = ((s8[7340032]{0:T(1024)(128)(4,1)}), s8[3145728]{0:T(1024)(128)(4,1)S(1)}, s32[]{:S(2)}) async-start(s8[7340032]{0:T(1024)(128)(4,1)} %bitcast.11), calls=%async_computation.3 | async-start | bytes 6291456
  38.6 21.3 %slice-start.5 = ((s8[7340032]{0:T(1024)(128)(4,1)}), s8[3145728]{0:T(1024)(128)(4,1)S(1)}, s32[]{:S(2)}) async-start(s8[7340032]{0:T(1024)(128)(4,1)} %bitcast.14), calls=%async_computation.5 | async-start | bytes 6291456
  41.2 18.6 %collective-permute-start.5 = (bf16[48,2048]{1,0:T(8,128)(2,1)S(1)}, bf16[48,2048]{1,0:T(8,128)(2,1)S(1)}, u32[]{:S(2)}, u32[]{:S(2)}) collective-permute-start(bf16[48,2048]{1,0:T(8,128)(2,1)S(1)} %get-tuple-element.25), channel_id=1, source_target_pairs={{0,28},{2,30},{4,0},{6,2},{8,4},{10,6},{12,8},{14,10},{16,12},{18,... | collective-permute-start | bytes 589832 | tf_op jit(solution)/shard_map/ppermute | solution.py:192
  41.6 18.2 %collective-permute-start.6 = (bf16[48,2048]{1,0:T(8,128)(2,1)S(1)}, bf16[48,2048]{1,0:T(8,128)(2,1)S(1)}, u32[]{:S(2)}, u32[]{:S(2)}) collective-permute-start(bf16[48,2048]{1,0:T(8,128)(2,1)S(1)} %get-tuple-element.26), channel_id=1, source_target_pairs={{0,30},{2,0},{4,2},{6,4},{8,6},{10,8},{12,10},{14,12},{16,14},{18,... | collective-permute-start | bytes 589832 | tf_op jit(solution)/shard_map/ppermute | solution.py:192
  41.6 18.2 %collective-permute-start.7 = (bf16[48,2048]{1,0:T(8,128)(2,1)S(1)}, bf16[48,2048]{1,0:T(8,128)(2,1)S(1)}, u32[]{:S(2)}, u32[]{:S(2)}) collective-permute-start(bf16[48,2048]{1,0:T(8,128)(2,1)S(1)} %get-tuple-element.28), channel_id=1, source_target_pairs={{0,2},{2,4},{4,6},{6,8},{8,10},{10,12},{12,14},{14,16},{16,18},{18... | collective-permute-start | bytes 589832 | tf_op jit(solution)/shard_map/ppermute | solution.py:192
  43.6 16.2 %collective-permute-start.8 = (bf16[48,2048]{1,0:T(8,128)(2,1)S(1)}, bf16[48,2048]{1,0:T(8,128)(2,1)S(1)}, u32[]{:S(2)}, u32[]{:S(2)}) collective-permute-start(bf16[48,2048]{1,0:T(8,128)(2,1)S(1)} %get-tuple-element.29), channel_id=1, source_target_pairs={{0,4},{2,6},{4,8},{6,10},{8,12},{10,14},{12,16},{14,18},{16,20},{1... | collective-permute-start | bytes 589832 | tf_op jit(solution)/shard_map/ppermute | solution.py:192
  46.2 13.6 %collective-permute-start.9 = (bf16[16,2048]{1,0:T(8,128)(2,1)S(1)}, bf16[16,2048]{1,0:T(8,128)(2,1)S(1)}, u32[]{:S(2)}, u32[]{:S(2)}) collective-permute-start(bf16[16,2048]{1,0:T(8,128)(2,1)S(1)} %get-tuple-element.30), channel_id=1, source_target_pairs={{0,6},{1,27},{2,8},{3,29},{4,10},{5,31},{6,12},{7,1},{8,14},{9,3},... | collective-permute-start | bytes 196616 | tf_op jit(solution)/shard_map/ppermute | solution.py:199
  68.1 16.4 %collective-permute-start.10 = (bf16[48,2048]{1,0:T(8,128)(2,1)S(1)}, bf16[48,2048]{1,0:T(8,128)(2,1)S(1)}, u32[]{:S(2)}, u32[]{:S(2)}) collective-permute-start(bf16[48,2048]{1,0:T(8,128)(2,1)S(1)} %get-tuple-element.31), channel_id=1, source_target_pairs={{0,4},{2,6},{4,8},{6,10},{8,12},{10,14},{12,16},{14,18},{16,20},{1... | collective-permute-start | bytes 589832 | tf_op jit(solution)/shard_map/ppermute | solution.py:192
  71.0 13.6 %collective-permute-start.11 = (bf16[48,2048]{1,0:T(8,128)(2,1)S(1)}, bf16[48,2048]{1,0:T(8,128)(2,1)S(1)}, u32[]{:S(2)}, u32[]{:S(2)}) collective-permute-start(bf16[48,2048]{1,0:T(8,128)(2,1)S(1)} %get-tuple-element.32), channel_id=1, source_target_pairs={{0,2},{2,4},{4,6},{6,8},{8,10},{10,12},{12,14},{14,16},{16,18},{18... | collective-permute-start | bytes 589832 | tf_op jit(solution)/shard_map/ppermute | solution.py:192
  71.0 13.6 %collective-permute-start.12 = (bf16[48,2048]{1,0:T(8,128)(2,1)S(1)}, bf16[48,2048]{1,0:T(8,128)(2,1)S(1)}, u32[]{:S(2)}, u32[]{:S(2)}) collective-permute-start(bf16[48,2048]{1,0:T(8,128)(2,1)S(1)} %get-tuple-element.34), channel_id=1, source_target_pairs={{0,30},{2,0},{4,2},{6,4},{8,6},{10,8},{12,10},{14,12},{16,14},{18,... | collective-permute-start | bytes 589832 | tf_op jit(solution)/shard_map/ppermute | solution.py:192
  74.2 10.7 %collective-permute-start.13 = (bf16[48,2048]{1,0:T(8,128)(2,1)S(1)}, bf16[48,2048]{1,0:T(8,128)(2,1)S(1)}, u32[]{:S(2)}, u32[]{:S(2)}) collective-permute-start(bf16[48,2048]{1,0:T(8,128)(2,1)S(1)} %get-tuple-element.35), channel_id=1, source_target_pairs={{0,28},{2,30},{4,0},{6,2},{8,4},{10,6},{12,8},{14,10},{16,12},{18,... | collective-permute-start | bytes 589832 | tf_op jit(solution)/shard_map/ppermute | solution.py:192
  74.4 10.2 %collective-permute-start.14 = (bf16[16,2048]{1,0:T(8,128)(2,1)S(1)}, bf16[16,2048]{1,0:T(8,128)(2,1)S(1)}, u32[]{:S(2)}, u32[]{:S(2)}) collective-permute-start(bf16[16,2048]{1,0:T(8,128)(2,1)S(1)} %get-tuple-element.36), channel_id=1, source_target_pairs={{0,26},{1,7},{2,28},{3,9},{4,30},{5,11},{6,0},{7,13},{8,2},{9,15},... | collective-permute-start | bytes 196616 | tf_op jit(solution)/shard_map/ppermute | solution.py:199
  85.5 1.7 %collective-permute-start.16 = (bf16[64,2048]{1,0:T(8,128)(2,1)S(1)}, bf16[64,2048]{1,0:T(8,128)(2,1)S(1)}, u32[]{:S(2)}, u32[]{:S(2)}) collective-permute-start(bf16[64,2048]{1,0:T(8,128)(2,1)S(1)} %get-tuple-element.42), channel_id=1, source_target_pairs={{0,1},{1,0},{2,3},{3,2},{4,5},{5,4},{6,7},{7,6},{8,9},{9,8},{10,11... | collective-permute-start | bytes 786440 | tf_op jit(solution)/shard_map/ppermute | solution.py:202
  85.6 9.0 %collective-permute-start.15 = (bf16[32,2048]{1,0:T(8,128)(2,1)S(1)}, bf16[32,2048]{1,0:T(8,128)(2,1)S(1)}, u32[]{:S(2)}, u32[]{:S(2)}) collective-permute-start(bf16[32,2048]{1,0:T(8,128)(2,1)S(1)} %get-tuple-element.40), channel_id=1, source_target_pairs={{0,1},{1,0},{2,3},{3,2},{4,5},{5,4},{6,7},{7,6},{8,9},{9,8},{10,11... | collective-permute-start | bytes 393224 | tf_op jit(solution)/shard_map/ppermute | solution.py:202
  87.2 20.8 %collective-permute-start.17 = (bf16[32,2048]{1,0:T(8,128)(2,1)S(1)}, bf16[32,2048]{1,0:T(8,128)(2,1)S(1)}, u32[]{:S(2)}, u32[]{:S(2)}) collective-permute-start(bf16[32,2048]{1,0:T(8,128)(2,1)S(1)} %get-tuple-element.43), channel_id=1, source_target_pairs={{0,22},{2,24},{4,26},{6,28},{8,30},{10,0},{12,2},{14,4},{16,6},{18... | collective-permute-start | bytes 393224 | tf_op jit(solution)/shard_map/ppermute | solution.py:192
  93.4 19.4 %collective-permute-start.18 = (bf16[32,2048]{1,0:T(8,128)(2,1)S(1)}, bf16[32,2048]{1,0:T(8,128)(2,1)S(1)}, u32[]{:S(2)}, u32[]{:S(2)}) collective-permute-start(bf16[32,2048]{1,0:T(8,128)(2,1)S(1)} %get-tuple-element.44), channel_id=1, source_target_pairs={{0,10},{2,12},{4,14},{6,16},{8,18},{10,20},{12,22},{14,24},{16,26}... | collective-permute-start | bytes 393224 | tf_op jit(solution)/shard_map/ppermute | solution.py:192

commit v4 on v3

--- a/solution.py
+++ b/solution.py
@@ -9,7 +9,7 @@
 from jax.sharding import PartitionSpec as P
 
 HOP = 5
-NEAR = (-2, -1, 0, 1, 2)
+NEAR = (2, -2, 1, -1, 0)
 GRP_EP = ("grp", "z", "c")
 META = 128
 LIMIT = 16 << 20
@@ -87,9 +87,9 @@
     source = sum((inside >= cap * i).astype(jnp.int32) for i in range(1, 6))
     slot = inside - source * cap
     across = block == len(NEAR)
-    source = jnp.where(across, source + jnp.where(c == 0, 2, 4), source)
-    step = jnp.where(across, jnp.where(c == 0, 3, -3), block + NEAR[0])
-    chip = z + step
+    source = jnp.where(across, source + 2, source)
+    step = sum(jnp.where(block == i, d, 0) for i, d in enumerate((*NEAR, 3)))
+    chip = z + jnp.where(c == 0, step, -step)
     chip = jnp.where(chip < 0, chip + chips, chip)
     chip = jnp.where(chip >= chips, chip - chips, chip)
     target = ((2 * chip + c) * cap + slot + source * 2 * chips * cap).astype(jnp.float32)
@@ -162,7 +162,7 @@
     for i in range(2):
         far_mine[i * rows : (i + 1) * rows, :] = total[(2 + 2 * i) * rows : (3 + 2 * i) * rows]
         far_other[i * rows : (i + 1) * rows, :] = total[
-            (3 + 2 * i) * rows : (4 + 2 * i) * rows
+            (5 - 2 * i) * rows : (6 - 2 * i) * rows
         ].astype(jnp.bfloat16)
 
 
@@ -189,13 +189,10 @@
     f32 = lambda *shape: jax.ShapeDtypeStruct(shape, jnp.float32)
 
     def shift(x, by):
-        return lax.ppermute(x, "z", [(i, (i + by) % chips) for i in range(chips)])
-
-    def across(x, sign):
         pairs = []
         for i in range(chips):
-            pairs.append((2 * i, (i + 3 * sign) % chips * 2))
-            pairs.append((2 * i + 1, (i - 3 * sign) % chips * 2 + 1))
+            pairs.append((2 * i, (i + by) % chips * 2))
+            pairs.append((2 * i + 1, (i - by) % chips * 2 + 1))
         return lax.ppermute(x, ("z", "c"), pairs)
 
     def swap(x):
@@ -218,7 +215,7 @@
         cost_estimate=pl.CostEstimate(flops=1 << 20, bytes_accessed=1 << 20, transcendentals=0),
     )(tokens, norm_gain[None, :], routes.T, route_logits.T)
     low, high = shift(own, HOP), shift(own, -HOP)
-    own2, low2, high2 = swap(own), swap(low), swap(high)
+    own2, high2, low2 = swap(own), swap(low), swap(high)
     near = 6 * cap
     slots = len(NEAR) * near + 2 * cap
     shapes = [bf16(near, width)] * len(NEAR) + [bf16(2 * cap, width)]
@@ -231,7 +228,7 @@
         scratch=[pltpu.VMEM((6 * rows, width + META), jnp.bfloat16)],
         flops=4 * 6 * slots * width * hidden,
     )(place, own, own2, low, low2, high, high2)
-    last = across(blocks[5], 1)
+    last = shift(blocks[5], 3)
     given = [shift(b, d) if d else b for b, d in zip(blocks, NEAR)] + [last]
     results = call(
         functools.partial(experts, 256),
@@ -241,7 +238,7 @@
         scratch=[pltpu.VMEM((slots, width), jnp.bfloat16), pltpu.VMEM((slots, width), jnp.float32)],
         flops=6 * slots * width * hidden,
     )(*given, w_gate[0], w_up[0], w_down[0])
-    last = across(results[5], -1)
+    last = shift(results[5], -3)
     back = [shift(b, -d) if d else b for b, d in zip(results, NEAR)] + [last]
     far_mine, far_other, mine, other = call(
         weigh,

time: 114 us -> 108 us (0.947)
  waiting for transfers between devices: 63 us -> 53.4 us
  starting transfers between devices: 38 us -> 40.5 us
    ppermute x14, waiting for transfers between devices: 60.7 us -> 51.4 us  [shift(): return lax.ppermute(x, ('z', 'c'), pairs)]
    ppermute x14, starting transfers between devices: 37.3 us -> 39.4 us  [shift(): return lax.ppermute(x, ('z', 'c'), pairs)]
  transfers between devices with their start and end apart: 19 -> 19, of which waited for: 9 -> 10; matrix products, arithmetic and copies ran while one was open for 0% -> 0% of each run, Pallas kernels for 0% -> 0%
where the time goes in v4:
time: 108 us; the launch traced here: 106 us
  waiting for transfers between devices  53.4 us (49%)
  starting transfers between devices  40.5 us (38%)
  Pallas kernels  12.3 us (11%)
    ppermute x14, waiting for transfers between devices, shift(): return lax.ppermute(x, ('z', 'c'), pairs)  51.4 us
    ppermute x14, starting transfers between devices, shift(): return lax.ppermute(x, ('z', 'c'), pairs)  39.4 us
    pallas_call x1, Pallas kernels, shards(): call(functools.partial(experts, 256), shapes, 9, limit=LIMIT, scratch=[pl...  8.17 us
  transfers between devices with their start and end apart: 19, of which 10 were waited for; matrix products, arithmetic and copies ran while one was open for 0% of the time, Pallas kernels for 0%

profile of v4, /device:TPU:86, one launch (start us, length us, event | category | flops | bytes accessed | tf_op | source)
XLA Modules:
  0.0 106.5 jit_solution(4467947421779183761)
XLA Ops:
  0.0 1.5 %shard_map.73.refs_0_ = bf16[32,2176]{1,0:T(8,128)(2,1)S(1)} custom-call(bf16[32,2048]{1,0:T(8,128)(2,1)} %tok_hbm.1, f32[1,2048]{1,0:T(1,128)} %bitcast.17, s32[4,32]{1,0:T(4,128)} %bitcast.18, f32[4,32]{1,0:T(4,128)} %bitcast.19), custom_call_target="tpu_custom_call" | custom-call | flops 1048576 | bytes 1048576 | tf_op jit(solution)/shard_map/pallas_call | solution.py:202
  1.5 14.8 %collective-permute-start.2 = (bf16[32,2176]{1,0:T(8,128)(2,1)S(1)}, bf16[32,2176]{1,0:T(8,128)(2,1)S(1)}, u32[]{:S(2)}, u32[]{:S(2)}) collective-permute-start(bf16[32,2176]{1,0:T(8,128)(2,1)S(1)} %shard_map.73.refs_0_), channel_id=1, source_target_pairs={{0,22},{1,11},{2,24},{3,13},{4,26},{5,15},{6,28},{7,17},{8,30},{9,... | collective-permute-start | bytes 417800 | tf_op jit(solution)/shard_map/ppermute | solution.py:196
  16.3 0.0 collective-permute-start.1
  16.3 0.0 collective-permute-start
  16.3 14.6 %collective-permute-done.2.refs_4_ = bf16[32,2176]{1,0:T(8,128)(2,1)S(1)} collective-permute-done((bf16[32,2176]{1,0:T(8,128)(2,1)S(1)}, bf16[32,2176]{1,0:T(8,128)(2,1)S(1)}, u32[]{:S(2)}, u32[]{:S(2)}) %collective-permute-start.2) | collective-permute-done | bytes 139296 | tf_op jit(solution)/shard_map/ppermute | solution.py:196
  31.0 0.0 collective-permute-start.3
  31.0 0.0 collective-permute-done.1.refs_2_
  31.0 0.5 collective-permute-start.4
  31.5 0.0 slice-start
  31.5 0.0 slice-start.2
  31.5 0.0 slice-start.4
  31.5 0.1 pad_add_fusion.place_ref
  31.6 0.0 slice-start.1
  31.6 0.0 slice-start.3
  31.6 0.0 slice-start.5
  31.6 0.0 collective-permute-done.refs_1_
  31.6 0.8 collective-permute-done.3.refs_3_
  32.3 0.2 collective-permute-done.4.refs_5_
  32.5 1.3 %shard_map.74 = (bf16[48,2048]{1,0:T(8,128)(2,1)S(1)}, bf16[48,2048]{1,0:T(8,128)(2,1)S(1)}, bf16[48,2048]{1,0:T(8,128)(2,1)S(1)}, bf16[48,2048]{1,0:T(8,128)(2,...) custom-call(s32[2]{0:T(128)S(1)} %pad_add_fusion.place_ref, ...), custom_call_target="tpu_custom_call" | custom-call | flops 22548578304 | bytes 1048576 | tf_op jit(solution)/shard_map/pallas_call | solution.py:223
  33.8 0.1 collective-permute-start.5
  34.0 4.1 %collective-permute-start.6 = (bf16[48,2048]{1,0:T(8,128)(2,1)S(1)}, bf16[48,2048]{1,0:T(8,128)(2,1)S(1)}, u32[]{:S(2)}, u32[]{:S(2)}) collective-permute-start(bf16[48,2048]{1,0:T(8,128)(2,1)S(1)} %get-tuple-element.26), channel_id=1, source_target_pairs={{0,28},{1,5},{2,30},{3,7},{4,0},{5,9},{6,2},{7,11},{8,4},{9,13},{1... | collective-permute-start | bytes 589832 | tf_op jit(solution)/shard_map/ppermute | solution.py:196
  38.1 2.8 %collective-permute-start.7 = (bf16[48,2048]{1,0:T(8,128)(2,1)S(1)}, bf16[48,2048]{1,0:T(8,128)(2,1)S(1)}, u32[]{:S(2)}, u32[]{:S(2)}) collective-permute-start(bf16[48,2048]{1,0:T(8,128)(2,1)S(1)} %get-tuple-element.27), channel_id=1, source_target_pairs={{0,2},{1,31},{2,4},{3,1},{4,6},{5,3},{6,8},{7,5},{8,10},{9,7},{10,... | collective-permute-start | bytes 589832 | tf_op jit(solution)/shard_map/ppermute | solution.py:196
  40.8 1.3 %collective-permute-start.8 = (bf16[48,2048]{1,0:T(8,128)(2,1)S(1)}, bf16[48,2048]{1,0:T(8,128)(2,1)S(1)}, u32[]{:S(2)}, u32[]{:S(2)}) collective-permute-start(bf16[48,2048]{1,0:T(8,128)(2,1)S(1)} %get-tuple-element.28), channel_id=1, source_target_pairs={{0,30},{1,3},{2,0},{3,5},{4,2},{5,7},{6,4},{7,9},{8,6},{9,11},{10,... | collective-permute-start | bytes 589832 | tf_op jit(solution)/shard_map/ppermute | solution.py:196
  42.2 0.9 collective-permute-start.9
  43.1 12.5 %collective-permute-done.9.refs_5_ = bf16[16,2048]{1,0:T(8,128)(2,1)S(1)} collective-permute-done((bf16[16,2048]{1,0:T(8,128)(2,1)S(1)}, bf16[16,2048]{1,0:T(8,128)(2,1)S(1)}, u32[]{:S(2)}, u32[]{:S(2)}) %collective-permute-start.9) | collective-permute-done | bytes 65568 | tf_op jit(solution)/shard_map/ppermute | solution.py:196
  55.5 0.0 collective-permute-done.5.refs_0_
  55.5 0.0 collective-permute-done.6.refs_1_
  55.5 0.0 collective-permute-done.7.refs_2_
  55.5 0.0 collective-permute-done.8.refs_3_
  55.5 0.0 slice-done
  55.6 0.0 slice-done.2
  55.6 0.0 slice-done.4
  55.6 0.0 slice-done.1
  55.6 0.0 slice-done.3
  55.6 0.0 slice-done.5
  55.6 8.2 %shard_map.75 = (bf16[48,2048]{1,0:T(8,128)(2,1)S(1)}, bf16[48,2048]{1,0:T(8,128)(2,1)S(1)}, bf16[48,2048]{1,0:T(8,128)(2,1)S(1)}, bf16[48,2048]{1,0:T(8,128)(2,...) custom-call(bf16[48,2048]{1,0:T(8,128)(2,1)S(1)} %collective-permute-done.5.refs_0_, ...), custom_call_target="tpu_custom_call" | custom-call | flops 5637144576 | bytes 1048576 | tf_op jit(solution)/shard_map/pallas_call | solution.py:233
  63.8 2.6 %collective-permute-start.10 = (bf16[48,2048]{1,0:T(8,128)(2,1)S(1)}, bf16[48,2048]{1,0:T(8,128)(2,1)S(1)}, u32[]{:S(2)}, u32[]{:S(2)}) collective-permute-start(bf16[48,2048]{1,0:T(8,128)(2,1)S(1)} %get-tuple-element.31), channel_id=1, source_target_pairs={{0,28},{1,5},{2,30},{3,7},{4,0},{5,9},{6,2},{7,11},{8,4},{9,13},{1... | collective-permute-start | bytes 589832 | tf_op jit(solution)/shard_map/ppermute | solution.py:196
  66.4 0.4 collective-permute-start.11
  66.8 1.4 %collective-permute-start.12 = (bf16[48,2048]{1,0:T(8,128)(2,1)S(1)}, bf16[48,2048]{1,0:T(8,128)(2,1)S(1)}, u32[]{:S(2)}, u32[]{:S(2)}) collective-permute-start(bf16[48,2048]{1,0:T(8,128)(2,1)S(1)} %get-tuple-element.33), channel_id=1, source_target_pairs={{0,30},{1,3},{2,0},{3,5},{4,2},{5,7},{6,4},{7,9},{8,6},{9,11},{10,... | collective-permute-start | bytes 589832 | tf_op jit(solution)/shard_map/ppermute | solution.py:196
  68.3 0.6 collective-permute-start.13
  68.9 3.4 %collective-permute-start.14 = (bf16[16,2048]{1,0:T(8,128)(2,1)S(1)}, bf16[16,2048]{1,0:T(8,128)(2,1)S(1)}, u32[]{:S(2)}, u32[]{:S(2)}) collective-permute-start(bf16[16,2048]{1,0:T(8,128)(2,1)S(1)} %get-tuple-element.36), channel_id=1, source_target_pairs={{0,26},{1,7},{2,28},{3,9},{4,30},{5,11},{6,0},{7,13},{8,2},{9,15},... | collective-permute-start | bytes 196616 | tf_op jit(solution)/shard_map/ppermute | solution.py:196
  72.2 7.9 %collective-permute-done.14.refs_5_ = bf16[16,2048]{1,0:T(8,128)(2,1)S(1)} collective-permute-done((bf16[16,2048]{1,0:T(8,128)(2,1)S(1)}, bf16[16,2048]{1,0:T(8,128)(2,1)S(1)}, u32[]{:S(2)}, u32[]{:S(2)}) %collective-permute-start.14) | collective-permute-done | bytes 65568 | tf_op jit(solution)/shard_map/ppermute | solution.py:196
  80.1 0.0 collective-permute-done.10.refs_0_
  80.1 0.0 collective-permute-done.11.refs_1_
  80.1 0.9 collective-permute-done.12.refs_2_
  81.0 0.2 collective-permute-done.13.refs_3_
  81.2 0.6 shard_map.76
  81.8 0.1 collective-permute-start.16
  81.9 0.5 collective-permute-start.15
  82.4 1.0 collective-permute-done.16.other
  83.5 5.3 %collective-permute-start.17 = (bf16[32,2048]{1,0:T(8,128)(2,1)S(1)}, bf16[32,2048]{1,0:T(8,128)(2,1)S(1)}, u32[]{:S(2)}, u32[]{:S(2)}) collective-permute-start(bf16[32,2048]{1,0:T(8,128)(2,1)S(1)} %get-tuple-element.43), channel_id=1, source_target_pairs={{0,22},{1,11},{2,24},{3,13},{4,26},{5,15},{6,28},{7,17},{8,30},{9,... | collective-permute-start | bytes 393224 | tf_op jit(solution)/shard_map/ppermute | solution.py:196
  88.8 1.6 %collective-permute-start.18 = (bf16[32,2048]{1,0:T(8,128)(2,1)S(1)}, bf16[32,2048]{1,0:T(8,128)(2,1)S(1)}, u32[]{:S(2)}, u32[]{:S(2)}) collective-permute-start(bf16[32,2048]{1,0:T(8,128)(2,1)S(1)} %get-tuple-element.44), channel_id=1, source_target_pairs={{0,10},{1,23},{2,12},{3,25},{4,14},{5,27},{6,16},{7,29},{8,18},{9,... | collective-permute-start | bytes 393224 | tf_op jit(solution)/shard_map/ppermute | solution.py:196
  90.4 0.0 collective-permute-done.15.other
  90.4 12.4 %collective-permute-done.17.one = bf16[32,2048]{1,0:T(8,128)(2,1)S(1)} collective-permute-done((bf16[32,2048]{1,0:T(8,128)(2,1)S(1)}, bf16[32,2048]{1,0:T(8,128)(2,1)S(1)}, u32[]{:S(2)}, u32[]{:S(2)}) %collective-permute-start.17) | collective-permute-done | bytes 131104 | tf_op jit(solution)/shard_map/ppermute | solution.py:196
  102.8 3.0 %collective-permute-done.18.two = bf16[32,2048]{1,0:T(8,128)(2,1)S(1)} collective-permute-done((bf16[32,2048]{1,0:T(8,128)(2,1)S(1)}, bf16[32,2048]{1,0:T(8,128)(2,1)S(1)}, u32[]{:S(2)}, u32[]{:S(2)}) %collective-permute-start.18) | collective-permute-done | bytes 131104 | tf_op jit(solution)/shard_map/ppermute | solution.py:196
  105.8 0.7 shard_map.78
  (4 shorter events, 0.0 us)
Async XLA Ops:
  1.5 29.5 %collective-permute-start.2 = (bf16[32,2176]{1,0:T(8,128)(2,1)S(1)}, bf16[32,2176]{1,0:T(8,128)(2,1)S(1)}, u32[]{:S(2)}, u32[]{:S(2)}) collective-permute-start(bf16[32,2176]{1,0:T(8,128)(2,1)S(1)} %shard_map.73.refs_0_), channel_id=1, source_target_pairs={{0,22},{1,11},{2,24},{3,13},{4,26},{5,15},{6,28},{7,17},{8,30},{9,... | collective-permute-start | bytes 417800 | tf_op jit(solution)/shard_map/ppermute | solution.py:196
  16.3 14.7 %collective-permute-start.1 = (bf16[32,2176]{1,0:T(8,128)(2,1)S(1)}, bf16[32,2176]{1,0:T(8,128)(2,1)S(1)}, u32[]{:S(2)}, u32[]{:S(2)}) collective-permute-start(bf16[32,2176]{1,0:T(8,128)(2,1)S(1)} %shard_map.73.refs_0_), channel_id=1, source_target_pairs={{0,10},{1,23},{2,12},{3,25},{4,14},{5,27},{6,16},{7,29},{8,18},{9,... | collective-permute-start | bytes 417800 | tf_op jit(solution)/shard_map/ppermute | solution.py:196
  16.3 15.2 %collective-permute-start = (bf16[32,2176]{1,0:T(8,128)(2,1)S(1)}, bf16[32,2176]{1,0:T(8,128)(2,1)S(1)}, u32[]{:S(2)}, u32[]{:S(2)}) collective-permute-start(bf16[32,2176]{1,0:T(8,128)(2,1)S(1)} %shard_map.73.refs_0_), channel_id=1, source_target_pairs={{0,1},{1,0},{2,3},{3,2},{4,5},{5,4},{6,7},{7,6},{8,9},{9,8},{10,11... | collective-permute-start | bytes 417800 | tf_op jit(solution)/shard_map/ppermute | solution.py:199
  31.0 1.4 %collective-permute-start.3 = (bf16[32,2176]{1,0:T(8,128)(2,1)S(1)}, bf16[32,2176]{1,0:T(8,128)(2,1)S(1)}, u32[]{:S(2)}, u32[]{:S(2)}) collective-permute-start(bf16[32,2176]{1,0:T(8,128)(2,1)S(1)} %collective-permute-done.2.refs_4_), channel_id=1, source_target_pairs={{0,1},{1,0},{2,3},{3,2},{4,5},{5,4},{6,7},{7,6},{8,9},{9,8},{10,11... | collective-permute-start | bytes 417800 | tf_op jit(solution)/shard_map/ppermute | solution.py:199
  31.0 1.6 %collective-permute-start.4 = (bf16[32,2176]{1,0:T(8,128)(2,1)S(1)}, bf16[32,2176]{1,0:T(8,128)(2,1)S(1)}, u32[]{:S(2)}, u32[]{:S(2)}) collective-permute-start(bf16[32,2176]{1,0:T(8,128)(2,1)S(1)} %collective-permute-done.1.refs_2_), channel_id=1, source_target_pairs={{0,1},{1,0},{2,3},{3,2},{4,5},{5,4},{6,7},{7,6},{8,9},{9,8},{10,11... | collective-permute-start | bytes 417800 | tf_op jit(solution)/shard_map/ppermute | solution.py:199
  31.5 24.1 %slice-start = ((s8[7340032]{0:T(1024)(128)(4,1)}), s8[4194304]{0:T(1024)(128)(4,1)S(1)}, s32[]{:S(2)}) async-start(s8[7340032]{0:T(1024)(128)(4,1)} %bitcast.8), calls=%async_computation | async-start | bytes 8388608
  31.5 24.1 %slice-start.2 = ((s8[7340032]{0:T(1024)(128)(4,1)}), s8[4194304]{0:T(1024)(128)(4,1)S(1)}, s32[]{:S(2)}) async-start(s8[7340032]{0:T(1024)(128)(4,1)} %bitcast.11), calls=%async_computation.2 | async-start | bytes 8388608
  31.5 24.1 %slice-start.4 = ((s8[7340032]{0:T(1024)(128)(4,1)}), s8[4194304]{0:T(1024)(128)(4,1)S(1)}, s32[]{:S(2)}) async-start(s8[7340032]{0:T(1024)(128)(4,1)} %bitcast.14), calls=%async_computation.4 | async-start | bytes 8388608
  31.6 24.0 %slice-start.1 = ((s8[7340032]{0:T(1024)(128)(4,1)}), s8[3145728]{0:T(1024)(128)(4,1)S(1)}, s32[]{:S(2)}) async-start(s8[7340032]{0:T(1024)(128)(4,1)} %bitcast.8), calls=%async_computation.1 | async-start | bytes 6291456
  31.6 24.0 %slice-start.3 = ((s8[7340032]{0:T(1024)(128)(4,1)}), s8[3145728]{0:T(1024)(128)(4,1)S(1)}, s32[]{:S(2)}) async-start(s8[7340032]{0:T(1024)(128)(4,1)} %bitcast.11), calls=%async_computation.3 | async-start | bytes 6291456
  31.6 24.0 %slice-start.5 = ((s8[7340032]{0:T(1024)(128)(4,1)}), s8[3145728]{0:T(1024)(128)(4,1)S(1)}, s32[]{:S(2)}) async-start(s8[7340032]{0:T(1024)(128)(4,1)} %bitcast.14), calls=%async_computation.5 | async-start | bytes 6291456
  33.8 21.7 %collective-permute-start.5 = (bf16[48,2048]{1,0:T(8,128)(2,1)S(1)}, bf16[48,2048]{1,0:T(8,128)(2,1)S(1)}, u32[]{:S(2)}, u32[]{:S(2)}) collective-permute-start(bf16[48,2048]{1,0:T(8,128)(2,1)S(1)} %get-tuple-element.25), channel_id=1, source_target_pairs={{0,4},{1,29},{2,6},{3,31},{4,8},{5,1},{6,10},{7,3},{8,12},{9,5},{1... | collective-permute-start | bytes 589832 | tf_op jit(solution)/shard_map/ppermute | solution.py:196
  34.0 21.6 %collective-permute-start.6 = (bf16[48,2048]{1,0:T(8,128)(2,1)S(1)}, bf16[48,2048]{1,0:T(8,128)(2,1)S(1)}, u32[]{:S(2)}, u32[]{:S(2)}) collective-permute-start(bf16[48,2048]{1,0:T(8,128)(2,1)S(1)} %get-tuple-element.26), channel_id=1, source_target_pairs={{0,28},{1,5},{2,30},{3,7},{4,0},{5,9},{6,2},{7,11},{8,4},{9,13},{1... | collective-permute-start | bytes 589832 | tf_op jit(solution)/shard_map/ppermute | solution.py:196
  38.1 17.5 %collective-permute-start.7 = (bf16[48,2048]{1,0:T(8,128)(2,1)S(1)}, bf16[48,2048]{1,0:T(8,128)(2,1)S(1)}, u32[]{:S(2)}, u32[]{:S(2)}) collective-permute-start(bf16[48,2048]{1,0:T(8,128)(2,1)S(1)} %get-tuple-element.27), channel_id=1, source_target_pairs={{0,2},{1,31},{2,4},{3,1},{4,6},{5,3},{6,8},{7,5},{8,10},{9,7},{10,... | collective-permute-start | bytes 589832 | tf_op jit(solution)/shard_map/ppermute | solution.py:196
  40.8 14.7 %collective-permute-start.8 = (bf16[48,2048]{1,0:T(8,128)(2,1)S(1)}, bf16[48,2048]{1,0:T(8,128)(2,1)S(1)}, u32[]{:S(2)}, u32[]{:S(2)}) collective-permute-start(bf16[48,2048]{1,0:T(8,128)(2,1)S(1)} %get-tuple-element.28), channel_id=1, source_target_pairs={{0,30},{1,3},{2,0},{3,5},{4,2},{5,7},{6,4},{7,9},{8,6},{9,11},{10,... | collective-permute-start | bytes 589832 | tf_op jit(solution)/shard_map/ppermute | solution.py:196
  42.2 13.4 %collective-permute-start.9 = (bf16[16,2048]{1,0:T(8,128)(2,1)S(1)}, bf16[16,2048]{1,0:T(8,128)(2,1)S(1)}, u32[]{:S(2)}, u32[]{:S(2)}) collective-permute-start(bf16[16,2048]{1,0:T(8,128)(2,1)S(1)} %get-tuple-element.30), channel_id=1, source_target_pairs={{0,6},{1,27},{2,8},{3,29},{4,10},{5,31},{6,12},{7,1},{8,14},{9,3},... | collective-permute-start | bytes 196616 | tf_op jit(solution)/shard_map/ppermute | solution.py:196
  63.8 16.3 %collective-permute-start.10 = (bf16[48,2048]{1,0:T(8,128)(2,1)S(1)}, bf16[48,2048]{1,0:T(8,128)(2,1)S(1)}, u32[]{:S(2)}, u32[]{:S(2)}) collective-permute-start(bf16[48,2048]{1,0:T(8,128)(2,1)S(1)} %get-tuple-element.31), channel_id=1, source_target_pairs={{0,28},{1,5},{2,30},{3,7},{4,0},{5,9},{6,2},{7,11},{8,4},{9,13},{1... | collective-permute-start | bytes 589832 | tf_op jit(solution)/shard_map/ppermute | solution.py:196
  66.4 13.7 %collective-permute-start.11 = (bf16[48,2048]{1,0:T(8,128)(2,1)S(1)}, bf16[48,2048]{1,0:T(8,128)(2,1)S(1)}, u32[]{:S(2)}, u32[]{:S(2)}) collective-permute-start(bf16[48,2048]{1,0:T(8,128)(2,1)S(1)} %get-tuple-element.32), channel_id=1, source_target_pairs={{0,4},{1,29},{2,6},{3,31},{4,8},{5,1},{6,10},{7,3},{8,12},{9,5},{1... | collective-permute-start | bytes 589832 | tf_op jit(solution)/shard_map/ppermute | solution.py:196
  66.8 14.2 %collective-permute-start.12 = (bf16[48,2048]{1,0:T(8,128)(2,1)S(1)}, bf16[48,2048]{1,0:T(8,128)(2,1)S(1)}, u32[]{:S(2)}, u32[]{:S(2)}) collective-permute-start(bf16[48,2048]{1,0:T(8,128)(2,1)S(1)} %get-tuple-element.33), channel_id=1, source_target_pairs={{0,30},{1,3},{2,0},{3,5},{4,2},{5,7},{6,4},{7,9},{8,6},{9,11},{10,... | collective-permute-start | bytes 589832 | tf_op jit(solution)/shard_map/ppermute | solution.py:196
  68.3 12.9 %collective-permute-start.13 = (bf16[48,2048]{1,0:T(8,128)(2,1)S(1)}, bf16[48,2048]{1,0:T(8,128)(2,1)S(1)}, u32[]{:S(2)}, u32[]{:S(2)}) collective-permute-start(bf16[48,2048]{1,0:T(8,128)(2,1)S(1)} %get-tuple-element.34), channel_id=1, source_target_pairs={{0,2},{1,31},{2,4},{3,1},{4,6},{5,3},{6,8},{7,5},{8,10},{9,7},{10,... | collective-permute-start | bytes 589832 | tf_op jit(solution)/shard_map/ppermute | solution.py:196
  68.9 11.3 %collective-permute-start.14 = (bf16[16,2048]{1,0:T(8,128)(2,1)S(1)}, bf16[16,2048]{1,0:T(8,128)(2,1)S(1)}, u32[]{:S(2)}, u32[]{:S(2)}) collective-permute-start(bf16[16,2048]{1,0:T(8,128)(2,1)S(1)} %get-tuple-element.36), channel_id=1, source_target_pairs={{0,26},{1,7},{2,28},{3,9},{4,30},{5,11},{6,0},{7,13},{8,2},{9,15},... | collective-permute-start | bytes 196616 | tf_op jit(solution)/shard_map/ppermute | solution.py:196
  81.8 1.7 %collective-permute-start.16 = (bf16[64,2048]{1,0:T(8,128)(2,1)S(1)}, bf16[64,2048]{1,0:T(8,128)(2,1)S(1)}, u32[]{:S(2)}, u32[]{:S(2)}) collective-permute-start(bf16[64,2048]{1,0:T(8,128)(2,1)S(1)} %get-tuple-element.42), channel_id=1, source_target_pairs={{0,1},{1,0},{2,3},{3,2},{4,5},{5,4},{6,7},{7,6},{8,9},{9,8},{10,11... | collective-permute-start | bytes 786440 | tf_op jit(solution)/shard_map/ppermute | solution.py:199
  81.9 8.5 %collective-permute-start.15 = (bf16[32,2048]{1,0:T(8,128)(2,1)S(1)}, bf16[32,2048]{1,0:T(8,128)(2,1)S(1)}, u32[]{:S(2)}, u32[]{:S(2)}) collective-permute-start(bf16[32,2048]{1,0:T(8,128)(2,1)S(1)} %get-tuple-element.40), channel_id=1, source_target_pairs={{0,1},{1,0},{2,3},{3,2},{4,5},{5,4},{6,7},{7,6},{8,9},{9,8},{10,11... | collective-permute-start | bytes 393224 | tf_op jit(solution)/shard_map/ppermute | solution.py:199
  83.5 19.3 %collective-permute-start.17 = (bf16[32,2048]{1,0:T(8,128)(2,1)S(1)}, bf16[32,2048]{1,0:T(8,128)(2,1)S(1)}, u32[]{:S(2)}, u32[]{:S(2)}) collective-permute-start(bf16[32,2048]{1,0:T(8,128)(2,1)S(1)} %get-tuple-element.43), channel_id=1, source_target_pairs={{0,22},{1,11},{2,24},{3,13},{4,26},{5,15},{6,28},{7,17},{8,30},{9,... | collective-permute-start | bytes 393224 | tf_op jit(solution)/shard_map/ppermute | solution.py:196
  88.8 17.0 %collective-permute-start.18 = (bf16[32,2048]{1,0:T(8,128)(2,1)S(1)}, bf16[32,2048]{1,0:T(8,128)(2,1)S(1)}, u32[]{:S(2)}, u32[]{:S(2)}) collective-permute-start(bf16[32,2048]{1,0:T(8,128)(2,1)S(1)} %get-tuple-element.44), channel_id=1, source_target_pairs={{0,10},{1,23},{2,12},{3,25},{4,14},{5,27},{6,16},{7,29},{8,18},{9,... | collective-permute-start | bytes 393224 | tf_op jit(solution)/shard_map/ppermute | solution.py:196

commit v5 on v4

--- a/solution.py
+++ b/solution.py
@@ -73,33 +73,30 @@
     out_ref[:, width:] = meta.astype(jnp.bfloat16)
 
 
-def hand_on(chips, cap, top, place_ref, *refs):
-    sources, refs = refs[:6], refs[6:]
-    blocks, (high_ref, low_ref, all_ref) = refs[:6], refs[6:]
+def hand_on(chips, cap, top, count, place_ref, *refs):
+    sources, refs = refs[:count], refs[count:]
+    blocks, (high_ref, low_ref, all_ref) = refs[:-3], refs[-3:]
     rows = sources[0].shape[0]
     width = blocks[0].shape[1]
     z, c = place_ref[0], place_ref[1]
-    near = 6 * cap
-    slots = len(NEAR) * near + 2 * cap
+    near = count * cap
+    slots = high_ref.shape[1]
     col = lax.broadcasted_iota(jnp.int32, (1, slots), 1)
     block = sum((col >= near * i).astype(jnp.int32) for i in range(1, len(NEAR) + 1))
     inside = col - block * near
-    source = sum((inside >= cap * i).astype(jnp.int32) for i in range(1, 6))
+    source = sum((inside >= cap * i).astype(jnp.int32) for i in range(1, count))
     slot = inside - source * cap
-    across = block == len(NEAR)
-    source = jnp.where(across, source + 2, source)
     step = sum(jnp.where(block == i, d, 0) for i, d in enumerate((*NEAR, 3)))
     chip = z + jnp.where(c == 0, step, -step)
     chip = jnp.where(chip < 0, chip + chips, chip)
     chip = jnp.where(chip >= chips, chip - chips, chip)
     target = ((2 * chip + c) * cap + slot + source * 2 * chips * cap).astype(jnp.float32)
-    for s in range(6):
+    for s in range(count):
         all_ref[s * rows : (s + 1) * rows, :] = sources[s][...]
     meta = all_ref[:, width:].astype(jnp.float32)
-    offset = (lax.broadcasted_iota(jnp.int32, (6 * rows, 1), 0) // rows * (2 * chips * cap)).astype(
-        jnp.float32
-    )
-    pick = jnp.zeros((6 * rows, slots), jnp.float32)
+    index = lax.broadcasted_iota(jnp.int32, (count * rows, 1), 0) // rows
+    offset = (index * (2 * chips * cap)).astype(jnp.float32)
+    pick = jnp.zeros((count * rows, slots), jnp.float32)
     high, low = pick, pick
     for k in range(top):
         hit = meta[:, k : k + 1] + offset == target
@@ -114,18 +111,23 @@
         (((0,), (0,)), ((), ())),
         preferred_element_type=jnp.float32,
     ).astype(jnp.bfloat16)
-    for i in range(len(NEAR)):
-        blocks[i][...] = taken[i * near : (i + 1) * near]
-    blocks[5][...] = taken[len(NEAR) * near :]
-
-
-def experts(tile, *refs):
-    blocks, (gate_ref, up_ref, down_ref), refs = refs[:6], refs[6:9], refs[9:]
-    outs, (x_ref, total_ref) = refs[:6], refs[6:]
+    at = 0
+    for b in blocks:
+        b[...] = taken[at : at + b.shape[0]]
+        at += b.shape[0]
+
+
+def gather(blocks, x_ref):
     at = 0
     for b in blocks:
         x_ref[at : at + b.shape[0], :] = b[...]
         at += b.shape[0]
+
+
+def experts(tile, count, *refs):
+    blocks, (gate_ref, up_ref, down_ref), refs = refs[:count], refs[count : count + 3], refs[count + 3 :]
+    outs, (x_ref, total_ref) = refs[:count], refs[count:]
+    gather(blocks, x_ref)
     hidden = gate_ref.shape[1]
     total_ref[...] = jnp.zeros_like(total_ref)
 
@@ -146,24 +148,29 @@
         at += o.shape[0]
 
 
-def weigh(*refs):
-    blocks, (high_ref, low_ref), refs = refs[:6], refs[6:8], refs[8:]
-    far_mine, far_other, mine, other, x_ref = refs
-    at = 0
-    for b in blocks:
-        x_ref[at : at + b.shape[0], :] = b[...]
-        at += b.shape[0]
+def weighted(blocks, high_ref, low_ref, x_ref):
+    gather(blocks, x_ref)
     x = x_ref[...]
     total = jnp.dot(high_ref[...], x, preferred_element_type=jnp.float32)
-    total += jnp.dot(low_ref[...], x, preferred_element_type=jnp.float32)
+    return total + jnp.dot(low_ref[...], x, preferred_element_type=jnp.float32)
+
+
+def weigh_near(*refs):
+    mine, other, x_ref = refs[-3:]
+    total = weighted(refs[:-5], *refs[-5:-3], x_ref)
     rows = mine.shape[0]
     mine[...] = total[:rows]
-    other[...] = total[rows : 2 * rows].astype(jnp.bfloat16)
-    for i in range(2):
-        far_mine[i * rows : (i + 1) * rows, :] = total[(2 + 2 * i) * rows : (3 + 2 * i) * rows]
-        far_other[i * rows : (i + 1) * rows, :] = total[
-            (5 - 2 * i) * rows : (6 - 2 * i) * rows
-        ].astype(jnp.bfloat16)
+    other[...] = total[rows:].astype(jnp.bfloat16)
+
+
+def weigh_far(*refs):
+    mine, other, x_ref = refs[-3:]
+    total = weighted(refs[:-5], *refs[-5:-3], x_ref)
+    rows = mine.shape[0] // 2
+    mine[:rows] = total[:rows]
+    mine[rows:] = total[2 * rows : 3 * rows]
+    other[:rows] = total[3 * rows :].astype(jnp.bfloat16)
+    other[rows:] = total[rows : 2 * rows].astype(jnp.bfloat16)
 
 
 def join(mine, other, one, two):
@@ -214,38 +221,53 @@
         compiler_params=pltpu.CompilerParams(vmem_limit_bytes=60 << 20),
         cost_estimate=pl.CostEstimate(flops=1 << 20, bytes_accessed=1 << 20, transcendentals=0),
     )(tokens, norm_gain[None, :], routes.T, route_logits.T)
+    own2 = swap(own)
     low, high = shift(own, HOP), shift(own, -HOP)
-    own2, high2, low2 = swap(own), swap(low), swap(high)
-    near = 6 * cap
-    slots = len(NEAR) * near + 2 * cap
-    shapes = [bf16(near, width)] * len(NEAR) + [bf16(2 * cap, width)]
-    weight = bf16(6 * rows, slots)
-    *blocks, w_high, w_low = call(
-        functools.partial(hand_on, chips, cap, top),
-        shapes + [weight, weight],
-        7,
-        smem=1,
-        scratch=[pltpu.VMEM((6 * rows, width + META), jnp.bfloat16)],
-        flops=4 * 6 * slots * width * hidden,
-    )(place, own, own2, low, low2, high, high2)
-    last = shift(blocks[5], 3)
-    given = [shift(b, d) if d else b for b, d in zip(blocks, NEAR)] + [last]
-    results = call(
-        functools.partial(experts, 256),
-        shapes,
-        9,
-        limit=LIMIT,
-        scratch=[pltpu.VMEM((slots, width), jnp.bfloat16), pltpu.VMEM((slots, width), jnp.float32)],
-        flops=6 * slots * width * hidden,
-    )(*given, w_gate[0], w_up[0], w_down[0])
-    last = shift(results[5], -3)
-    back = [shift(b, -d) if d else b for b, d in zip(results, NEAR)] + [last]
-    far_mine, far_other, mine, other = call(
-        weigh,
-        [f32(2 * rows, width), bf16(2 * rows, width), f32(rows, width), bf16(rows, width)],
-        8,
-        scratch=[pltpu.VMEM((slots, width), jnp.bfloat16)],
-    )(*back, w_high, w_low)
+    high2, low2 = swap(low), swap(high)
+    steps = (*NEAR, 3)
+
+    def hand(sources, sizes, flops):
+        count = len(sources)
+        weight = bf16(count * rows, sum(sizes))
+        *blocks, w_high, w_low = call(
+            functools.partial(hand_on, chips, cap, top, count),
+            [bf16(n, width) for n in sizes] + [weight, weight],
+            count + 1,
+            smem=1,
+            scratch=[pltpu.VMEM((count * rows, width + META), jnp.bfloat16)],
+            flops=flops,
+        )(place, *sources)
+        return [shift(b, d) if d else b for b, d in zip(blocks, steps)], (w_high, w_low)
+
+    def run(blocks):
+        slots = sum(b.shape[0] for b in blocks)
+        experts_of = call(
+            functools.partial(experts, 256, len(blocks)),
+            [bf16(*b.shape) for b in blocks],
+            len(blocks) + 3,
+            scratch=[pltpu.VMEM((slots, width), jnp.bfloat16), pltpu.VMEM((slots, width), jnp.float32)],
+            flops=6 * slots * width * hidden,
+        )
+        return experts_of(*blocks, w_gate[0], w_up[0], w_down[0])
+
+    def weigh(body, blocks, weights, rows):
+        back = [shift(b, -d) if d else b for b, d in zip(blocks, steps)]
+        slots = sum(b.shape[0] for b in blocks)
+        sums_of = call(
+            body,
+            [f32(rows, width), bf16(rows, width)],
+            len(back) + 2,
+            scratch=[pltpu.VMEM((slots, width), jnp.bfloat16)],
+        )
+        return sums_of(*back, *weights)
+
+    heavy = 24 * 256 * width * hidden
+    near, near_weights = hand((own, own2), [2 * cap] * 5, heavy)
+    far, far_weights = hand((low, low2, high, high2), [4 * cap] * 5 + [2 * cap], 1 << 28)
+    near = run(near)
+    far = run(far)
+    mine, other = weigh(weigh_near, near, near_weights, rows)
+    far_mine, far_other = weigh(weigh_far, far, far_weights, 2 * rows)
     one, two = call(join, [bf16(rows, width)] * 2, 2)(far_mine, swap(far_other))
     return call(finish, bf16(rows, width), 4)(mine, swap(other), shift(one, -HOP), shift(two, HOP))
 
@@ -263,6 +285,7 @@
         P(ep, None, None),
         P(ep, None, None),
     )
+
     return jax.shard_map(
         shards, mesh=split, in_specs=placed, out_specs=P(GRP_EP, None), check_vma=False
     )

time: 108 us -> 133 us (1.23)
  starting transfers between devices: 40.5 us -> 55.2 us
  local copies, waits for them, and re-layouts: 0.02 us -> 9.25 us
  Pallas kernels: 12.3 us -> 16.9 us
  waiting for transfers between devices: 53.4 us -> 51 us
    ppermute x14 -> x22, starting transfers between devices: 39.4 us -> 54.4 us  [shift(): return lax.ppermute(x, ('z', 'c'), pairs)]
    unnamed x12 -> x10, local copies, waits for them, and re-layouts: 0.02 us -> 9.25 us
    pallas_call x3 -> x6, Pallas kernels: 10.1 us -> 14.6 us  [the longest x2 11.9 us: run(): return experts_of(*blocks, w_gate[0], w_up[0], w_down[0])]
    ppermute x14 -> x22, waiting for transfers between devices: 51.4 us -> 50 us  [shift(): return lax.ppermute(x, ('z', 'c'), pairs)]
  transfers between devices with their start and end apart: 19 -> 27, of which waited for: 10 -> 10; matrix products, arithmetic and copies ran while one was open for 0% -> 0% of each run, Pallas kernels for 0% -> 10%
where the time goes in v5:
time: 133 us
  starting transfers between devices  55.2 us (42%)
  waiting for transfers between devices  51 us (38%)
  Pallas kernels  16.9 us (13%)
  local copies, waits for them, and re-layouts  9.25 us (7%)
    ppermute x22, starting transfers between devices, shift(): return lax.ppermute(x, ('z', 'c'), pairs)  54.4 us
    ppermute x22, waiting for transfers between devices, shift(): return lax.ppermute(x, ('z', 'c'), pairs)  50 us
    pallas_call x2, Pallas kernels, run(): return experts_of(*blocks, w_gate[0], w_up[0], w_down[0])  11.9 us
    unnamed x10, local copies, waits for them, and re-layouts  9.25 us
  transfers between devices with their start and end apart: 27, of which 10 were waited for; matrix products, arithmetic and copies ran while one was open for 0% of the time, Pallas kernels for 10%

profile of v5, /device:TPU:86, one launch (start us, length us, event | category | flops | bytes accessed | tf_op | source)
XLA Modules:
  0.0 132.5 jit_solution(7208015107228809967)
XLA Ops:
  0.0 1.5 %shard_map.73.refs_0_ = bf16[32,2176]{1,0:T(8,128)(2,1)S(1)} custom-call(bf16[32,2048]{1,0:T(8,128)(2,1)} %tok_hbm.1, f32[1,2048]{1,0:T(1,128)} %bitcast.16, s32[4,32]{1,0:T(4,128)} %bitcast.17, f32[4,32]{1,0:T(4,128)} %bitcast.18), custom_call_target="tpu_custom_call" | custom-call | flops 1048576 | bytes 1048576 | tf_op jit(solution)/shard_map/pallas_call | solution.py:209
  1.5 14.8 %collective-permute-start.11 = (bf16[32,2176]{1,0:T(8,128)(2,1)S(1)}, bf16[32,2176]{1,0:T(8,128)(2,1)S(1)}, u32[]{:S(2)}, u32[]{:S(2)}) collective-permute-start(bf16[32,2176]{1,0:T(8,128)(2,1)S(1)} %shard_map.73.refs_0_), channel_id=1, source_target_pairs={{0,22},{1,11},{2,24},{3,13},{4,26},{5,15},{6,28},{7,17},{8,30},{9,... | collective-permute-start | bytes 417800 | tf_op jit(solution)/shard_map/ppermute | solution.py:203
  16.3 0.0 collective-permute-start.10
  16.3 14.6 %collective-permute-done.11.refs_2_ = bf16[32,2176]{1,0:T(8,128)(2,1)S(1)} collective-permute-done((bf16[32,2176]{1,0:T(8,128)(2,1)S(1)}, bf16[32,2176]{1,0:T(8,128)(2,1)S(1)}, u32[]{:S(2)}, u32[]{:S(2)}) %collective-permute-start.11) | collective-permute-done | bytes 139296 | tf_op jit(solution)/shard_map/ppermute | solution.py:203
  31.0 0.0 collective-permute-start.12
  31.0 0.0 collective-permute-done.10.refs_0_
  31.0 0.5 collective-permute-start.13
  31.5 0.1 pad_add_fusion.place_ref
  31.6 0.8 collective-permute-done.12.refs_1_
  32.3 0.2 collective-permute-done.13.refs_3_
  32.5 1.1 shard_map.77
  33.6 0.1 collective-permute-start.14
  33.8 4.1 %collective-permute-start.15 = (bf16[32,2048]{1,0:T(8,128)(2,1)S(1)}, bf16[32,2048]{1,0:T(8,128)(2,1)S(1)}, u32[]{:S(2)}, u32[]{:S(2)}) collective-permute-start(bf16[32,2048]{1,0:T(8,128)(2,1)S(1)} %get-tuple-element.52), channel_id=1, source_target_pairs={{0,28},{1,5},{2,30},{3,7},{4,0},{5,9},{6,2},{7,11},{8,4},{9,13},{1... | collective-permute-start | bytes 393224 | tf_op jit(solution)/shard_map/ppermute | solution.py:203
  37.9 2.8 %collective-permute-start.16 = (bf16[32,2048]{1,0:T(8,128)(2,1)S(1)}, bf16[32,2048]{1,0:T(8,128)(2,1)S(1)}, u32[]{:S(2)}, u32[]{:S(2)}) collective-permute-start(bf16[32,2048]{1,0:T(8,128)(2,1)S(1)} %get-tuple-element.53), channel_id=1, source_target_pairs={{0,2},{1,31},{2,4},{3,1},{4,6},{5,3},{6,8},{7,5},{8,10},{9,7},{10,... | collective-permute-start | bytes 393224 | tf_op jit(solution)/shard_map/ppermute | solution.py:203
  40.6 1.3 %collective-permute-start.17 = (bf16[32,2048]{1,0:T(8,128)(2,1)S(1)}, bf16[32,2048]{1,0:T(8,128)(2,1)S(1)}, u32[]{:S(2)}, u32[]{:S(2)}) collective-permute-start(bf16[32,2048]{1,0:T(8,128)(2,1)S(1)} %get-tuple-element.54), channel_id=1, source_target_pairs={{0,30},{1,3},{2,0},{3,5},{4,2},{5,7},{6,4},{7,9},{8,6},{9,11},{10,... | collective-permute-start | bytes 393224 | tf_op jit(solution)/shard_map/ppermute | solution.py:203
  42.0 0.9 collective-permute-start.18
  42.9 8.1 %collective-permute-done.18.refs_5_ = bf16[16,2048]{1,0:T(8,128)(2,1)S(1)} collective-permute-done((bf16[16,2048]{1,0:T(8,128)(2,1)S(1)}, bf16[16,2048]{1,0:T(8,128)(2,1)S(1)}, u32[]{:S(2)}, u32[]{:S(2)}) %collective-permute-start.18) | collective-permute-done | bytes 65568 | tf_op jit(solution)/shard_map/ppermute | solution.py:203
  51.0 0.0 collective-permute-start
  51.0 0.0 collective-permute-done.14.refs_0_
  51.0 0.0 collective-permute-done.15.refs_1_
  51.0 0.0 collective-permute-done.16.refs_2_
  51.0 0.0 copy-start
  51.0 3.1 %copy-done = bf16[1,2048,1792]{2,1,0:T(8,128)(2,1)S(1)} copy-done((bf16[1,2048,1792]{2,1,0:T(8,128)(2,1)S(1)}, bf16[1,2048,1792]{2,1,0:T(8,128)(2,1)}, u32[]{:S(2)}) %copy-start) | copy-done | bytes 7340056
  54.1 3.1 %copy-done.1 = bf16[1,2048,1792]{2,1,0:T(8,128)(2,1)S(1)} copy-done((bf16[1,2048,1792]{2,1,0:T(8,128)(2,1)S(1)}, bf16[1,2048,1792]{2,1,0:T(8,128)(2,1)}, u32[]{:S(2)}) %copy-start.1) | copy-done | bytes 7340056
  57.2 3.1 %copy-done.2 = bf16[1,1792,2048]{2,1,0:T(8,128)(2,1)S(1)} copy-done((bf16[1,1792,2048]{2,1,0:T(8,128)(2,1)S(1)}, bf16[1,1792,2048]{2,1,0:T(8,128)(2,1)}, u32[]{:S(2)}) %copy-start.2) | copy-done | bytes 7340056
  60.3 6.4 %shard_map.78 = (bf16[32,2048]{1,0:T(8,128)(2,1)S(1)}, bf16[32,2048]{1,0:T(8,128)(2,1)S(1)}, bf16[32,2048]{1,0:T(8,128)(2,1)S(1)}, bf16[32,2048]{1,0:T(8,128)(2,...) custom-call(bf16[32,2048]{1,0:T(8,128)(2,1)S(1)} %collective-permute-done.14.refs_0_, ...), custom_call_target="tpu_custom_call" | custom-call | flops 3875536896 | bytes 1048576 | tf_op jit(solution)/shard_map/pallas_call | solution.py:251
  66.6 2.4 %collective-permute-start.19 = (bf16[32,2048]{1,0:T(8,128)(2,1)S(1)}, bf16[32,2048]{1,0:T(8,128)(2,1)S(1)}, u32[]{:S(2)}, u32[]{:S(2)}) collective-permute-start(bf16[32,2048]{1,0:T(8,128)(2,1)S(1)} %get-tuple-element.57), channel_id=1, source_target_pairs={{0,28},{1,5},{2,30},{3,7},{4,0},{5,9},{6,2},{7,11},{8,4},{9,13},{1... | collective-permute-start | bytes 393224 | tf_op jit(solution)/shard_map/ppermute | solution.py:203
  69.1 0.6 collective-permute-start.20
  69.7 2.7 %collective-permute-start.21 = (bf16[32,2048]{1,0:T(8,128)(2,1)S(1)}, bf16[32,2048]{1,0:T(8,128)(2,1)S(1)}, u32[]{:S(2)}, u32[]{:S(2)}) collective-permute-start(bf16[32,2048]{1,0:T(8,128)(2,1)S(1)} %get-tuple-element.59), channel_id=1, source_target_pairs={{0,30},{1,3},{2,0},{3,5},{4,2},{5,7},{6,4},{7,9},{8,6},{9,11},{10,... | collective-permute-start | bytes 393224 | tf_op jit(solution)/shard_map/ppermute | solution.py:203
  72.3 0.0 collective-permute-start.22
  72.3 0.0 collective-permute-done.refs_1_
  72.4 0.0 slice-start.1
  72.4 3.2 %collective-permute-start.23 = (bf16[16,2048]{1,0:T(8,128)(2,1)S(1)}, bf16[16,2048]{1,0:T(8,128)(2,1)S(1)}, u32[]{:S(2)}, u32[]{:S(2)}) collective-permute-start(bf16[16,2048]{1,0:T(8,128)(2,1)S(1)} %get-tuple-element.62), channel_id=1, source_target_pairs={{0,26},{1,7},{2,28},{3,9},{4,30},{5,11},{6,0},{7,13},{8,2},{9,15},... | collective-permute-start | bytes 196616 | tf_op jit(solution)/shard_map/ppermute | solution.py:203
  75.5 0.9 shard_map.74
  76.5 6.4 %collective-permute-done.23.refs_5_ = bf16[16,2048]{1,0:T(8,128)(2,1)S(1)} collective-permute-done((bf16[16,2048]{1,0:T(8,128)(2,1)S(1)}, bf16[16,2048]{1,0:T(8,128)(2,1)S(1)}, u32[]{:S(2)}, u32[]{:S(2)}) %collective-permute-start.23) | collective-permute-done | bytes 65568 | tf_op jit(solution)/shard_map/ppermute | solution.py:203
  82.9 0.8 collective-permute-start.1
  83.7 0.0 collective-permute-done.19.refs_0_
  83.7 3.3 %collective-permute-start.2 = (bf16[16,2048]{1,0:T(8,128)(2,1)S(1)}, bf16[16,2048]{1,0:T(8,128)(2,1)S(1)}, u32[]{:S(2)}, u32[]{:S(2)}) collective-permute-start(bf16[16,2048]{1,0:T(8,128)(2,1)S(1)} %get-tuple-element.38), channel_id=1, source_target_pairs={{0,28},{1,5},{2,30},{3,7},{4,0},{5,9},{6,2},{7,11},{8,4},{9,13},{1... | collective-permute-start | bytes 196616 | tf_op jit(solution)/shard_map/ppermute | solution.py:203
  87.0 0.0 collective-permute-done.20.refs_1_
  87.0 0.0 collective-permute-start.3
  87.0 0.0 collective-permute-done.21.refs_2_
  87.0 3.2 %collective-permute-start.4 = (bf16[16,2048]{1,0:T(8,128)(2,1)S(1)}, bf16[16,2048]{1,0:T(8,128)(2,1)S(1)}, u32[]{:S(2)}, u32[]{:S(2)}) collective-permute-start(bf16[16,2048]{1,0:T(8,128)(2,1)S(1)} %get-tuple-element.40), channel_id=1, source_target_pairs={{0,30},{1,3},{2,0},{3,5},{4,2},{5,7},{6,4},{7,9},{8,6},{9,11},{10,... | collective-permute-start | bytes 196616 | tf_op jit(solution)/shard_map/ppermute | solution.py:203
  90.2 0.0 collective-permute-done.22.refs_3_
  90.2 0.4 shard_map.79
  90.7 0.1 collective-permute-start.24
  90.8 0.0 collective-permute-done.2.refs_1_
  90.9 2.0 %collective-permute-done.3.refs_2_ = bf16[16,2048]{1,0:T(8,128)(2,1)S(1)} collective-permute-done((bf16[16,2048]{1,0:T(8,128)(2,1)S(1)}, bf16[16,2048]{1,0:T(8,128)(2,1)S(1)}, u32[]{:S(2)}, u32[]{:S(2)}) %collective-permute-start.3) | collective-permute-done | bytes 65568 | tf_op jit(solution)/shard_map/ppermute | solution.py:203
  92.8 0.0 collective-permute-done.4.refs_3_
  92.8 5.5 %shard_map.75 = (bf16[16,2048]{1,0:T(8,128)(2,1)S(1)}, bf16[16,2048]{1,0:T(8,128)(2,1)S(1)}, bf16[16,2048]{1,0:T(8,128)(2,1)S(1)}, bf16[16,2048]{1,0:T(8,128)(2,1)S(1)}, bf16[16,2048]{1,0:T(8,128)(2,1)S(1)}) custom-call(bf16[16,2048]{1,0:T(8,128)(2,1)S(1)} %collective-permute-done.1.refs_0_, bf16[16,2048]{1,0:T(8,128)(2,1)S(1)} %collective-permute-done.2.refs_1_, ...), custom_call_target="tpu_custom_call" | custom-call | flops 1761607680 | bytes 1048576 | tf_op jit(solution)/shard_map/pallas_call | solution.py:251
  98.3 1.7 %collective-permute-start.5 = (bf16[16,2048]{1,0:T(8,128)(2,1)S(1)}, bf16[16,2048]{1,0:T(8,128)(2,1)S(1)}, u32[]{:S(2)}, u32[]{:S(2)}) collective-permute-start(bf16[16,2048]{1,0:T(8,128)(2,1)S(1)} %get-tuple-element.42), channel_id=1, source_target_pairs={{0,28},{1,5},{2,30},{3,7},{4,0},{5,9},{6,2},{7,11},{8,4},{9,13},{1... | collective-permute-start | bytes 196616 | tf_op jit(solution)/shard_map/ppermute | solution.py:203
  100.0 1.3 %collective-permute-start.6 = (bf16[16,2048]{1,0:T(8,128)(2,1)S(1)}, bf16[16,2048]{1,0:T(8,128)(2,1)S(1)}, u32[]{:S(2)}, u32[]{:S(2)}) collective-permute-start(bf16[16,2048]{1,0:T(8,128)(2,1)S(1)} %get-tuple-element.43), channel_id=1, source_target_pairs={{0,4},{1,29},{2,6},{3,31},{4,8},{5,1},{6,10},{7,3},{8,12},{9,5},{1... | collective-permute-start | bytes 196616 | tf_op jit(solution)/shard_map/ppermute | solution.py:203
  101.3 4.1 %collective-permute-start.7 = (bf16[16,2048]{1,0:T(8,128)(2,1)S(1)}, bf16[16,2048]{1,0:T(8,128)(2,1)S(1)}, u32[]{:S(2)}, u32[]{:S(2)}) collective-permute-start(bf16[16,2048]{1,0:T(8,128)(2,1)S(1)} %get-tuple-element.44), channel_id=1, source_target_pairs={{0,30},{1,3},{2,0},{3,5},{4,2},{5,7},{6,4},{7,9},{8,6},{9,11},{10,... | collective-permute-start | bytes 196616 | tf_op jit(solution)/shard_map/ppermute | solution.py:203
  105.5 0.0 collective-permute-start.8
  105.5 0.0 collective-permute-done.5.refs_0_
  105.5 1.0 collective-permute-done.6.refs_1_
  106.5 0.9 collective-permute-done.7.refs_2_
  107.4 3.6 %collective-permute-done.8.refs_3_ = bf16[16,2048]{1,0:T(8,128)(2,1)S(1)} collective-permute-done((bf16[16,2048]{1,0:T(8,128)(2,1)S(1)}, bf16[16,2048]{1,0:T(8,128)(2,1)S(1)}, u32[]{:S(2)}, u32[]{:S(2)}) %collective-permute-start.8) | collective-permute-done | bytes 65568 | tf_op jit(solution)/shard_map/ppermute | solution.py:203
  110.9 0.3 shard_map.76
  111.2 0.1 collective-permute-start.9
  111.4 0.0 collective-permute-done.24.other
  111.4 2.8 %collective-permute-start.25 = (bf16[32,2048]{1,0:T(8,128)(2,1)S(1)}, bf16[32,2048]{1,0:T(8,128)(2,1)S(1)}, u32[]{:S(2)}, u32[]{:S(2)}) collective-permute-start(bf16[32,2048]{1,0:T(8,128)(2,1)S(1)} %get-tuple-element.67), channel_id=1, source_target_pairs={{0,22},{1,11},{2,24},{3,13},{4,26},{5,15},{6,28},{7,17},{8,30},{9,... | collective-permute-start | bytes 393224 | tf_op jit(solution)/shard_map/ppermute | solution.py:203
  114.3 4.1 %collective-permute-start.26 = (bf16[32,2048]{1,0:T(8,128)(2,1)S(1)}, bf16[32,2048]{1,0:T(8,128)(2,1)S(1)}, u32[]{:S(2)}, u32[]{:S(2)}) collective-permute-start(bf16[32,2048]{1,0:T(8,128)(2,1)S(1)} %get-tuple-element.68), channel_id=1, source_target_pairs={{0,10},{1,23},{2,12},{3,25},{4,14},{5,27},{6,16},{7,29},{8,18},{9,... | collective-permute-start | bytes 393224 | tf_op jit(solution)/shard_map/ppermute | solution.py:203
  118.4 13.5 %collective-permute-done.25.one = bf16[32,2048]{1,0:T(8,128)(2,1)S(1)} collective-permute-done((bf16[32,2048]{1,0:T(8,128)(2,1)S(1)}, bf16[32,2048]{1,0:T(8,128)(2,1)S(1)}, u32[]{:S(2)}, u32[]{:S(2)}) %collective-permute-start.25) | collective-permute-done | bytes 131104 | tf_op jit(solution)/shard_map/ppermute | solution.py:203
  131.8 0.7 shard_map.81
  (11 shorter events, 0.1 us)
Async XLA Ops:
  1.5 29.5 %collective-permute-start.11 = (bf16[32,2176]{1,0:T(8,128)(2,1)S(1)}, bf16[32,2176]{1,0:T(8,128)(2,1)S(1)}, u32[]{:S(2)}, u32[]{:S(2)}) collective-permute-start(bf16[32,2176]{1,0:T(8,128)(2,1)S(1)} %shard_map.73.refs_0_), channel_id=1, source_target_pairs={{0,22},{1,11},{2,24},{3,13},{4,26},{5,15},{6,28},{7,17},{8,30},{9,... | collective-permute-start | bytes 417800 | tf_op jit(solution)/shard_map/ppermute | solution.py:203
  16.3 14.7 %collective-permute-start.10 = (bf16[32,2176]{1,0:T(8,128)(2,1)S(1)}, bf16[32,2176]{1,0:T(8,128)(2,1)S(1)}, u32[]{:S(2)}, u32[]{:S(2)}) collective-permute-start(bf16[32,2176]{1,0:T(8,128)(2,1)S(1)} %shard_map.73.refs_0_), channel_id=1, source_target_pairs={{0,10},{1,23},{2,12},{3,25},{4,14},{5,27},{6,16},{7,29},{8,18},{9,... | collective-permute-start | bytes 417800 | tf_op jit(solution)/shard_map/ppermute | solution.py:203
  31.0 1.4 %collective-permute-start.12 = (bf16[32,2176]{1,0:T(8,128)(2,1)S(1)}, bf16[32,2176]{1,0:T(8,128)(2,1)S(1)}, u32[]{:S(2)}, u32[]{:S(2)}) collective-permute-start(bf16[32,2176]{1,0:T(8,128)(2,1)S(1)} %collective-permute-done.11.refs_2_), channel_id=1, source_target_pairs={{0,1},{1,0},{2,3},{3,2},{4,5},{5,4},{6,7},{7,6},{8,9},{9,8},{10,11... | collective-permute-start | bytes 417800 | tf_op jit(solution)/shard_map/ppermute | solution.py:206
  31.0 1.6 %collective-permute-start.13 = (bf16[32,2176]{1,0:T(8,128)(2,1)S(1)}, bf16[32,2176]{1,0:T(8,128)(2,1)S(1)}, u32[]{:S(2)}, u32[]{:S(2)}) collective-permute-start(bf16[32,2176]{1,0:T(8,128)(2,1)S(1)} %collective-permute-done.10.refs_0_), channel_id=1, source_target_pairs={{0,1},{1,0},{2,3},{3,2},{4,5},{5,4},{6,7},{7,6},{8,9},{9,8},{10,11... | collective-permute-start | bytes 417800 | tf_op jit(solution)/shard_map/ppermute | solution.py:206
  33.6 17.3 %collective-permute-start.14 = (bf16[32,2048]{1,0:T(8,128)(2,1)S(1)}, bf16[32,2048]{1,0:T(8,128)(2,1)S(1)}, u32[]{:S(2)}, u32[]{:S(2)}) collective-permute-start(bf16[32,2048]{1,0:T(8,128)(2,1)S(1)} %get-tuple-element.51), channel_id=1, source_target_pairs={{0,4},{1,29},{2,6},{3,31},{4,8},{5,1},{6,10},{7,3},{8,12},{9,5},{1... | collective-permute-start | bytes 393224 | tf_op jit(solution)/shard_map/ppermute | solution.py:203
  33.8 17.2 %collective-permute-start.15 = (bf16[32,2048]{1,0:T(8,128)(2,1)S(1)}, bf16[32,2048]{1,0:T(8,128)(2,1)S(1)}, u32[]{:S(2)}, u32[]{:S(2)}) collective-permute-start(bf16[32,2048]{1,0:T(8,128)(2,1)S(1)} %get-tuple-element.52), channel_id=1, source_target_pairs={{0,28},{1,5},{2,30},{3,7},{4,0},{5,9},{6,2},{7,11},{8,4},{9,13},{1... | collective-permute-start | bytes 393224 | tf_op jit(solution)/shard_map/ppermute | solution.py:203
  37.9 13.1 %collective-permute-start.16 = (bf16[32,2048]{1,0:T(8,128)(2,1)S(1)}, bf16[32,2048]{1,0:T(8,128)(2,1)S(1)}, u32[]{:S(2)}, u32[]{:S(2)}) collective-permute-start(bf16[32,2048]{1,0:T(8,128)(2,1)S(1)} %get-tuple-element.53), channel_id=1, source_target_pairs={{0,2},{1,31},{2,4},{3,1},{4,6},{5,3},{6,8},{7,5},{8,10},{9,7},{10,... | collective-permute-start | bytes 393224 | tf_op jit(solution)/shard_map/ppermute | solution.py:203
  40.6 10.3 %collective-permute-start.17 = (bf16[32,2048]{1,0:T(8,128)(2,1)S(1)}, bf16[32,2048]{1,0:T(8,128)(2,1)S(1)}, u32[]{:S(2)}, u32[]{:S(2)}) collective-permute-start(bf16[32,2048]{1,0:T(8,128)(2,1)S(1)} %get-tuple-element.54), channel_id=1, source_target_pairs={{0,30},{1,3},{2,0},{3,5},{4,2},{5,7},{6,4},{7,9},{8,6},{9,11},{10,... | collective-permute-start | bytes 393224 | tf_op jit(solution)/shard_map/ppermute | solution.py:203
  42.0 9.0 %collective-permute-start.18 = (bf16[16,2048]{1,0:T(8,128)(2,1)S(1)}, bf16[16,2048]{1,0:T(8,128)(2,1)S(1)}, u32[]{:S(2)}, u32[]{:S(2)}) collective-permute-start(bf16[16,2048]{1,0:T(8,128)(2,1)S(1)} %get-tuple-element.56), channel_id=1, source_target_pairs={{0,6},{1,27},{2,8},{3,29},{4,10},{5,31},{6,12},{7,1},{8,14},{9,3},... | collective-permute-start | bytes 196616 | tf_op jit(solution)/shard_map/ppermute | solution.py:203
  51.0 21.4 %collective-permute-start = (bf16[32,2176]{1,0:T(8,128)(2,1)S(1)}, bf16[32,2176]{1,0:T(8,128)(2,1)S(1)}, u32[]{:S(2)}, u32[]{:S(2)}) collective-permute-start(bf16[32,2176]{1,0:T(8,128)(2,1)S(1)} %shard_map.73.refs_0_), channel_id=1, source_target_pairs={{0,1},{1,0},{2,3},{3,2},{4,5},{5,4},{6,7},{7,6},{8,9},{9,8},{10,11... | collective-permute-start | bytes 417800 | tf_op jit(solution)/shard_map/ppermute | solution.py:206
  51.0 3.1 %copy-start = (bf16[1,2048,1792]{2,1,0:T(8,128)(2,1)S(1)}, bf16[1,2048,1792]{2,1,0:T(8,128)(2,1)}, u32[]{:S(2)}) copy-start(bf16[1,2048,1792]{2,1,0:T(8,128)(2,1)} %param.11) | copy-start | bytes 22020100
  54.1 3.1 %copy-start.1 = (bf16[1,2048,1792]{2,1,0:T(8,128)(2,1)S(1)}, bf16[1,2048,1792]{2,1,0:T(8,128)(2,1)}, u32[]{:S(2)}) copy-start(bf16[1,2048,1792]{2,1,0:T(8,128)(2,1)} %param.12) | copy-start | bytes 22020100
  57.2 3.1 %copy-start.2 = (bf16[1,1792,2048]{2,1,0:T(8,128)(2,1)S(1)}, bf16[1,1792,2048]{2,1,0:T(8,128)(2,1)}, u32[]{:S(2)}) copy-start(bf16[1,1792,2048]{2,1,0:T(8,128)(2,1)} %param.13) | copy-start | bytes 22020100
  66.6 17.1 %collective-permute-start.19 = (bf16[32,2048]{1,0:T(8,128)(2,1)S(1)}, bf16[32,2048]{1,0:T(8,128)(2,1)S(1)}, u32[]{:S(2)}, u32[]{:S(2)}) collective-permute-start(bf16[32,2048]{1,0:T(8,128)(2,1)S(1)} %get-tuple-element.57), channel_id=1, source_target_pairs={{0,28},{1,5},{2,30},{3,7},{4,0},{5,9},{6,2},{7,11},{8,4},{9,13},{1... | collective-permute-start | bytes 393224 | tf_op jit(solution)/shard_map/ppermute | solution.py:203
  69.1 17.9 %collective-permute-start.20 = (bf16[32,2048]{1,0:T(8,128)(2,1)S(1)}, bf16[32,2048]{1,0:T(8,128)(2,1)S(1)}, u32[]{:S(2)}, u32[]{:S(2)}) collective-permute-start(bf16[32,2048]{1,0:T(8,128)(2,1)S(1)} %get-tuple-element.58), channel_id=1, source_target_pairs={{0,4},{1,29},{2,6},{3,31},{4,8},{5,1},{6,10},{7,3},{8,12},{9,5},{1... | collective-permute-start | bytes 393224 | tf_op jit(solution)/shard_map/ppermute | solution.py:203
  69.7 17.3 %collective-permute-start.21 = (bf16[32,2048]{1,0:T(8,128)(2,1)S(1)}, bf16[32,2048]{1,0:T(8,128)(2,1)S(1)}, u32[]{:S(2)}, u32[]{:S(2)}) collective-permute-start(bf16[32,2048]{1,0:T(8,128)(2,1)S(1)} %get-tuple-element.59), channel_id=1, source_target_pairs={{0,30},{1,3},{2,0},{3,5},{4,2},{5,7},{6,4},{7,9},{8,6},{9,11},{10,... | collective-permute-start | bytes 393224 | tf_op jit(solution)/shard_map/ppermute | solution.py:203
  72.3 17.9 %collective-permute-start.22 = (bf16[32,2048]{1,0:T(8,128)(2,1)S(1)}, bf16[32,2048]{1,0:T(8,128)(2,1)S(1)}, u32[]{:S(2)}, u32[]{:S(2)}) collective-permute-start(bf16[32,2048]{1,0:T(8,128)(2,1)S(1)} %get-tuple-element.60), channel_id=1, source_target_pairs={{0,2},{1,31},{2,4},{3,1},{4,6},{5,3},{6,8},{7,5},{8,10},{9,7},{10,... | collective-permute-start | bytes 393224 | tf_op jit(solution)/shard_map/ppermute | solution.py:203
  72.3 20.5 %slice-start = ((s8[7340032]{0:T(1024)(128)(4,1)}), s8[4194304]{0:T(1024)(128)(4,1)S(1)}, s32[]{:S(2)}) async-start(s8[7340032]{0:T(1024)(128)(4,1)} %bitcast.9), calls=%async_computation | async-start | bytes 8388608
  72.4 20.5 %slice-start.1 = ((s8[7340032]{0:T(1024)(128)(4,1)}), s8[3145728]{0:T(1024)(128)(4,1)S(1)}, s32[]{:S(2)}) async-start(s8[7340032]{0:T(1024)(128)(4,1)} %bitcast.9), calls=%async_computation.1 | async-start | bytes 6291456
  72.4 10.5 %collective-permute-start.23 = (bf16[16,2048]{1,0:T(8,128)(2,1)S(1)}, bf16[16,2048]{1,0:T(8,128)(2,1)S(1)}, u32[]{:S(2)}, u32[]{:S(2)}) collective-permute-start(bf16[16,2048]{1,0:T(8,128)(2,1)S(1)} %get-tuple-element.62), channel_id=1, source_target_pairs={{0,26},{1,7},{2,28},{3,9},{4,30},{5,11},{6,0},{7,13},{8,2},{9,15},... | collective-permute-start | bytes 196616 | tf_op jit(solution)/shard_map/ppermute | solution.py:203
  82.9 8.0 %collective-permute-start.1 = (bf16[16,2048]{1,0:T(8,128)(2,1)S(1)}, bf16[16,2048]{1,0:T(8,128)(2,1)S(1)}, u32[]{:S(2)}, u32[]{:S(2)}) collective-permute-start(bf16[16,2048]{1,0:T(8,128)(2,1)S(1)} %get-tuple-element.37), channel_id=1, source_target_pairs={{0,4},{1,29},{2,6},{3,31},{4,8},{5,1},{6,10},{7,3},{8,12},{9,5},{1... | collective-permute-start | bytes 196616 | tf_op jit(solution)/shard_map/ppermute | solution.py:203
  83.7 7.1 %collective-permute-start.2 = (bf16[16,2048]{1,0:T(8,128)(2,1)S(1)}, bf16[16,2048]{1,0:T(8,128)(2,1)S(1)}, u32[]{:S(2)}, u32[]{:S(2)}) collective-permute-start(bf16[16,2048]{1,0:T(8,128)(2,1)S(1)} %get-tuple-element.38), channel_id=1, source_target_pairs={{0,28},{1,5},{2,30},{3,7},{4,0},{5,9},{6,2},{7,11},{8,4},{9,13},{1... | collective-permute-start | bytes 196616 | tf_op jit(solution)/shard_map/ppermute | solution.py:203
  87.0 5.8 %collective-permute-start.3 = (bf16[16,2048]{1,0:T(8,128)(2,1)S(1)}, bf16[16,2048]{1,0:T(8,128)(2,1)S(1)}, u32[]{:S(2)}, u32[]{:S(2)}) collective-permute-start(bf16[16,2048]{1,0:T(8,128)(2,1)S(1)} %get-tuple-element.39), channel_id=1, source_target_pairs={{0,2},{1,31},{2,4},{3,1},{4,6},{5,3},{6,8},{7,5},{8,10},{9,7},{10,... | collective-permute-start | bytes 196616 | tf_op jit(solution)/shard_map/ppermute | solution.py:203
  87.0 5.8 %collective-permute-start.4 = (bf16[16,2048]{1,0:T(8,128)(2,1)S(1)}, bf16[16,2048]{1,0:T(8,128)(2,1)S(1)}, u32[]{:S(2)}, u32[]{:S(2)}) collective-permute-start(bf16[16,2048]{1,0:T(8,128)(2,1)S(1)} %get-tuple-element.40), channel_id=1, source_target_pairs={{0,30},{1,3},{2,0},{3,5},{4,2},{5,7},{6,4},{7,9},{8,6},{9,11},{10,... | collective-permute-start | bytes 196616 | tf_op jit(solution)/shard_map/ppermute | solution.py:203
  90.7 20.7 %collective-permute-start.24 = (bf16[64,2048]{1,0:T(8,128)(2,1)S(1)}, bf16[64,2048]{1,0:T(8,128)(2,1)S(1)}, u32[]{:S(2)}, u32[]{:S(2)}) collective-permute-start(bf16[64,2048]{1,0:T(8,128)(2,1)S(1)} %get-tuple-element.66), channel_id=1, source_target_pairs={{0,1},{1,0},{2,3},{3,2},{4,5},{5,4},{6,7},{7,6},{8,9},{9,8},{10,11... | collective-permute-start | bytes 786440 | tf_op jit(solution)/shard_map/ppermute | solution.py:206
  98.3 7.1 %collective-permute-start.5 = (bf16[16,2048]{1,0:T(8,128)(2,1)S(1)}, bf16[16,2048]{1,0:T(8,128)(2,1)S(1)}, u32[]{:S(2)}, u32[]{:S(2)}) collective-permute-start(bf16[16,2048]{1,0:T(8,128)(2,1)S(1)} %get-tuple-element.42), channel_id=1, source_target_pairs={{0,28},{1,5},{2,30},{3,7},{4,0},{5,9},{6,2},{7,11},{8,4},{9,13},{1... | collective-permute-start | bytes 196616 | tf_op jit(solution)/shard_map/ppermute | solution.py:203
  100.0 6.5 %collective-permute-start.6 = (bf16[16,2048]{1,0:T(8,128)(2,1)S(1)}, bf16[16,2048]{1,0:T(8,128)(2,1)S(1)}, u32[]{:S(2)}, u32[]{:S(2)}) collective-permute-start(bf16[16,2048]{1,0:T(8,128)(2,1)S(1)} %get-tuple-element.43), channel_id=1, source_target_pairs={{0,4},{1,29},{2,6},{3,31},{4,8},{5,1},{6,10},{7,3},{8,12},{9,5},{1... | collective-permute-start | bytes 196616 | tf_op jit(solution)/shard_map/ppermute | solution.py:203
  101.3 6.0 %collective-permute-start.7 = (bf16[16,2048]{1,0:T(8,128)(2,1)S(1)}, bf16[16,2048]{1,0:T(8,128)(2,1)S(1)}, u32[]{:S(2)}, u32[]{:S(2)}) collective-permute-start(bf16[16,2048]{1,0:T(8,128)(2,1)S(1)} %get-tuple-element.44), channel_id=1, source_target_pairs={{0,30},{1,3},{2,0},{3,5},{4,2},{5,7},{6,4},{7,9},{8,6},{9,11},{10,... | collective-permute-start | bytes 196616 | tf_op jit(solution)/shard_map/ppermute | solution.py:203
  105.5 5.5 %collective-permute-start.8 = (bf16[16,2048]{1,0:T(8,128)(2,1)S(1)}, bf16[16,2048]{1,0:T(8,128)(2,1)S(1)}, u32[]{:S(2)}, u32[]{:S(2)}) collective-permute-start(bf16[16,2048]{1,0:T(8,128)(2,1)S(1)} %get-tuple-element.45), channel_id=1, source_target_pairs={{0,2},{1,31},{2,4},{3,1},{4,6},{5,3},{6,8},{7,5},{8,10},{9,7},{10,... | collective-permute-start | bytes 196616 | tf_op jit(solution)/shard_map/ppermute | solution.py:203
  111.2 7.1 %collective-permute-start.9 = (bf16[32,2048]{1,0:T(8,128)(2,1)S(1)}, bf16[32,2048]{1,0:T(8,128)(2,1)S(1)}, u32[]{:S(2)}, u32[]{:S(2)}) collective-permute-start(bf16[32,2048]{1,0:T(8,128)(2,1)S(1)} %get-tuple-element.50), channel_id=1, source_target_pairs={{0,1},{1,0},{2,3},{3,2},{4,5},{5,4},{6,7},{7,6},{8,9},{9,8},{10,11... | collective-permute-start | bytes 393224 | tf_op jit(solution)/shard_map/ppermute | solution.py:206
  111.4 20.4 %collective-permute-start.25 = (bf16[32,2048]{1,0:T(8,128)(2,1)S(1)}, bf16[32,2048]{1,0:T(8,128)(2,1)S(1)}, u32[]{:S(2)}, u32[]{:S(2)}) collective-permute-start(bf16[32,2048]{1,0:T(8,128)(2,1)S(1)} %get-tuple-element.67), channel_id=1, source_target_pairs={{0,22},{1,11},{2,24},{3,13},{4,26},{5,15},{6,28},{7,17},{8,30},{9,... | collective-permute-start | bytes 393224 | tf_op jit(solution)/shard_map/ppermute | solution.py:203
  114.3 17.6 %collective-permute-start.26 = (bf16[32,2048]{1,0:T(8,128)(2,1)S(1)}, bf16[32,2048]{1,0:T(8,128)(2,1)S(1)}, u32[]{:S(2)}, u32[]{:S(2)}) collective-permute-start(bf16[32,2048]{1,0:T(8,128)(2,1)S(1)} %get-tuple-element.68), channel_id=1, source_target_pairs={{0,10},{1,23},{2,12},{3,25},{4,14},{5,27},{6,16},{7,29},{8,18},{9,... | collective-permute-start | bytes 393224 | tf_op jit(solution)/shard_map/ppermute | solution.py:203

commit v6 on v5

--- a/solution.py
+++ b/solution.py
@@ -10,6 +10,7 @@
 
 HOP = 5
 NEAR = (2, -2, 1, -1, 0)
+EARLY = 2
 GRP_EP = ("grp", "z", "c")
 META = 128
 LIMIT = 16 << 20
@@ -124,8 +125,9 @@
         at += b.shape[0]
 
 
-def experts(tile, count, *refs):
-    blocks, (gate_ref, up_ref, down_ref), refs = refs[:count], refs[count : count + 3], refs[count + 3 :]
+def experts(tile, count, held, *refs):
+    blocks, carried, refs = refs[:count], refs[count : count + held], refs[count + held :]
+    (gate_ref, up_ref, down_ref), refs = refs[:3], refs[3:]
     outs, (x_ref, total_ref) = refs[:count], refs[count:]
     gather(blocks, x_ref)
     hidden = gate_ref.shape[1]
@@ -143,34 +145,42 @@
         total_ref[...] += jnp.dot(active, down_ref[cols, :], preferred_element_type=jnp.float32)
 
     at = 0
-    for o in outs:
-        o[...] = total_ref[at : at + o.shape[0], :].astype(jnp.bfloat16)
-        at += o.shape[0]
-
-
-def weighted(blocks, high_ref, low_ref, x_ref):
-    gather(blocks, x_ref)
+    for i, (b, o) in enumerate(zip(blocks, outs)):
+        o[: b.shape[0]] = total_ref[at : at + b.shape[0], :].astype(jnp.bfloat16)
+        if EARLY <= i < EARLY + held:
+            o[b.shape[0] :] = carried[i - EARLY][...]
+        at += b.shape[0]
+
+
+def weigh(*refs):
+    early, blocks, refs = refs[:EARLY], refs[EARLY : EARLY + 6], refs[EARLY + 6 :]
+    (high_ref, low_ref, near_high, near_low), refs = refs[:4], refs[4:]
+    far_mine, far_other, mine, other, x_ref, near_ref = refs
+    at, near_at, small = 0, 0, early[0].shape[0]
+    for e in early:
+        near_ref[near_at : near_at + small, :] = e[...]
+        near_at += small
+    for i, b in enumerate(blocks):
+        both = EARLY <= i < len(NEAR)
+        size = b.shape[0] - (small if both else 0)
+        x_ref[at : at + size, :] = b[:size]
+        at += size
+        if both:
+            near_ref[near_at : near_at + small, :] = b[size:]
+            near_at += small
     x = x_ref[...]
     total = jnp.dot(high_ref[...], x, preferred_element_type=jnp.float32)
-    return total + jnp.dot(low_ref[...], x, preferred_element_type=jnp.float32)
-
-
-def weigh_near(*refs):
-    mine, other, x_ref = refs[-3:]
-    total = weighted(refs[:-5], *refs[-5:-3], x_ref)
+    total += jnp.dot(low_ref[...], x, preferred_element_type=jnp.float32)
     rows = mine.shape[0]
+    far_mine[:rows] = total[:rows]
+    far_mine[rows:] = total[2 * rows : 3 * rows]
+    far_other[:rows] = total[3 * rows :].astype(jnp.bfloat16)
+    far_other[rows:] = total[rows : 2 * rows].astype(jnp.bfloat16)
+    x = near_ref[...]
+    total = jnp.dot(near_high[...], x, preferred_element_type=jnp.float32)
+    total += jnp.dot(near_low[...], x, preferred_element_type=jnp.float32)
     mine[...] = total[:rows]
     other[...] = total[rows:].astype(jnp.bfloat16)
-
-
-def weigh_far(*refs):
-    mine, other, x_ref = refs[-3:]
-    total = weighted(refs[:-5], *refs[-5:-3], x_ref)
-    rows = mine.shape[0] // 2
-    mine[:rows] = total[:rows]
-    mine[rows:] = total[2 * rows : 3 * rows]
-    other[:rows] = total[3 * rows :].astype(jnp.bfloat16)
-    other[rows:] = total[rows : 2 * rows].astype(jnp.bfloat16)
 
 
 def join(mine, other, one, two):
@@ -239,35 +249,38 @@
         )(place, *sources)
         return [shift(b, d) if d else b for b, d in zip(blocks, steps)], (w_high, w_low)
 
-    def run(blocks):
+    def run(blocks, carried=()):
         slots = sum(b.shape[0] for b in blocks)
+        sizes = [b.shape[0] for b in blocks]
+        for i, b in enumerate(carried):
+            sizes[EARLY + i] += b.shape[0]
         experts_of = call(
-            functools.partial(experts, 256, len(blocks)),
-            [bf16(*b.shape) for b in blocks],
-            len(blocks) + 3,
+            functools.partial(experts, 256, len(blocks), len(carried)),
+            [bf16(n, width) for n in sizes],
+            len(blocks) + len(carried) + 3,
             scratch=[pltpu.VMEM((slots, width), jnp.bfloat16), pltpu.VMEM((slots, width), jnp.float32)],
             flops=6 * slots * width * hidden,
         )
-        return experts_of(*blocks, w_gate[0], w_up[0], w_down[0])
-
-    def weigh(body, blocks, weights, rows):
-        back = [shift(b, -d) if d else b for b, d in zip(blocks, steps)]
-        slots = sum(b.shape[0] for b in blocks)
-        sums_of = call(
-            body,
-            [f32(rows, width), bf16(rows, width)],
-            len(back) + 2,
-            scratch=[pltpu.VMEM((slots, width), jnp.bfloat16)],
-        )
-        return sums_of(*back, *weights)
+        return experts_of(*blocks, *carried, w_gate[0], w_up[0], w_down[0])
+
+    def back(blocks):
+        return [shift(b, -d) if d else b for b, d in zip(blocks, steps)]
 
     heavy = 24 * 256 * width * hidden
     near, near_weights = hand((own, own2), [2 * cap] * 5, heavy)
     far, far_weights = hand((low, low2, high, high2), [4 * cap] * 5 + [2 * cap], 1 << 28)
     near = run(near)
-    far = run(far)
-    mine, other = weigh(weigh_near, near, near_weights, rows)
-    far_mine, far_other = weigh(weigh_far, far, far_weights, 2 * rows)
+    early = back(near[:EARLY])
+    late = back(run(far, near[EARLY:]))
+    far_mine, far_other, mine, other = call(
+        weigh,
+        [f32(2 * rows, width), bf16(2 * rows, width), f32(rows, width), bf16(rows, width)],
+        EARLY + 10,
+        scratch=[
+            pltpu.VMEM((far_weights[0].shape[1], width), jnp.bfloat16),
+            pltpu.VMEM((near_weights[0].shape[1], width), jnp.bfloat16),
+        ],
+    )(*early, *late, *far_weights, *near_weights)
     one, two = call(join, [bf16(rows, width)] * 2, 2)(far_mine, swap(far_other))
     return call(finish, bf16(rows, width), 4)(mine, swap(other), shift(one, -HOP), shift(two, HOP))
 

time: 133 us -> 110 us (0.83)
  waiting for transfers between devices: 51 us -> 39.6 us
  local copies, waits for them, and re-layouts: 9.25 us -> 0.03 us
  starting transfers between devices: 55.2 us -> 52 us
    ppermute x22 -> x20, waiting for transfers between devices: 50 us -> 38.5 us  [shift(): return lax.ppermute(x, ('z', 'c'), pairs)]
    unnamed x10 -> x12, local copies, waits for them, and re-layouts: 9.25 us -> 0.03 us
    ppermute x22 -> x20, starting transfers between devices: 54.4 us -> 50.9 us  [shift(): return lax.ppermute(x, ('z', 'c'), pairs)]
    pallas_call x4 -> x3, Pallas kernels: 12.6 us -> 12.5 us  [the longest x2 11.9 us: run(): return experts_of(*blocks, *carried, w_gate[0], w_up[0], w_down[0])]
  transfers between devices with their start and end apart: 27 -> 25, of which waited for: 10 -> 8; matrix products, arithmetic and copies ran while one was open for 0% -> 0% of each run, Pallas kernels for 10% -> 13%
where the time goes in v6:
time: 110 us; the launch traced here: 109 us
  starting transfers between devices  52 us (47%)
  waiting for transfers between devices  39.6 us (36%)
  Pallas kernels  16.8 us (15%)
    ppermute x20, starting transfers between devices, shift(): return lax.ppermute(x, ('z', 'c'), pairs)  50.9 us
    ppermute x20, waiting for transfers between devices, shift(): return lax.ppermute(x, ('z', 'c'), pairs)  38.5 us
    pallas_call x2, Pallas kernels, run(): return experts_of(*blocks, *carried, w_gate[0], w_up[0], w_down[0])  11.9 us
  transfers between devices with their start and end apart: 25, of which 8 were waited for; matrix products, arithmetic and copies ran while one was open for 0% of the time, Pallas kernels for 13%

profile of v6, /device:TPU:86, one launch (start us, length us, event | category | flops | bytes accessed | tf_op | source)
XLA Modules:
  0.0 108.7 jit_solution(15013644605746720676)
XLA Ops:
  0.0 1.5 %shard_map.73.refs_0_ = bf16[32,2176]{1,0:T(8,128)(2,1)S(1)} custom-call(bf16[32,2048]{1,0:T(8,128)(2,1)} %tok_hbm.1, f32[1,2048]{1,0:T(1,128)} %bitcast.20, s32[4,32]{1,0:T(4,128)} %bitcast.21, f32[4,32]{1,0:T(4,128)} %bitcast.22), custom_call_target="tpu_custom_call" | custom-call | flops 1048576 | bytes 1048576 | tf_op jit(solution)/shard_map/pallas_call | solution.py:219
  1.5 14.8 %collective-permute-start.8 = (bf16[32,2176]{1,0:T(8,128)(2,1)S(1)}, bf16[32,2176]{1,0:T(8,128)(2,1)S(1)}, u32[]{:S(2)}, u32[]{:S(2)}) collective-permute-start(bf16[32,2176]{1,0:T(8,128)(2,1)S(1)} %shard_map.73.refs_0_), channel_id=1, source_target_pairs={{0,22},{1,11},{2,24},{3,13},{4,26},{5,15},{6,28},{7,17},{8,30},{9,... | collective-permute-start | bytes 417800 | tf_op jit(solution)/shard_map/ppermute | solution.py:213
  16.3 0.0 collective-permute-start.7
  16.3 0.0 collective-permute-start
  16.3 0.0 slice-start.2
  16.3 0.0 slice-start.4
  16.4 0.1 pad_add_fusion.place_ref
  16.4 14.5 %collective-permute-done.8.refs_2_ = bf16[32,2176]{1,0:T(8,128)(2,1)S(1)} collective-permute-done((bf16[32,2176]{1,0:T(8,128)(2,1)S(1)}, bf16[32,2176]{1,0:T(8,128)(2,1)S(1)}, u32[]{:S(2)}, u32[]{:S(2)}) %collective-permute-start.8) | collective-permute-done | bytes 139296 | tf_op jit(solution)/shard_map/ppermute | solution.py:213
  31.0 0.0 collective-permute-start.9
  31.0 0.0 collective-permute-done.7.refs_0_
  31.0 0.5 collective-permute-start.10
  31.5 0.0 collective-permute-done.refs_1_
  31.5 0.9 shard_map.74
  32.4 0.1 collective-permute-start.1
  32.5 4.1 %collective-permute-start.2 = (bf16[16,2048]{1,0:T(8,128)(2,1)S(1)}, bf16[16,2048]{1,0:T(8,128)(2,1)S(1)}, u32[]{:S(2)}, u32[]{:S(2)}) collective-permute-start(bf16[16,2048]{1,0:T(8,128)(2,1)S(1)} %get-tuple-element.38), channel_id=1, source_target_pairs={{0,28},{1,5},{2,30},{3,7},{4,0},{5,9},{6,2},{7,11},{8,4},{9,13},{1... | collective-permute-start | bytes 196616 | tf_op jit(solution)/shard_map/ppermute | solution.py:213
  36.6 2.4 %collective-permute-start.3 = (bf16[16,2048]{1,0:T(8,128)(2,1)S(1)}, bf16[16,2048]{1,0:T(8,128)(2,1)S(1)}, u32[]{:S(2)}, u32[]{:S(2)}) collective-permute-start(bf16[16,2048]{1,0:T(8,128)(2,1)S(1)} %get-tuple-element.39), channel_id=1, source_target_pairs={{0,2},{1,31},{2,4},{3,1},{4,6},{5,3},{6,8},{7,5},{8,10},{9,7},{10,... | collective-permute-start | bytes 196616 | tf_op jit(solution)/shard_map/ppermute | solution.py:213
  39.1 0.0 collective-permute-done.9.refs_1_
  39.1 1.3 %collective-permute-start.4 = (bf16[16,2048]{1,0:T(8,128)(2,1)S(1)}, bf16[16,2048]{1,0:T(8,128)(2,1)S(1)}, u32[]{:S(2)}, u32[]{:S(2)}) collective-permute-start(bf16[16,2048]{1,0:T(8,128)(2,1)S(1)} %get-tuple-element.40), channel_id=1, source_target_pairs={{0,30},{1,3},{2,0},{3,5},{4,2},{5,7},{6,4},{7,9},{8,6},{9,11},{10,... | collective-permute-start | bytes 196616 | tf_op jit(solution)/shard_map/ppermute | solution.py:213
  40.4 0.0 collective-permute-done.10.refs_3_
  40.4 1.1 %shard_map.76 = (bf16[32,2048]{1,0:T(8,128)(2,1)S(1)}, bf16[32,2048]{1,0:T(8,128)(2,1)S(1)}, bf16[32,2048]{1,0:T(8,128)(2,1)S(1)}, bf16[32,2048]{1,0:T(8,128)(2,...) custom-call(s32[2]{0:T(128)S(1)} %pad_add_fusion.place_ref, ...), custom_call_target="tpu_custom_call" | custom-call | flops 268435456 | bytes 1048576 | tf_op jit(solution)/shard_map/pallas_call | solution.py:242
  41.6 1.0 collective-permute-start.15
  42.6 0.0 collective-permute-done.1.refs_0_
  42.6 1.5 %collective-permute-start.11 = (bf16[32,2048]{1,0:T(8,128)(2,1)S(1)}, bf16[32,2048]{1,0:T(8,128)(2,1)S(1)}, u32[]{:S(2)}, u32[]{:S(2)}) collective-permute-start(bf16[32,2048]{1,0:T(8,128)(2,1)S(1)} %get-tuple-element.44), channel_id=1, source_target_pairs={{0,4},{1,29},{2,6},{3,31},{4,8},{5,1},{6,10},{7,3},{8,12},{9,5},{1... | collective-permute-start | bytes 393224 | tf_op jit(solution)/shard_map/ppermute | solution.py:213
  44.0 0.0 collective-permute-done.2.refs_1_
  44.0 2.7 %collective-permute-start.12 = (bf16[32,2048]{1,0:T(8,128)(2,1)S(1)}, bf16[32,2048]{1,0:T(8,128)(2,1)S(1)}, u32[]{:S(2)}, u32[]{:S(2)}) collective-permute-start(bf16[32,2048]{1,0:T(8,128)(2,1)S(1)} %get-tuple-element.45), channel_id=1, source_target_pairs={{0,28},{1,5},{2,30},{3,7},{4,0},{5,9},{6,2},{7,11},{8,4},{9,13},{1... | collective-permute-start | bytes 393224 | tf_op jit(solution)/shard_map/ppermute | solution.py:213
  46.7 0.0 collective-permute-done.3.refs_2_
  46.7 3.2 %collective-permute-start.13 = (bf16[32,2048]{1,0:T(8,128)(2,1)S(1)}, bf16[32,2048]{1,0:T(8,128)(2,1)S(1)}, u32[]{:S(2)}, u32[]{:S(2)}) collective-permute-start(bf16[32,2048]{1,0:T(8,128)(2,1)S(1)} %get-tuple-element.46), channel_id=1, source_target_pairs={{0,2},{1,31},{2,4},{3,1},{4,6},{5,3},{6,8},{7,5},{8,10},{9,7},{10,... | collective-permute-start | bytes 393224 | tf_op jit(solution)/shard_map/ppermute | solution.py:213
  49.9 0.0 collective-permute-done.4.refs_3_
  50.0 0.0 collective-permute-start.14
  50.0 0.0 slice-done
  50.0 0.0 slice-done.2
  50.0 0.0 slice-done.4
  50.0 0.0 slice-done.1
  50.0 5.5 %shard_map.75 = (bf16[16,2048]{1,0:T(8,128)(2,1)S(1)}, bf16[16,2048]{1,0:T(8,128)(2,1)S(1)}, bf16[16,2048]{1,0:T(8,128)(2,1)S(1)}, bf16[16,2048]{1,0:T(8,128)(2,1)S(1)}, bf16[16,2048]{1,0:T(8,128)(2,1)S(1)}) custom-call(bf16[16,2048]{1,0:T(8,128)(2,1)S(1)} %collective-permute-done.1.refs_0_, bf16[16,2048]{1,0:T(8,128)(2,1)S(1)} %collective-permute-done.2.refs_1_, ...), custom_call_target="tpu_custom_call" | custom-call | flops 1761607680 | bytes 1048576 | tf_op jit(solution)/shard_map/pallas_call | solution.py:264
  55.5 0.0 collective-permute-done.15.refs_5_
  55.5 1.7 %collective-permute-start.5 = (bf16[16,2048]{1,0:T(8,128)(2,1)S(1)}, bf16[16,2048]{1,0:T(8,128)(2,1)S(1)}, u32[]{:S(2)}, u32[]{:S(2)}) collective-permute-start(bf16[16,2048]{1,0:T(8,128)(2,1)S(1)} %get-tuple-element.42), channel_id=1, source_target_pairs={{0,28},{1,5},{2,30},{3,7},{4,0},{5,9},{6,2},{7,11},{8,4},{9,13},{1... | collective-permute-start | bytes 196616 | tf_op jit(solution)/shard_map/ppermute | solution.py:213
  57.2 0.0 collective-permute-done.11.refs_0_
  57.2 0.0 collective-permute-done.12.refs_1_
  57.2 0.8 collective-permute-done.13.refs_2_
  58.0 0.9 collective-permute-done.14.refs_3_
  58.9 6.4 %shard_map.77 = (bf16[32,2048]{1,0:T(8,128)(2,1)S(1)}, bf16[32,2048]{1,0:T(8,128)(2,1)S(1)}, bf16[48,2048]{1,0:T(8,128)(2,1)S(1)}, bf16[48,2048]{1,0:T(8,128)(2,...) custom-call(bf16[32,2048]{1,0:T(8,128)(2,1)S(1)} %collective-permute-done.11.refs_0_, ...), custom_call_target="tpu_custom_call" | custom-call | flops 3875536896 | bytes 1048576 | tf_op jit(solution)/shard_map/pallas_call | solution.py:264
  65.3 1.6 %collective-permute-start.18 = (bf16[48,2048]{1,0:T(8,128)(2,1)S(1)}, bf16[48,2048]{1,0:T(8,128)(2,1)S(1)}, u32[]{:S(2)}, u32[]{:S(2)}) collective-permute-start(bf16[48,2048]{1,0:T(8,128)(2,1)S(1)} %get-tuple-element.55), channel_id=1, source_target_pairs={{0,30},{1,3},{2,0},{3,5},{4,2},{5,7},{6,4},{7,9},{8,6},{9,11},{10,... | collective-permute-start | bytes 589832 | tf_op jit(solution)/shard_map/ppermute | solution.py:213
  66.9 0.6 collective-permute-start.19
  67.4 0.0 collective-permute-start.6
  67.4 4.1 %collective-permute-start.16 = (bf16[32,2048]{1,0:T(8,128)(2,1)S(1)}, bf16[32,2048]{1,0:T(8,128)(2,1)S(1)}, u32[]{:S(2)}, u32[]{:S(2)}) collective-permute-start(bf16[32,2048]{1,0:T(8,128)(2,1)S(1)} %get-tuple-element.53), channel_id=1, source_target_pairs={{0,28},{1,5},{2,30},{3,7},{4,0},{5,9},{6,2},{7,11},{8,4},{9,13},{1... | collective-permute-start | bytes 393224 | tf_op jit(solution)/shard_map/ppermute | solution.py:213
  71.6 0.0 collective-permute-done.5.refs_0_
  71.6 0.0 collective-permute-start.17
  71.6 5.8 %collective-permute-done.6.refs_1_ = bf16[16,2048]{1,0:T(8,128)(2,1)S(1)} collective-permute-done((bf16[16,2048]{1,0:T(8,128)(2,1)S(1)}, bf16[16,2048]{1,0:T(8,128)(2,1)S(1)}, u32[]{:S(2)}, u32[]{:S(2)}) %collective-permute-start.6) | collective-permute-done | bytes 65568 | tf_op jit(solution)/shard_map/ppermute | solution.py:213
  77.3 4.8 %collective-permute-start.20 = (bf16[16,2048]{1,0:T(8,128)(2,1)S(1)}, bf16[16,2048]{1,0:T(8,128)(2,1)S(1)}, u32[]{:S(2)}, u32[]{:S(2)}) collective-permute-start(bf16[16,2048]{1,0:T(8,128)(2,1)S(1)} %get-tuple-element.58), channel_id=1, source_target_pairs={{0,26},{1,7},{2,28},{3,9},{4,30},{5,11},{6,0},{7,13},{8,2},{9,15},... | collective-permute-start | bytes 196616 | tf_op jit(solution)/shard_map/ppermute | solution.py:213
  82.1 1.9 %collective-permute-done.20.refs_7_ = bf16[16,2048]{1,0:T(8,128)(2,1)S(1)} collective-permute-done((bf16[16,2048]{1,0:T(8,128)(2,1)S(1)}, bf16[16,2048]{1,0:T(8,128)(2,1)S(1)}, u32[]{:S(2)}, u32[]{:S(2)}) %collective-permute-start.20) | collective-permute-done | bytes 65568 | tf_op jit(solution)/shard_map/ppermute | solution.py:213
  84.1 0.0 collective-permute-done.16.refs_2_
  84.1 0.0 collective-permute-done.17.refs_3_
  84.1 0.0 collective-permute-done.18.refs_4_
  84.1 0.0 collective-permute-done.19.refs_5_
  84.1 0.6 shard_map.78
  84.7 0.1 collective-permute-start.22
  84.8 0.5 collective-permute-start.21
  85.3 1.0 collective-permute-done.22.other
  86.4 5.6 %collective-permute-start.23 = (bf16[32,2048]{1,0:T(8,128)(2,1)S(1)}, bf16[32,2048]{1,0:T(8,128)(2,1)S(1)}, u32[]{:S(2)}, u32[]{:S(2)}) collective-permute-start(bf16[32,2048]{1,0:T(8,128)(2,1)S(1)} %get-tuple-element.67), channel_id=1, source_target_pairs={{0,22},{1,11},{2,24},{3,13},{4,26},{5,15},{6,28},{7,17},{8,30},{9,... | collective-permute-start | bytes 393224 | tf_op jit(solution)/shard_map/ppermute | solution.py:213
  91.9 1.4 %collective-permute-start.24 = (bf16[32,2048]{1,0:T(8,128)(2,1)S(1)}, bf16[32,2048]{1,0:T(8,128)(2,1)S(1)}, u32[]{:S(2)}, u32[]{:S(2)}) collective-permute-start(bf16[32,2048]{1,0:T(8,128)(2,1)S(1)} %get-tuple-element.68), channel_id=1, source_target_pairs={{0,10},{1,23},{2,12},{3,25},{4,14},{5,27},{6,16},{7,29},{8,18},{9,... | collective-permute-start | bytes 393224 | tf_op jit(solution)/shard_map/ppermute | solution.py:213
  93.3 0.0 collective-permute-done.21.other
  93.3 3.2 %collective-permute-done.23.one = bf16[32,2048]{1,0:T(8,128)(2,1)S(1)} collective-permute-done((bf16[32,2048]{1,0:T(8,128)(2,1)S(1)}, bf16[32,2048]{1,0:T(8,128)(2,1)S(1)}, u32[]{:S(2)}, u32[]{:S(2)}) %collective-permute-start.23) | collective-permute-done | bytes 131104 | tf_op jit(solution)/shard_map/ppermute | solution.py:213
  96.5 11.5 %collective-permute-done.24.two = bf16[32,2048]{1,0:T(8,128)(2,1)S(1)} collective-permute-done((bf16[32,2048]{1,0:T(8,128)(2,1)S(1)}, bf16[32,2048]{1,0:T(8,128)(2,1)S(1)}, u32[]{:S(2)}, u32[]{:S(2)}) %collective-permute-start.24) | collective-permute-done | bytes 131104 | tf_op jit(solution)/shard_map/ppermute | solution.py:213
  108.0 0.7 shard_map.80
  (10 shorter events, 0.1 us)
Async XLA Ops:
  1.5 29.5 %collective-permute-start.8 = (bf16[32,2176]{1,0:T(8,128)(2,1)S(1)}, bf16[32,2176]{1,0:T(8,128)(2,1)S(1)}, u32[]{:S(2)}, u32[]{:S(2)}) collective-permute-start(bf16[32,2176]{1,0:T(8,128)(2,1)S(1)} %shard_map.73.refs_0_), channel_id=1, source_target_pairs={{0,22},{1,11},{2,24},{3,13},{4,26},{5,15},{6,28},{7,17},{8,30},{9,... | collective-permute-start | bytes 417800 | tf_op jit(solution)/shard_map/ppermute | solution.py:213
  16.3 14.7 %collective-permute-start.7 = (bf16[32,2176]{1,0:T(8,128)(2,1)S(1)}, bf16[32,2176]{1,0:T(8,128)(2,1)S(1)}, u32[]{:S(2)}, u32[]{:S(2)}) collective-permute-start(bf16[32,2176]{1,0:T(8,128)(2,1)S(1)} %shard_map.73.refs_0_), channel_id=1, source_target_pairs={{0,10},{1,23},{2,12},{3,25},{4,14},{5,27},{6,16},{7,29},{8,18},{9,... | collective-permute-start | bytes 417800 | tf_op jit(solution)/shard_map/ppermute | solution.py:213
  16.3 15.2 %collective-permute-start = (bf16[32,2176]{1,0:T(8,128)(2,1)S(1)}, bf16[32,2176]{1,0:T(8,128)(2,1)S(1)}, u32[]{:S(2)}, u32[]{:S(2)}) collective-permute-start(bf16[32,2176]{1,0:T(8,128)(2,1)S(1)} %shard_map.73.refs_0_), channel_id=1, source_target_pairs={{0,1},{1,0},{2,3},{3,2},{4,5},{5,4},{6,7},{7,6},{8,9},{9,8},{10,11... | collective-permute-start | bytes 417800 | tf_op jit(solution)/shard_map/ppermute | solution.py:216
  16.3 33.6 %slice-start = ((s8[7340032]{0:T(1024)(128)(4,1)}), s8[4194304]{0:T(1024)(128)(4,1)S(1)}, s32[]{:S(2)}) async-start(s8[7340032]{0:T(1024)(128)(4,1)} %bitcast.8), calls=%async_computation | async-start | bytes 8388608
  16.3 33.6 %slice-start.2 = ((s8[7340032]{0:T(1024)(128)(4,1)}), s8[4194304]{0:T(1024)(128)(4,1)S(1)}, s32[]{:S(2)}) async-start(s8[7340032]{0:T(1024)(128)(4,1)} %bitcast.12), calls=%async_computation.2 | async-start | bytes 8388608
  16.3 33.6 %slice-start.4 = ((s8[7340032]{0:T(1024)(128)(4,1)}), s8[4194304]{0:T(1024)(128)(4,1)S(1)}, s32[]{:S(2)}) async-start(s8[7340032]{0:T(1024)(128)(4,1)} %bitcast.16), calls=%async_computation.4 | async-start | bytes 8388608
  16.4 33.6 %slice-start.1 = ((s8[7340032]{0:T(1024)(128)(4,1)}), s8[3145728]{0:T(1024)(128)(4,1)S(1)}, s32[]{:S(2)}) async-start(s8[7340032]{0:T(1024)(128)(4,1)} %bitcast.8), calls=%async_computation.1 | async-start | bytes 6291456
  16.4 33.6 %slice-start.3 = ((s8[7340032]{0:T(1024)(128)(4,1)}), s8[3145728]{0:T(1024)(128)(4,1)S(1)}, s32[]{:S(2)}) async-start(s8[7340032]{0:T(1024)(128)(4,1)} %bitcast.12), calls=%async_computation.3 | async-start | bytes 6291456
  16.4 33.6 %slice-start.5 = ((s8[7340032]{0:T(1024)(128)(4,1)}), s8[3145728]{0:T(1024)(128)(4,1)S(1)}, s32[]{:S(2)}) async-start(s8[7340032]{0:T(1024)(128)(4,1)} %bitcast.16), calls=%async_computation.5 | async-start | bytes 6291456
  31.0 8.1 %collective-permute-start.9 = (bf16[32,2176]{1,0:T(8,128)(2,1)S(1)}, bf16[32,2176]{1,0:T(8,128)(2,1)S(1)}, u32[]{:S(2)}, u32[]{:S(2)}) collective-permute-start(bf16[32,2176]{1,0:T(8,128)(2,1)S(1)} %collective-permute-done.8.refs_2_), channel_id=1, source_target_pairs={{0,1},{1,0},{2,3},{3,2},{4,5},{5,4},{6,7},{7,6},{8,9},{9,8},{10,11... | collective-permute-start | bytes 417800 | tf_op jit(solution)/shard_map/ppermute | solution.py:216
  31.0 9.5 %collective-permute-start.10 = (bf16[32,2176]{1,0:T(8,128)(2,1)S(1)}, bf16[32,2176]{1,0:T(8,128)(2,1)S(1)}, u32[]{:S(2)}, u32[]{:S(2)}) collective-permute-start(bf16[32,2176]{1,0:T(8,128)(2,1)S(1)} %collective-permute-done.7.refs_0_), channel_id=1, source_target_pairs={{0,1},{1,0},{2,3},{3,2},{4,5},{5,4},{6,7},{7,6},{8,9},{9,8},{10,11... | collective-permute-start | bytes 417800 | tf_op jit(solution)/shard_map/ppermute | solution.py:216
  32.4 10.2 %collective-permute-start.1 = (bf16[16,2048]{1,0:T(8,128)(2,1)S(1)}, bf16[16,2048]{1,0:T(8,128)(2,1)S(1)}, u32[]{:S(2)}, u32[]{:S(2)}) collective-permute-start(bf16[16,2048]{1,0:T(8,128)(2,1)S(1)} %get-tuple-element.37), channel_id=1, source_target_pairs={{0,4},{1,29},{2,6},{3,31},{4,8},{5,1},{6,10},{7,3},{8,12},{9,5},{1... | collective-permute-start | bytes 196616 | tf_op jit(solution)/shard_map/ppermute | solution.py:213
  32.5 11.5 %collective-permute-start.2 = (bf16[16,2048]{1,0:T(8,128)(2,1)S(1)}, bf16[16,2048]{1,0:T(8,128)(2,1)S(1)}, u32[]{:S(2)}, u32[]{:S(2)}) collective-permute-start(bf16[16,2048]{1,0:T(8,128)(2,1)S(1)} %get-tuple-element.38), channel_id=1, source_target_pairs={{0,28},{1,5},{2,30},{3,7},{4,0},{5,9},{6,2},{7,11},{8,4},{9,13},{1... | collective-permute-start | bytes 196616 | tf_op jit(solution)/shard_map/ppermute | solution.py:213
  36.6 10.1 %collective-permute-start.3 = (bf16[16,2048]{1,0:T(8,128)(2,1)S(1)}, bf16[16,2048]{1,0:T(8,128)(2,1)S(1)}, u32[]{:S(2)}, u32[]{:S(2)}) collective-permute-start(bf16[16,2048]{1,0:T(8,128)(2,1)S(1)} %get-tuple-element.39), channel_id=1, source_target_pairs={{0,2},{1,31},{2,4},{3,1},{4,6},{5,3},{6,8},{7,5},{8,10},{9,7},{10,... | collective-permute-start | bytes 196616 | tf_op jit(solution)/shard_map/ppermute | solution.py:213
  39.1 10.9 %collective-permute-start.4 = (bf16[16,2048]{1,0:T(8,128)(2,1)S(1)}, bf16[16,2048]{1,0:T(8,128)(2,1)S(1)}, u32[]{:S(2)}, u32[]{:S(2)}) collective-permute-start(bf16[16,2048]{1,0:T(8,128)(2,1)S(1)} %get-tuple-element.40), channel_id=1, source_target_pairs={{0,30},{1,3},{2,0},{3,5},{4,2},{5,7},{6,4},{7,9},{8,6},{9,11},{10,... | collective-permute-start | bytes 196616 | tf_op jit(solution)/shard_map/ppermute | solution.py:213
  41.6 14.0 %collective-permute-start.15 = (bf16[16,2048]{1,0:T(8,128)(2,1)S(1)}, bf16[16,2048]{1,0:T(8,128)(2,1)S(1)}, u32[]{:S(2)}, u32[]{:S(2)}) collective-permute-start(bf16[16,2048]{1,0:T(8,128)(2,1)S(1)} %get-tuple-element.49), channel_id=1, source_target_pairs={{0,6},{1,27},{2,8},{3,29},{4,10},{5,31},{6,12},{7,1},{8,14},{9,3},... | collective-permute-start | bytes 196616 | tf_op jit(solution)/shard_map/ppermute | solution.py:213
  42.6 14.6 %collective-permute-start.11 = (bf16[32,2048]{1,0:T(8,128)(2,1)S(1)}, bf16[32,2048]{1,0:T(8,128)(2,1)S(1)}, u32[]{:S(2)}, u32[]{:S(2)}) collective-permute-start(bf16[32,2048]{1,0:T(8,128)(2,1)S(1)} %get-tuple-element.44), channel_id=1, source_target_pairs={{0,4},{1,29},{2,6},{3,31},{4,8},{5,1},{6,10},{7,3},{8,12},{9,5},{1... | collective-permute-start | bytes 393224 | tf_op jit(solution)/shard_map/ppermute | solution.py:213
  44.0 13.2 %collective-permute-start.12 = (bf16[32,2048]{1,0:T(8,128)(2,1)S(1)}, bf16[32,2048]{1,0:T(8,128)(2,1)S(1)}, u32[]{:S(2)}, u32[]{:S(2)}) collective-permute-start(bf16[32,2048]{1,0:T(8,128)(2,1)S(1)} %get-tuple-element.45), channel_id=1, source_target_pairs={{0,28},{1,5},{2,30},{3,7},{4,0},{5,9},{6,2},{7,11},{8,4},{9,13},{1... | collective-permute-start | bytes 393224 | tf_op jit(solution)/shard_map/ppermute | solution.py:213
  46.7 11.3 %collective-permute-start.13 = (bf16[32,2048]{1,0:T(8,128)(2,1)S(1)}, bf16[32,2048]{1,0:T(8,128)(2,1)S(1)}, u32[]{:S(2)}, u32[]{:S(2)}) collective-permute-start(bf16[32,2048]{1,0:T(8,128)(2,1)S(1)} %get-tuple-element.46), channel_id=1, source_target_pairs={{0,2},{1,31},{2,4},{3,1},{4,6},{5,3},{6,8},{7,5},{8,10},{9,7},{10,... | collective-permute-start | bytes 393224 | tf_op jit(solution)/shard_map/ppermute | solution.py:213
  50.0 8.9 %collective-permute-start.14 = (bf16[32,2048]{1,0:T(8,128)(2,1)S(1)}, bf16[32,2048]{1,0:T(8,128)(2,1)S(1)}, u32[]{:S(2)}, u32[]{:S(2)}) collective-permute-start(bf16[32,2048]{1,0:T(8,128)(2,1)S(1)} %get-tuple-element.47), channel_id=1, source_target_pairs={{0,30},{1,3},{2,0},{3,5},{4,2},{5,7},{6,4},{7,9},{8,6},{9,11},{10,... | collective-permute-start | bytes 393224 | tf_op jit(solution)/shard_map/ppermute | solution.py:213
  55.5 16.0 %collective-permute-start.5 = (bf16[16,2048]{1,0:T(8,128)(2,1)S(1)}, bf16[16,2048]{1,0:T(8,128)(2,1)S(1)}, u32[]{:S(2)}, u32[]{:S(2)}) collective-permute-start(bf16[16,2048]{1,0:T(8,128)(2,1)S(1)} %get-tuple-element.42), channel_id=1, source_target_pairs={{0,28},{1,5},{2,30},{3,7},{4,0},{5,9},{6,2},{7,11},{8,4},{9,13},{1... | collective-permute-start | bytes 196616 | tf_op jit(solution)/shard_map/ppermute | solution.py:213
  65.3 18.8 %collective-permute-start.18 = (bf16[48,2048]{1,0:T(8,128)(2,1)S(1)}, bf16[48,2048]{1,0:T(8,128)(2,1)S(1)}, u32[]{:S(2)}, u32[]{:S(2)}) collective-permute-start(bf16[48,2048]{1,0:T(8,128)(2,1)S(1)} %get-tuple-element.55), channel_id=1, source_target_pairs={{0,30},{1,3},{2,0},{3,5},{4,2},{5,7},{6,4},{7,9},{8,6},{9,11},{10,... | collective-permute-start | bytes 589832 | tf_op jit(solution)/shard_map/ppermute | solution.py:213
  66.9 17.2 %collective-permute-start.19 = (bf16[48,2048]{1,0:T(8,128)(2,1)S(1)}, bf16[48,2048]{1,0:T(8,128)(2,1)S(1)}, u32[]{:S(2)}, u32[]{:S(2)}) collective-permute-start(bf16[48,2048]{1,0:T(8,128)(2,1)S(1)} %get-tuple-element.56), channel_id=1, source_target_pairs={{0,2},{1,31},{2,4},{3,1},{4,6},{5,3},{6,8},{7,5},{8,10},{9,7},{10,... | collective-permute-start | bytes 589832 | tf_op jit(solution)/shard_map/ppermute | solution.py:213
  67.4 9.9 %collective-permute-start.6 = (bf16[16,2048]{1,0:T(8,128)(2,1)S(1)}, bf16[16,2048]{1,0:T(8,128)(2,1)S(1)}, u32[]{:S(2)}, u32[]{:S(2)}) collective-permute-start(bf16[16,2048]{1,0:T(8,128)(2,1)S(1)} %get-tuple-element.43), channel_id=1, source_target_pairs={{0,4},{1,29},{2,6},{3,31},{4,8},{5,1},{6,10},{7,3},{8,12},{9,5},{1... | collective-permute-start | bytes 196616 | tf_op jit(solution)/shard_map/ppermute | solution.py:213
  67.4 16.6 %collective-permute-start.16 = (bf16[32,2048]{1,0:T(8,128)(2,1)S(1)}, bf16[32,2048]{1,0:T(8,128)(2,1)S(1)}, u32[]{:S(2)}, u32[]{:S(2)}) collective-permute-start(bf16[32,2048]{1,0:T(8,128)(2,1)S(1)} %get-tuple-element.53), channel_id=1, source_target_pairs={{0,28},{1,5},{2,30},{3,7},{4,0},{5,9},{6,2},{7,11},{8,4},{9,13},{1... | collective-permute-start | bytes 393224 | tf_op jit(solution)/shard_map/ppermute | solution.py:213
  71.6 12.5 %collective-permute-start.17 = (bf16[32,2048]{1,0:T(8,128)(2,1)S(1)}, bf16[32,2048]{1,0:T(8,128)(2,1)S(1)}, u32[]{:S(2)}, u32[]{:S(2)}) collective-permute-start(bf16[32,2048]{1,0:T(8,128)(2,1)S(1)} %get-tuple-element.54), channel_id=1, source_target_pairs={{0,4},{1,29},{2,6},{3,31},{4,8},{5,1},{6,10},{7,3},{8,12},{9,5},{1... | collective-permute-start | bytes 393224 | tf_op jit(solution)/shard_map/ppermute | solution.py:213
  77.3 6.7 %collective-permute-start.20 = (bf16[16,2048]{1,0:T(8,128)(2,1)S(1)}, bf16[16,2048]{1,0:T(8,128)(2,1)S(1)}, u32[]{:S(2)}, u32[]{:S(2)}) collective-permute-start(bf16[16,2048]{1,0:T(8,128)(2,1)S(1)} %get-tuple-element.58), channel_id=1, source_target_pairs={{0,26},{1,7},{2,28},{3,9},{4,30},{5,11},{6,0},{7,13},{8,2},{9,15},... | collective-permute-start | bytes 196616 | tf_op jit(solution)/shard_map/ppermute | solution.py:213
  84.7 1.7 %collective-permute-start.22 = (bf16[64,2048]{1,0:T(8,128)(2,1)S(1)}, bf16[64,2048]{1,0:T(8,128)(2,1)S(1)}, u32[]{:S(2)}, u32[]{:S(2)}) collective-permute-start(bf16[64,2048]{1,0:T(8,128)(2,1)S(1)} %get-tuple-element.66), channel_id=1, source_target_pairs={{0,1},{1,0},{2,3},{3,2},{4,5},{5,4},{6,7},{7,6},{8,9},{9,8},{10,11... | collective-permute-start | bytes 786440 | tf_op jit(solution)/shard_map/ppermute | solution.py:216
  84.8 8.5 %collective-permute-start.21 = (bf16[32,2048]{1,0:T(8,128)(2,1)S(1)}, bf16[32,2048]{1,0:T(8,128)(2,1)S(1)}, u32[]{:S(2)}, u32[]{:S(2)}) collective-permute-start(bf16[32,2048]{1,0:T(8,128)(2,1)S(1)} %get-tuple-element.64), channel_id=1, source_target_pairs={{0,1},{1,0},{2,3},{3,2},{4,5},{5,4},{6,7},{7,6},{8,9},{9,8},{10,11... | collective-permute-start | bytes 393224 | tf_op jit(solution)/shard_map/ppermute | solution.py:216
  86.4 10.1 %collective-permute-start.23 = (bf16[32,2048]{1,0:T(8,128)(2,1)S(1)}, bf16[32,2048]{1,0:T(8,128)(2,1)S(1)}, u32[]{:S(2)}, u32[]{:S(2)}) collective-permute-start(bf16[32,2048]{1,0:T(8,128)(2,1)S(1)} %get-tuple-element.67), channel_id=1, source_target_pairs={{0,22},{1,11},{2,24},{3,13},{4,26},{5,15},{6,28},{7,17},{8,30},{9,... | collective-permute-start | bytes 393224 | tf_op jit(solution)/shard_map/ppermute | solution.py:213
  91.9 16.0 %collective-permute-start.24 = (bf16[32,2048]{1,0:T(8,128)(2,1)S(1)}, bf16[32,2048]{1,0:T(8,128)(2,1)S(1)}, u32[]{:S(2)}, u32[]{:S(2)}) collective-permute-start(bf16[32,2048]{1,0:T(8,128)(2,1)S(1)} %get-tuple-element.68), channel_id=1, source_target_pairs={{0,10},{1,23},{2,12},{3,25},{4,14},{5,27},{6,16},{7,29},{8,18},{9,... | collective-permute-start | bytes 393224 | tf_op jit(solution)/shard_map/ppermute | solution.py:213

commit v7 on v5

--- a/solution.py
+++ b/solution.py
@@ -73,7 +73,7 @@
     out_ref[:, width:] = meta.astype(jnp.bfloat16)
 
 
-def hand_on(chips, cap, top, count, place_ref, *refs):
+def hand_on(chips, cap, top, count, cross, place_ref, *refs):
     sources, refs = refs[:count], refs[count:]
     blocks, (high_ref, low_ref, all_ref) = refs[:-3], refs[-3:]
     rows = sources[0].shape[0]
@@ -90,6 +90,7 @@
     chip = z + jnp.where(c == 0, step, -step)
     chip = jnp.where(chip < 0, chip + chips, chip)
     chip = jnp.where(chip >= chips, chip - chips, chip)
+    source = jnp.where(block == len(NEAR), cross, source)
     target = ((2 * chip + c) * cap + slot + source * 2 * chips * cap).astype(jnp.float32)
     for s in range(count):
         all_ref[s * rows : (s + 1) * rows, :] = sources[s][...]
@@ -124,9 +125,10 @@
         at += b.shape[0]
 
 
-def experts(tile, count, *refs):
+def experts(tile, counts, *refs):
+    count = sum(counts)
     blocks, (gate_ref, up_ref, down_ref), refs = refs[:count], refs[count : count + 3], refs[count + 3 :]
-    outs, (x_ref, total_ref) = refs[:count], refs[count:]
+    outs, (x_ref, total_ref) = refs[:-2], refs[-2:]
     gather(blocks, x_ref)
     hidden = gate_ref.shape[1]
     total_ref[...] = jnp.zeros_like(total_ref)
@@ -142,42 +144,41 @@
         active = (gate * jax.nn.sigmoid(1.702 * gate) * (upper + 1.0)).astype(jnp.bfloat16)
         total_ref[...] += jnp.dot(active, down_ref[cols, :], preferred_element_type=jnp.float32)
 
-    at = 0
-    for o in outs:
-        o[...] = total_ref[at : at + o.shape[0], :].astype(jnp.bfloat16)
-        at += o.shape[0]
-
-
-def weighted(blocks, high_ref, low_ref, x_ref):
-    gather(blocks, x_ref)
-    x = x_ref[...]
-    total = jnp.dot(high_ref[...], x, preferred_element_type=jnp.float32)
-    return total + jnp.dot(low_ref[...], x, preferred_element_type=jnp.float32)
-
-
-def weigh_near(*refs):
-    mine, other, x_ref = refs[-3:]
-    total = weighted(refs[:-5], *refs[-5:-3], x_ref)
-    rows = mine.shape[0]
-    mine[...] = total[:rows]
-    other[...] = total[rows:].astype(jnp.bfloat16)
-
-
-def weigh_far(*refs):
-    mine, other, x_ref = refs[-3:]
-    total = weighted(refs[:-5], *refs[-5:-3], x_ref)
-    rows = mine.shape[0] // 2
-    mine[:rows] = total[:rows]
-    mine[rows:] = total[2 * rows : 3 * rows]
-    other[:rows] = total[3 * rows :].astype(jnp.bfloat16)
-    other[rows:] = total[rows : 2 * rows].astype(jnp.bfloat16)
-
-
-def join(mine, other, one, two):
-    rows = one.shape[0]
-    total = mine[...] + other[...].astype(jnp.float32)
-    one[...] = total[:rows].astype(jnp.bfloat16)
-    two[...] = total[rows:].astype(jnp.bfloat16)
+    at, filled = 0, [0] * len(outs)
+    i = 0
+    for group in counts:
+        for j in range(group):
+            size = blocks[i].shape[0]
+            outs[j][filled[j] : filled[j] + size] = total_ref[at : at + size, :].astype(jnp.bfloat16)
+            filled[j] += size
+            at += size
+            i += 1
+
+
+def weigh(counts, *refs):
+    blocks, refs = refs[: max(counts)], refs[max(counts) :]
+    weights, refs = refs[: 2 * len(counts)], refs[2 * len(counts) :]
+    outs, scratch = refs[: 2 * len(counts)], refs[2 * len(counts) :]
+    taken = [0] * len(blocks)
+    for g, count in enumerate(counts):
+        high_ref, low_ref = weights[2 * g : 2 * g + 2]
+        mine, other = outs[2 * g : 2 * g + 2]
+        x_ref, rows = scratch[g], mine.shape[0]
+        cap, at = x_ref.shape[0] // (2 * len(NEAR)), 0
+        for j in range(count):
+            size = 2 * cap if j < len(NEAR) else cap
+            x_ref[at : at + size, :] = blocks[j][taken[j] : taken[j] + size]
+            taken[j] += size
+            at += size
+        x = x_ref[...]
+        total = jnp.dot(high_ref[...], x, preferred_element_type=jnp.float32)
+        total += jnp.dot(low_ref[...], x, preferred_element_type=jnp.float32)
+        mine[...] = total[:rows]
+        other[...] = total[rows:].astype(jnp.bfloat16)
+
+
+def join(mine, other, out):
+    out[...] = (mine[...] + other[...].astype(jnp.float32)).astype(jnp.bfloat16)
 
 
 def finish(mine, other, one, two, out):
@@ -221,55 +222,71 @@
         compiler_params=pltpu.CompilerParams(vmem_limit_bytes=60 << 20),
         cost_estimate=pl.CostEstimate(flops=1 << 20, bytes_accessed=1 << 20, transcendentals=0),
     )(tokens, norm_gain[None, :], routes.T, route_logits.T)
-    own2 = swap(own)
-    low, high = shift(own, HOP), shift(own, -HOP)
-    high2, low2 = swap(low), swap(high)
     steps = (*NEAR, 3)
 
-    def hand(sources, sizes, flops):
-        count = len(sources)
-        weight = bf16(count * rows, sum(sizes))
-        *blocks, w_high, w_low = call(
-            functools.partial(hand_on, chips, cap, top, count),
+    def hand(sources, cross, flops):
+        sizes = [2 * cap] * len(NEAR) + ([] if cross is None else [cap])
+        weight = bf16(2 * rows, sum(sizes))
+        hand_of = call(
+            functools.partial(hand_on, chips, cap, top, 2, cross or 0),
             [bf16(n, width) for n in sizes] + [weight, weight],
-            count + 1,
+            3,
             smem=1,
-            scratch=[pltpu.VMEM((count * rows, width + META), jnp.bfloat16)],
+            scratch=[pltpu.VMEM((2 * rows, width + META), jnp.bfloat16)],
             flops=flops,
-        )(place, *sources)
+        )
+        *blocks, w_high, w_low = hand_of(place, *sources)
         return [shift(b, d) if d else b for b, d in zip(blocks, steps)], (w_high, w_low)
 
-    def run(blocks):
+    def run(*groups):
+        counts = [len(g) for g in groups]
+        blocks = [b for g in groups for b in g]
         slots = sum(b.shape[0] for b in blocks)
+        sizes = [0] * max(counts)
+        for g in groups:
+            for j, b in enumerate(g):
+                sizes[j] += b.shape[0]
         experts_of = call(
-            functools.partial(experts, 256, len(blocks)),
-            [bf16(*b.shape) for b in blocks],
+            functools.partial(experts, 256, counts),
+            [bf16(n, width) for n in sizes],
             len(blocks) + 3,
             scratch=[pltpu.VMEM((slots, width), jnp.bfloat16), pltpu.VMEM((slots, width), jnp.float32)],
             flops=6 * slots * width * hidden,
         )
-        return experts_of(*blocks, w_gate[0], w_up[0], w_down[0])
-
-    def weigh(body, blocks, weights, rows):
-        back = [shift(b, -d) if d else b for b, d in zip(blocks, steps)]
-        slots = sum(b.shape[0] for b in blocks)
+        results = experts_of(*blocks, w_gate[0], w_up[0], w_down[0])
+        return [shift(b, -d) if d else b for b, d in zip(results, steps)]
+
+    def sums(back, *weights):
+        counts = [len(NEAR) + (w[0].shape[1] > 2 * cap * len(NEAR)) for w in weights]
         sums_of = call(
-            body,
-            [f32(rows, width), bf16(rows, width)],
-            len(back) + 2,
-            scratch=[pltpu.VMEM((slots, width), jnp.bfloat16)],
+            functools.partial(weigh, counts),
+            [f32(rows, width), bf16(rows, width)] * len(weights),
+            len(back) + 2 * len(weights),
+            scratch=[pltpu.VMEM((w[0].shape[1], width), jnp.bfloat16) for w in weights],
         )
-        return sums_of(*back, *weights)
-
-    heavy = 24 * 256 * width * hidden
-    near, near_weights = hand((own, own2), [2 * cap] * 5, heavy)
-    far, far_weights = hand((low, low2, high, high2), [4 * cap] * 5 + [2 * cap], 1 << 28)
-    near = run(near)
-    far = run(far)
-    mine, other = weigh(weigh_near, near, near_weights, rows)
-    far_mine, far_other = weigh(weigh_far, far, far_weights, 2 * rows)
-    one, two = call(join, [bf16(rows, width)] * 2, 2)(far_mine, swap(far_other))
-    return call(finish, bf16(rows, width), 4)(mine, swap(other), shift(one, -HOP), shift(two, HOP))
+        return sums_of(*back, *(w for pair in weights for w in pair))
+
+    def home(mine, other, by):
+        other = swap(other)
+        total = call(join, bf16(rows, width), 2)(mine, other)
+        return shift(total, by)
+
+    own2 = swap(own)
+    low = shift(own, HOP)
+    high = shift(own, -HOP)
+    high2 = swap(low)
+    low2 = swap(high)
+    near, near_weights = hand((own, own2), None, 24 * 256 * width * hidden)
+    one, one_weights = hand((low, high2), 0, 1 << 26)
+    two, two_weights = hand((high, low2), 1, 1 << 26)
+    back_one = run(near, one)
+    back_two = run(two)
+    mine, other, one_mine, one_other = sums(back_one, near_weights, one_weights)
+    two_mine, two_other = sums(back_two, two_weights)
+    one = home(one_mine, one_other, -HOP)
+    two = home(two_mine, two_other, HOP)
+    other = swap(other)
+    return call(finish, bf16(rows, width), 4)(mine, other, one, two)
 
 
 def solution(mesh):

time: 133 us -> 130 us (0.977)
  the two profiles are of different devices: /device:TPU:86 before, /device:TPU:69 now
where the time goes in v7:
time: 130 us
  starting transfers between devices  84.9 us (65%)
  waiting for transfers between devices  26.9 us (21%)
  Pallas kernels  17.6 us (14%)
    ppermute x28, starting transfers between devices, shift(): return lax.ppermute(x, ('z', 'c'), pairs)  65 us
    ppermute x28, waiting for transfers between devices, shift(): return lax.ppermute(x, ('z', 'c'), pairs)  26.9 us
    ppermute x6, starting transfers between devices, swap(): return lax.ppermute(x, 'c', [(0, 1), (1, 0)])  20 us
    pallas_call x2, Pallas kernels, run(): results = experts_of(*blocks, w_gate[0], w_up[0], w_down[0])  11.8 us
    pallas_call x3, Pallas kernels, hand(): *blocks, w_high, w_low = hand_of(place, *sources)  2.8 us
  transfers between devices with their start and end apart: 34, of which 6 were waited for; matrix products, arithmetic and copies ran while one was open for 0% of the time, Pallas kernels for 12%

profile of v7, /device:TPU:69, one launch (start us, length us, event | category | flops | bytes accessed | tf_op | source)
XLA Modules:
  0.0 129.7 jit_solution(13107017269530437929)
XLA Ops:
  0.0 1.5 %shard_map.73.refs_0_ = bf16[32,2176]{1,0:T(8,128)(2,1)S(1)} custom-call(bf16[32,2048]{1,0:T(8,128)(2,1)} %tok_hbm.1, f32[1,2048]{1,0:T(1,128)} %bitcast.20, s32[4,32]{1,0:T(4,128)} %bitcast.21, f32[4,32]{1,0:T(4,128)} %bitcast.22), custom_call_target="tpu_custom_call" | custom-call | flops 1048576 | bytes 1048576 | tf_op jit(solution)/shard_map/pallas_call | solution.py:210
  1.5 10.2 %collective-permute-start.20 = (bf16[32,2176]{1,0:T(8,128)(2,1)S(1)}, bf16[32,2176]{1,0:T(8,128)(2,1)S(1)}, u32[]{:S(2)}, u32[]{:S(2)}) collective-permute-start(bf16[32,2176]{1,0:T(8,128)(2,1)S(1)} %shard_map.73.refs_0_), channel_id=1, source_target_pairs={{0,22},{1,11},{2,24},{3,13},{4,26},{5,15},{6,28},{7,17},{8,30},{9,... | collective-permute-start | bytes 417800 | tf_op jit(solution)/shard_map/ppermute | solution.py:204
  11.7 5.3 %collective-permute-start.5 = (bf16[32,2176]{1,0:T(8,128)(2,1)S(1)}, bf16[32,2176]{1,0:T(8,128)(2,1)S(1)}, u32[]{:S(2)}, u32[]{:S(2)}) collective-permute-start(bf16[32,2176]{1,0:T(8,128)(2,1)S(1)} %shard_map.73.refs_0_), channel_id=1, source_target_pairs={{0,10},{1,23},{2,12},{3,25},{4,14},{5,27},{6,16},{7,29},{8,18},{9,... | collective-permute-start | bytes 417800 | tf_op jit(solution)/shard_map/ppermute | solution.py:204
  17.0 1.4 %collective-permute-start = (bf16[32,2176]{1,0:T(8,128)(2,1)S(1)}, bf16[32,2176]{1,0:T(8,128)(2,1)S(1)}, u32[]{:S(2)}, u32[]{:S(2)}) collective-permute-start(bf16[32,2176]{1,0:T(8,128)(2,1)S(1)} %shard_map.73.refs_0_), channel_id=1, source_target_pairs={{0,1},{1,0},{2,3},{3,2},{4,5},{5,4},{6,7},{7,6},{8,9},{9,8},{10,11... | collective-permute-start | bytes 417800 | tf_op jit(solution)/shard_map/ppermute | solution.py:207
  18.4 0.1 pad_add_fusion.place_ref
  18.4 1.2 collective-permute-done.20.refs_0_
  19.7 9.4 %collective-permute-start.21 = (bf16[32,2176]{1,0:T(8,128)(2,1)S(1)}, bf16[32,2176]{1,0:T(8,128)(2,1)S(1)}, u32[]{:S(2)}, u32[]{:S(2)}) collective-permute-start(bf16[32,2176]{1,0:T(8,128)(2,1)S(1)} %collective-permute-done.20.refs_0_), channel_id=1, source_target_pairs={{0,1},{1,0},{2,3},{3,2},{4,5},{5,4},{6,7},{7,6},{8,9},{9,8},{10,11... | collective-permute-start | bytes 417800 | tf_op jit(solution)/shard_map/ppermute | solution.py:207
  29.1 0.0 collective-permute-done.5.refs_0_
  29.1 0.5 collective-permute-start.6
  29.6 0.0 collective-permute-done.refs_1_
  29.6 0.9 shard_map.74
  30.6 5.9 %collective-permute-start.1 = (bf16[16,2048]{1,0:T(8,128)(2,1)S(1)}, bf16[16,2048]{1,0:T(8,128)(2,1)S(1)}, u32[]{:S(2)}, u32[]{:S(2)}) collective-permute-start(bf16[16,2048]{1,0:T(8,128)(2,1)S(1)} %get-tuple-element.46), channel_id=1, source_target_pairs={{0,4},{1,29},{2,6},{3,31},{4,8},{5,1},{6,10},{7,3},{8,12},{9,5},{1... | collective-permute-start | bytes 196616 | tf_op jit(solution)/shard_map/ppermute | solution.py:204
  36.4 5.8 %collective-permute-start.3 = (bf16[16,2048]{1,0:T(8,128)(2,1)S(1)}, bf16[16,2048]{1,0:T(8,128)(2,1)S(1)}, u32[]{:S(2)}, u32[]{:S(2)}) collective-permute-start(bf16[16,2048]{1,0:T(8,128)(2,1)S(1)} %get-tuple-element.48), channel_id=1, source_target_pairs={{0,2},{1,31},{2,4},{3,1},{4,6},{5,3},{6,8},{7,5},{8,10},{9,7},{10,... | collective-permute-start | bytes 196616 | tf_op jit(solution)/shard_map/ppermute | solution.py:204
  42.2 0.0 collective-permute-done.21.refs_1_
  42.2 0.0 collective-permute-start.4
  42.2 0.9 shard_map.79
  43.2 0.0 collective-permute-done.1.refs_0_
  43.2 1.3 collective-permute-start.22
  44.5 0.0 collective-permute-done.2.refs_1_
  44.5 1.2 collective-permute-start.23
  45.7 3.9 %collective-permute-start.24 = (bf16[16,2048]{1,0:T(8,128)(2,1)S(1)}, bf16[16,2048]{1,0:T(8,128)(2,1)S(1)}, u32[]{:S(2)}, u32[]{:S(2)}) collective-permute-start(bf16[16,2048]{1,0:T(8,128)(2,1)S(1)} %get-tuple-element.73), channel_id=1, source_target_pairs={{0,2},{1,31},{2,4},{3,1},{4,6},{5,3},{6,8},{7,5},{8,10},{9,7},{10,... | collective-permute-start | bytes 196616 | tf_op jit(solution)/shard_map/ppermute | solution.py:204
  49.5 0.0 collective-permute-done.4.refs_3_
  49.5 0.0 collective-permute-start.25
  49.6 0.0 collective-permute-done.6.refs_1_
  49.6 1.3 collective-permute-start.26
  50.9 0.9 shard_map.75
  51.8 3.0 %collective-permute-done.26.refs_5_ = bf16[8,2048]{1,0:T(8,128)(2,1)S(1)} collective-permute-done((bf16[8,2048]{1,0:T(8,128)(2,1)S(1)}, bf16[8,2048]{1,0:T(8,128)(2,1)S(1)}, u32[]{:S(2)}, u32[]{:S(2)}) %collective-permute-start.26) | collective-permute-done | bytes 32800 | tf_op jit(solution)/shard_map/ppermute | solution.py:204
  54.8 2.2 %collective-permute-start.11 = (bf16[8,2048]{1,0:T(8,128)(2,1)S(1)}, bf16[8,2048]{1,0:T(8,128)(2,1)S(1)}, u32[]{:S(2)}, u32[]{:S(2)}) collective-permute-start(bf16[8,2048]{1,0:T(8,128)(2,1)S(1)} %get-tuple-element.56), channel_id=1, source_target_pairs={{0,6},{1,27},{2,8},{3,29},{4,10},{5,31},{6,12},{7,1},{8,14},{9,3},... | collective-permute-start | bytes 98312 | tf_op jit(solution)/shard_map/ppermute | solution.py:204
  57.0 4.3 %collective-permute-start.7 = (bf16[16,2048]{1,0:T(8,128)(2,1)S(1)}, bf16[16,2048]{1,0:T(8,128)(2,1)S(1)}, u32[]{:S(2)}, u32[]{:S(2)}) collective-permute-start(bf16[16,2048]{1,0:T(8,128)(2,1)S(1)} %get-tuple-element.51), channel_id=1, source_target_pairs={{0,4},{1,29},{2,6},{3,31},{4,8},{5,1},{6,10},{7,3},{8,12},{9,5},{1... | collective-permute-start | bytes 196616 | tf_op jit(solution)/shard_map/ppermute | solution.py:204
  61.3 0.0 collective-permute-start.8
  61.3 0.0 collective-permute-done.24.refs_2_
  61.3 0.4 collective-permute-start.9
  61.7 0.0 collective-permute-done.25.refs_3_
  61.7 1.2 collective-permute-start.10
  63.0 5.4 %shard_map.80 = (bf16[16,2048]{1,0:T(8,128)(2,1)S(1)}, bf16[16,2048]{1,0:T(8,128)(2,1)S(1)}, bf16[16,2048]{1,0:T(8,128)(2,1)S(1)}, bf16[16,2048]{1,0:T(8,128)(2,...) custom-call(bf16[16,2048]{1,0:T(8,128)(2,1)S(1)} %collective-permute-done.22.refs_0_, ...), custom_call_target="tpu_custom_call" | custom-call | flops 1937768448 | bytes 1048576 | tf_op jit(solution)/shard_map/pallas_call | solution.py:256
  68.4 0.0 collective-permute-done.11.refs_10_
  68.4 2.1 %collective-permute-start.31 = (bf16[8,2048]{1,0:T(8,128)(2,1)S(1)}, bf16[8,2048]{1,0:T(8,128)(2,1)S(1)}, u32[]{:S(2)}, u32[]{:S(2)}) collective-permute-start(bf16[8,2048]{1,0:T(8,128)(2,1)S(1)} %get-tuple-element.82), channel_id=1, source_target_pairs={{0,26},{1,7},{2,28},{3,9},{4,30},{5,11},{6,0},{7,13},{8,2},{9,15},... | collective-permute-start | bytes 98312 | tf_op jit(solution)/shard_map/ppermute | solution.py:204
  70.5 0.0 collective-permute-done.7.refs_5_
  70.5 0.4 collective-permute-start.27
  70.9 0.0 collective-permute-done.8.refs_6_
  70.9 3.2 %collective-permute-start.28 = (bf16[16,2048]{1,0:T(8,128)(2,1)S(1)}, bf16[16,2048]{1,0:T(8,128)(2,1)S(1)}, u32[]{:S(2)}, u32[]{:S(2)}) collective-permute-start(bf16[16,2048]{1,0:T(8,128)(2,1)S(1)} %get-tuple-element.78), channel_id=1, source_target_pairs={{0,4},{1,29},{2,6},{3,31},{4,8},{5,1},{6,10},{7,3},{8,12},{9,5},{1... | collective-permute-start | bytes 196616 | tf_op jit(solution)/shard_map/ppermute | solution.py:204
  74.1 0.4 collective-permute-start.29
  74.5 6.4 %shard_map.76 = (bf16[32,2048]{1,0:T(8,128)(2,1)S(1)}, bf16[32,2048]{1,0:T(8,128)(2,1)S(1)}, bf16[32,2048]{1,0:T(8,128)(2,1)S(1)}, bf16[32,2048]{1,0:T(8,128)(2,...) custom-call(bf16[16,2048]{1,0:T(8,128)(2,1)S(1)} %collective-permute-done.1.refs_0_, ...), custom_call_target="tpu_custom_call" | custom-call | flops 3699376128 | bytes 1048576 | tf_op jit(solution)/shard_map/pallas_call | solution.py:256
  80.9 0.1 collective-permute-start.12
  81.0 3.5 %collective-permute-start.13 = (bf16[32,2048]{1,0:T(8,128)(2,1)S(1)}, bf16[32,2048]{1,0:T(8,128)(2,1)S(1)}, u32[]{:S(2)}, u32[]{:S(2)}) collective-permute-start(bf16[32,2048]{1,0:T(8,128)(2,1)S(1)} %get-tuple-element.58), channel_id=1, source_target_pairs={{0,4},{1,29},{2,6},{3,31},{4,8},{5,1},{6,10},{7,3},{8,12},{9,5},{1... | collective-permute-start | bytes 393224 | tf_op jit(solution)/shard_map/ppermute | solution.py:204
  84.6 0.0 collective-permute-done.27.refs_0_
  84.6 0.0 collective-permute-start.14
  84.6 0.0 collective-permute-done.28.refs_1_
  84.6 2.6 %collective-permute-start.15 = (bf16[32,2048]{1,0:T(8,128)(2,1)S(1)}, bf16[32,2048]{1,0:T(8,128)(2,1)S(1)}, u32[]{:S(2)}, u32[]{:S(2)}) collective-permute-start(bf16[32,2048]{1,0:T(8,128)(2,1)S(1)} %get-tuple-element.60), channel_id=1, source_target_pairs={{0,2},{1,31},{2,4},{3,1},{4,6},{5,3},{6,8},{7,5},{8,10},{9,7},{10,... | collective-permute-start | bytes 393224 | tf_op jit(solution)/shard_map/ppermute | solution.py:204
  87.2 0.0 collective-permute-done.29.refs_2_
  87.2 0.1 collective-permute-start.30
  87.4 3.8 %collective-permute-done.30.refs_3_ = bf16[16,2048]{1,0:T(8,128)(2,1)S(1)} collective-permute-done((bf16[16,2048]{1,0:T(8,128)(2,1)S(1)}, bf16[16,2048]{1,0:T(8,128)(2,1)S(1)}, u32[]{:S(2)}, u32[]{:S(2)}) %collective-permute-start.30) | collective-permute-done | bytes 65568 | tf_op jit(solution)/shard_map/ppermute | solution.py:204
  91.1 3.1 %collective-permute-start.16 = (bf16[8,2048]{1,0:T(8,128)(2,1)S(1)}, bf16[8,2048]{1,0:T(8,128)(2,1)S(1)}, u32[]{:S(2)}, u32[]{:S(2)}) collective-permute-start(bf16[8,2048]{1,0:T(8,128)(2,1)S(1)} %get-tuple-element.62), channel_id=1, source_target_pairs={{0,26},{1,7},{2,28},{3,9},{4,30},{5,11},{6,0},{7,13},{8,2},{9,15},... | collective-permute-start | bytes 98312 | tf_op jit(solution)/shard_map/ppermute | solution.py:204
  94.2 0.3 shard_map.81
  94.5 2.7 %collective-permute-done.16.refs_5_ = bf16[8,2048]{1,0:T(8,128)(2,1)S(1)} collective-permute-done((bf16[8,2048]{1,0:T(8,128)(2,1)S(1)}, bf16[8,2048]{1,0:T(8,128)(2,1)S(1)}, u32[]{:S(2)}, u32[]{:S(2)}) %collective-permute-start.16) | collective-permute-done | bytes 32800 | tf_op jit(solution)/shard_map/ppermute | solution.py:204
  97.3 8.1 %collective-permute-start.32 = (bf16[32,2048]{1,0:T(8,128)(2,1)S(1)}, bf16[32,2048]{1,0:T(8,128)(2,1)S(1)}, u32[]{:S(2)}, u32[]{:S(2)}) collective-permute-start(bf16[32,2048]{1,0:T(8,128)(2,1)S(1)} %get-tuple-element.86), channel_id=1, source_target_pairs={{0,1},{1,0},{2,3},{3,2},{4,5},{5,4},{6,7},{7,6},{8,9},{9,8},{10,11... | collective-permute-start | bytes 393224 | tf_op jit(solution)/shard_map/ppermute | solution.py:207
  105.4 0.4 shard_map.77
  105.8 0.1 collective-permute-start.18
  105.9 0.5 collective-permute-start.17
  106.4 4.1 %collective-permute-start.33 = (bf16[32,2048]{1,0:T(8,128)(2,1)S(1)}, bf16[32,2048]{1,0:T(8,128)(2,1)S(1)}, u32[]{:S(2)}, u32[]{:S(2)}) collective-permute-start(bf16[32,2048]{1,0:T(8,128)(2,1)S(1)} %shard_map.82), channel_id=1, source_target_pairs={{0,10},{1,23},{2,12},{3,25},{4,14},{5,27},{6,16},{7,29},{8,18},{9,... | collective-permute-start | bytes 393224 | tf_op jit(solution)/shard_map/ppermute | solution.py:204
  110.5 2.4 %collective-permute-start.19 = (bf16[32,2048]{1,0:T(8,128)(2,1)S(1)}, bf16[32,2048]{1,0:T(8,128)(2,1)S(1)}, u32[]{:S(2)}, u32[]{:S(2)}) collective-permute-start(bf16[32,2048]{1,0:T(8,128)(2,1)S(1)} %shard_map.78), channel_id=1, source_target_pairs={{0,22},{1,11},{2,24},{3,13},{4,26},{5,15},{6,28},{7,17},{8,30},{9,... | collective-permute-start | bytes 393224 | tf_op jit(solution)/shard_map/ppermute | solution.py:204
  113.0 13.1 %collective-permute-done.33.two = bf16[32,2048]{1,0:T(8,128)(2,1)S(1)} collective-permute-done((bf16[32,2048]{1,0:T(8,128)(2,1)S(1)}, bf16[32,2048]{1,0:T(8,128)(2,1)S(1)}, u32[]{:S(2)}, u32[]{:S(2)}) %collective-permute-start.33) | collective-permute-done | bytes 131104 | tf_op jit(solution)/shard_map/ppermute | solution.py:204
  126.0 3.0 %collective-permute-done.19.one = bf16[32,2048]{1,0:T(8,128)(2,1)S(1)} collective-permute-done((bf16[32,2048]{1,0:T(8,128)(2,1)S(1)}, bf16[32,2048]{1,0:T(8,128)(2,1)S(1)}, u32[]{:S(2)}, u32[]{:S(2)}) %collective-permute-start.19) | collective-permute-done | bytes 131104 | tf_op jit(solution)/shard_map/ppermute | solution.py:204
  129.0 0.7 shard_map.83
  (31 shorter events, 0.1 us)
Async XLA Ops:
  1.5 18.2 %collective-permute-start.20 = (bf16[32,2176]{1,0:T(8,128)(2,1)S(1)}, bf16[32,2176]{1,0:T(8,128)(2,1)S(1)}, u32[]{:S(2)}, u32[]{:S(2)}) collective-permute-start(bf16[32,2176]{1,0:T(8,128)(2,1)S(1)} %shard_map.73.refs_0_), channel_id=1, source_target_pairs={{0,22},{1,11},{2,24},{3,13},{4,26},{5,15},{6,28},{7,17},{8,30},{9,... | collective-permute-start | bytes 417800 | tf_op jit(solution)/shard_map/ppermute | solution.py:204
  11.7 17.4 %collective-permute-start.5 = (bf16[32,2176]{1,0:T(8,128)(2,1)S(1)}, bf16[32,2176]{1,0:T(8,128)(2,1)S(1)}, u32[]{:S(2)}, u32[]{:S(2)}) collective-permute-start(bf16[32,2176]{1,0:T(8,128)(2,1)S(1)} %shard_map.73.refs_0_), channel_id=1, source_target_pairs={{0,10},{1,23},{2,12},{3,25},{4,14},{5,27},{6,16},{7,29},{8,18},{9,... | collective-permute-start | bytes 417800 | tf_op jit(solution)/shard_map/ppermute | solution.py:204
  17.0 12.7 %collective-permute-start = (bf16[32,2176]{1,0:T(8,128)(2,1)S(1)}, bf16[32,2176]{1,0:T(8,128)(2,1)S(1)}, u32[]{:S(2)}, u32[]{:S(2)}) collective-permute-start(bf16[32,2176]{1,0:T(8,128)(2,1)S(1)} %shard_map.73.refs_0_), channel_id=1, source_target_pairs={{0,1},{1,0},{2,3},{3,2},{4,5},{5,4},{6,7},{7,6},{8,9},{9,8},{10,11... | collective-permute-start | bytes 417800 | tf_op jit(solution)/shard_map/ppermute | solution.py:207
  18.3 44.5 %slice-start = ((s8[7340032]{0:T(1024)(128)(4,1)}), s8[4194304]{0:T(1024)(128)(4,1)S(1)}, s32[]{:S(2)}) async-start(s8[7340032]{0:T(1024)(128)(4,1)} %bitcast.8), calls=%async_computation | async-start | bytes 8388608
  18.3 44.5 %slice-start.2 = ((s8[7340032]{0:T(1024)(128)(4,1)}), s8[4194304]{0:T(1024)(128)(4,1)S(1)}, s32[]{:S(2)}) async-start(s8[7340032]{0:T(1024)(128)(4,1)} %bitcast.12), calls=%async_computation.2 | async-start | bytes 8388608
  18.4 44.5 %slice-start.4 = ((s8[7340032]{0:T(1024)(128)(4,1)}), s8[4194304]{0:T(1024)(128)(4,1)S(1)}, s32[]{:S(2)}) async-start(s8[7340032]{0:T(1024)(128)(4,1)} %bitcast.16), calls=%async_computation.4 | async-start | bytes 8388608
  18.4 44.5 %slice-start.1 = ((s8[7340032]{0:T(1024)(128)(4,1)}), s8[3145728]{0:T(1024)(128)(4,1)S(1)}, s32[]{:S(2)}) async-start(s8[7340032]{0:T(1024)(128)(4,1)} %bitcast.8), calls=%async_computation.1 | async-start | bytes 6291456
  18.4 44.5 %slice-start.3 = ((s8[7340032]{0:T(1024)(128)(4,1)}), s8[3145728]{0:T(1024)(128)(4,1)S(1)}, s32[]{:S(2)}) async-start(s8[7340032]{0:T(1024)(128)(4,1)} %bitcast.12), calls=%async_computation.3 | async-start | bytes 6291456
  18.4 44.5 %slice-start.5 = ((s8[7340032]{0:T(1024)(128)(4,1)}), s8[3145728]{0:T(1024)(128)(4,1)S(1)}, s32[]{:S(2)}) async-start(s8[7340032]{0:T(1024)(128)(4,1)} %bitcast.16), calls=%async_computation.5 | async-start | bytes 6291456
  19.7 22.6 %collective-permute-start.21 = (bf16[32,2176]{1,0:T(8,128)(2,1)S(1)}, bf16[32,2176]{1,0:T(8,128)(2,1)S(1)}, u32[]{:S(2)}, u32[]{:S(2)}) collective-permute-start(bf16[32,2176]{1,0:T(8,128)(2,1)S(1)} %collective-permute-done.20.refs_0_), channel_id=1, source_target_pairs={{0,1},{1,0},{2,3},{3,2},{4,5},{5,4},{6,7},{7,6},{8,9},{9,8},{10,11... | collective-permute-start | bytes 417800 | tf_op jit(solution)/shard_map/ppermute | solution.py:207
  29.1 20.4 %collective-permute-start.6 = (bf16[32,2176]{1,0:T(8,128)(2,1)S(1)}, bf16[32,2176]{1,0:T(8,128)(2,1)S(1)}, u32[]{:S(2)}, u32[]{:S(2)}) collective-permute-start(bf16[32,2176]{1,0:T(8,128)(2,1)S(1)} %collective-permute-done.5.refs_0_), channel_id=1, source_target_pairs={{0,1},{1,0},{2,3},{3,2},{4,5},{5,4},{6,7},{7,6},{8,9},{9,8},{10,11... | collective-permute-start | bytes 417800 | tf_op jit(solution)/shard_map/ppermute | solution.py:207
  30.6 12.6 %collective-permute-start.1 = (bf16[16,2048]{1,0:T(8,128)(2,1)S(1)}, bf16[16,2048]{1,0:T(8,128)(2,1)S(1)}, u32[]{:S(2)}, u32[]{:S(2)}) collective-permute-start(bf16[16,2048]{1,0:T(8,128)(2,1)S(1)} %get-tuple-element.46), channel_id=1, source_target_pairs={{0,4},{1,29},{2,6},{3,31},{4,8},{5,1},{6,10},{7,3},{8,12},{9,5},{1... | collective-permute-start | bytes 196616 | tf_op jit(solution)/shard_map/ppermute | solution.py:204
  36.4 8.0 %collective-permute-start.2 = (bf16[16,2048]{1,0:T(8,128)(2,1)S(1)}, bf16[16,2048]{1,0:T(8,128)(2,1)S(1)}, u32[]{:S(2)}, u32[]{:S(2)}) collective-permute-start(bf16[16,2048]{1,0:T(8,128)(2,1)S(1)} %get-tuple-element.47), channel_id=1, source_target_pairs={{0,28},{1,5},{2,30},{3,7},{4,0},{5,9},{6,2},{7,11},{8,4},{9,13},{1... | collective-permute-start | bytes 196616 | tf_op jit(solution)/shard_map/ppermute | solution.py:204
  36.4 9.2 %collective-permute-start.3 = (bf16[16,2048]{1,0:T(8,128)(2,1)S(1)}, bf16[16,2048]{1,0:T(8,128)(2,1)S(1)}, u32[]{:S(2)}, u32[]{:S(2)}) collective-permute-start(bf16[16,2048]{1,0:T(8,128)(2,1)S(1)} %get-tuple-element.48), channel_id=1, source_target_pairs={{0,2},{1,31},{2,4},{3,1},{4,6},{5,3},{6,8},{7,5},{8,10},{9,7},{10,... | collective-permute-start | bytes 196616 | tf_op jit(solution)/shard_map/ppermute | solution.py:204
  42.2 7.3 %collective-permute-start.4 = (bf16[16,2048]{1,0:T(8,128)(2,1)S(1)}, bf16[16,2048]{1,0:T(8,128)(2,1)S(1)}, u32[]{:S(2)}, u32[]{:S(2)}) collective-permute-start(bf16[16,2048]{1,0:T(8,128)(2,1)S(1)} %get-tuple-element.49), channel_id=1, source_target_pairs={{0,30},{1,3},{2,0},{3,5},{4,2},{5,7},{6,4},{7,9},{8,6},{9,11},{10,... | collective-permute-start | bytes 196616 | tf_op jit(solution)/shard_map/ppermute | solution.py:204
  43.2 13.8 %collective-permute-start.22 = (bf16[16,2048]{1,0:T(8,128)(2,1)S(1)}, bf16[16,2048]{1,0:T(8,128)(2,1)S(1)}, u32[]{:S(2)}, u32[]{:S(2)}) collective-permute-start(bf16[16,2048]{1,0:T(8,128)(2,1)S(1)} %get-tuple-element.71), channel_id=1, source_target_pairs={{0,4},{1,29},{2,6},{3,31},{4,8},{5,1},{6,10},{7,3},{8,12},{9,5},{1... | collective-permute-start | bytes 196616 | tf_op jit(solution)/shard_map/ppermute | solution.py:204
  44.5 16.8 %collective-permute-start.23 = (bf16[16,2048]{1,0:T(8,128)(2,1)S(1)}, bf16[16,2048]{1,0:T(8,128)(2,1)S(1)}, u32[]{:S(2)}, u32[]{:S(2)}) collective-permute-start(bf16[16,2048]{1,0:T(8,128)(2,1)S(1)} %get-tuple-element.72), channel_id=1, source_target_pairs={{0,28},{1,5},{2,30},{3,7},{4,0},{5,9},{6,2},{7,11},{8,4},{9,13},{1... | collective-permute-start | bytes 196616 | tf_op jit(solution)/shard_map/ppermute | solution.py:204
  45.7 15.7 %collective-permute-start.24 = (bf16[16,2048]{1,0:T(8,128)(2,1)S(1)}, bf16[16,2048]{1,0:T(8,128)(2,1)S(1)}, u32[]{:S(2)}, u32[]{:S(2)}) collective-permute-start(bf16[16,2048]{1,0:T(8,128)(2,1)S(1)} %get-tuple-element.73), channel_id=1, source_target_pairs={{0,2},{1,31},{2,4},{3,1},{4,6},{5,3},{6,8},{7,5},{8,10},{9,7},{10,... | collective-permute-start | bytes 196616 | tf_op jit(solution)/shard_map/ppermute | solution.py:204
  49.5 12.2 %collective-permute-start.25 = (bf16[16,2048]{1,0:T(8,128)(2,1)S(1)}, bf16[16,2048]{1,0:T(8,128)(2,1)S(1)}, u32[]{:S(2)}, u32[]{:S(2)}) collective-permute-start(bf16[16,2048]{1,0:T(8,128)(2,1)S(1)} %get-tuple-element.74), channel_id=1, source_target_pairs={{0,30},{1,3},{2,0},{3,5},{4,2},{5,7},{6,4},{7,9},{8,6},{9,11},{10,... | collective-permute-start | bytes 196616 | tf_op jit(solution)/shard_map/ppermute | solution.py:204
  49.6 5.2 %collective-permute-start.26 = (bf16[8,2048]{1,0:T(8,128)(2,1)S(1)}, bf16[8,2048]{1,0:T(8,128)(2,1)S(1)}, u32[]{:S(2)}, u32[]{:S(2)}) collective-permute-start(bf16[8,2048]{1,0:T(8,128)(2,1)S(1)} %get-tuple-element.76), channel_id=1, source_target_pairs={{0,6},{1,27},{2,8},{3,29},{4,10},{5,31},{6,12},{7,1},{8,14},{9,3},... | collective-permute-start | bytes 98312 | tf_op jit(solution)/shard_map/ppermute | solution.py:204
  54.8 13.6 %collective-permute-start.11 = (bf16[8,2048]{1,0:T(8,128)(2,1)S(1)}, bf16[8,2048]{1,0:T(8,128)(2,1)S(1)}, u32[]{:S(2)}, u32[]{:S(2)}) collective-permute-start(bf16[8,2048]{1,0:T(8,128)(2,1)S(1)} %get-tuple-element.56), channel_id=1, source_target_pairs={{0,6},{1,27},{2,8},{3,29},{4,10},{5,31},{6,12},{7,1},{8,14},{9,3},... | collective-permute-start | bytes 98312 | tf_op jit(solution)/shard_map/ppermute | solution.py:204
  57.0 13.5 %collective-permute-start.7 = (bf16[16,2048]{1,0:T(8,128)(2,1)S(1)}, bf16[16,2048]{1,0:T(8,128)(2,1)S(1)}, u32[]{:S(2)}, u32[]{:S(2)}) collective-permute-start(bf16[16,2048]{1,0:T(8,128)(2,1)S(1)} %get-tuple-element.51), channel_id=1, source_target_pairs={{0,4},{1,29},{2,6},{3,31},{4,8},{5,1},{6,10},{7,3},{8,12},{9,5},{1... | collective-permute-start | bytes 196616 | tf_op jit(solution)/shard_map/ppermute | solution.py:204
  61.3 9.6 %collective-permute-start.8 = (bf16[16,2048]{1,0:T(8,128)(2,1)S(1)}, bf16[16,2048]{1,0:T(8,128)(2,1)S(1)}, u32[]{:S(2)}, u32[]{:S(2)}) collective-permute-start(bf16[16,2048]{1,0:T(8,128)(2,1)S(1)} %get-tuple-element.52), channel_id=1, source_target_pairs={{0,28},{1,5},{2,30},{3,7},{4,0},{5,9},{6,2},{7,11},{8,4},{9,13},{1... | collective-permute-start | bytes 196616 | tf_op jit(solution)/shard_map/ppermute | solution.py:204
  61.3 12.8 %collective-permute-start.9 = (bf16[16,2048]{1,0:T(8,128)(2,1)S(1)}, bf16[16,2048]{1,0:T(8,128)(2,1)S(1)}, u32[]{:S(2)}, u32[]{:S(2)}) collective-permute-start(bf16[16,2048]{1,0:T(8,128)(2,1)S(1)} %get-tuple-element.53), channel_id=1, source_target_pairs={{0,2},{1,31},{2,4},{3,1},{4,6},{5,3},{6,8},{7,5},{8,10},{9,7},{10,... | collective-permute-start | bytes 196616 | tf_op jit(solution)/shard_map/ppermute | solution.py:204
  61.7 12.7 %collective-permute-start.10 = (bf16[16,2048]{1,0:T(8,128)(2,1)S(1)}, bf16[16,2048]{1,0:T(8,128)(2,1)S(1)}, u32[]{:S(2)}, u32[]{:S(2)}) collective-permute-start(bf16[16,2048]{1,0:T(8,128)(2,1)S(1)} %get-tuple-element.54), channel_id=1, source_target_pairs={{0,30},{1,3},{2,0},{3,5},{4,2},{5,7},{6,4},{7,9},{8,6},{9,11},{10,... | collective-permute-start | bytes 196616 | tf_op jit(solution)/shard_map/ppermute | solution.py:204
  68.4 12.6 %collective-permute-start.31 = (bf16[8,2048]{1,0:T(8,128)(2,1)S(1)}, bf16[8,2048]{1,0:T(8,128)(2,1)S(1)}, u32[]{:S(2)}, u32[]{:S(2)}) collective-permute-start(bf16[8,2048]{1,0:T(8,128)(2,1)S(1)} %get-tuple-element.82), channel_id=1, source_target_pairs={{0,26},{1,7},{2,28},{3,9},{4,30},{5,11},{6,0},{7,13},{8,2},{9,15},... | collective-permute-start | bytes 98312 | tf_op jit(solution)/shard_map/ppermute | solution.py:204
  70.5 14.1 %collective-permute-start.27 = (bf16[16,2048]{1,0:T(8,128)(2,1)S(1)}, bf16[16,2048]{1,0:T(8,128)(2,1)S(1)}, u32[]{:S(2)}, u32[]{:S(2)}) collective-permute-start(bf16[16,2048]{1,0:T(8,128)(2,1)S(1)} %get-tuple-element.77), channel_id=1, source_target_pairs={{0,28},{1,5},{2,30},{3,7},{4,0},{5,9},{6,2},{7,11},{8,4},{9,13},{1... | collective-permute-start | bytes 196616 | tf_op jit(solution)/shard_map/ppermute | solution.py:204
  70.9 13.7 %collective-permute-start.28 = (bf16[16,2048]{1,0:T(8,128)(2,1)S(1)}, bf16[16,2048]{1,0:T(8,128)(2,1)S(1)}, u32[]{:S(2)}, u32[]{:S(2)}) collective-permute-start(bf16[16,2048]{1,0:T(8,128)(2,1)S(1)} %get-tuple-element.78), channel_id=1, source_target_pairs={{0,4},{1,29},{2,6},{3,31},{4,8},{5,1},{6,10},{7,3},{8,12},{9,5},{1... | collective-permute-start | bytes 196616 | tf_op jit(solution)/shard_map/ppermute | solution.py:204
  74.1 13.2 %collective-permute-start.29 = (bf16[16,2048]{1,0:T(8,128)(2,1)S(1)}, bf16[16,2048]{1,0:T(8,128)(2,1)S(1)}, u32[]{:S(2)}, u32[]{:S(2)}) collective-permute-start(bf16[16,2048]{1,0:T(8,128)(2,1)S(1)} %get-tuple-element.79), channel_id=1, source_target_pairs={{0,30},{1,3},{2,0},{3,5},{4,2},{5,7},{6,4},{7,9},{8,6},{9,11},{10,... | collective-permute-start | bytes 196616 | tf_op jit(solution)/shard_map/ppermute | solution.py:204
  80.9 24.5 %collective-permute-start.12 = (bf16[32,2048]{1,0:T(8,128)(2,1)S(1)}, bf16[32,2048]{1,0:T(8,128)(2,1)S(1)}, u32[]{:S(2)}, u32[]{:S(2)}) collective-permute-start(bf16[32,2048]{1,0:T(8,128)(2,1)S(1)} %get-tuple-element.57), channel_id=1, source_target_pairs={{0,28},{1,5},{2,30},{3,7},{4,0},{5,9},{6,2},{7,11},{8,4},{9,13},{1... | collective-permute-start | bytes 393224 | tf_op jit(solution)/shard_map/ppermute | solution.py:204
  81.0 24.3 %collective-permute-start.13 = (bf16[32,2048]{1,0:T(8,128)(2,1)S(1)}, bf16[32,2048]{1,0:T(8,128)(2,1)S(1)}, u32[]{:S(2)}, u32[]{:S(2)}) collective-permute-start(bf16[32,2048]{1,0:T(8,128)(2,1)S(1)} %get-tuple-element.58), channel_id=1, source_target_pairs={{0,4},{1,29},{2,6},{3,31},{4,8},{5,1},{6,10},{7,3},{8,12},{9,5},{1... | collective-permute-start | bytes 393224 | tf_op jit(solution)/shard_map/ppermute | solution.py:204
  84.6 20.8 %collective-permute-start.14 = (bf16[32,2048]{1,0:T(8,128)(2,1)S(1)}, bf16[32,2048]{1,0:T(8,128)(2,1)S(1)}, u32[]{:S(2)}, u32[]{:S(2)}) collective-permute-start(bf16[32,2048]{1,0:T(8,128)(2,1)S(1)} %get-tuple-element.59), channel_id=1, source_target_pairs={{0,30},{1,3},{2,0},{3,5},{4,2},{5,7},{6,4},{7,9},{8,6},{9,11},{10,... | collective-permute-start | bytes 393224 | tf_op jit(solution)/shard_map/ppermute | solution.py:204
  84.6 20.7 %collective-permute-start.15 = (bf16[32,2048]{1,0:T(8,128)(2,1)S(1)}, bf16[32,2048]{1,0:T(8,128)(2,1)S(1)}, u32[]{:S(2)}, u32[]{:S(2)}) collective-permute-start(bf16[32,2048]{1,0:T(8,128)(2,1)S(1)} %get-tuple-element.60), channel_id=1, source_target_pairs={{0,2},{1,31},{2,4},{3,1},{4,6},{5,3},{6,8},{7,5},{8,10},{9,7},{10,... | collective-permute-start | bytes 393224 | tf_op jit(solution)/shard_map/ppermute | solution.py:204
  87.2 3.9 %collective-permute-start.30 = (bf16[16,2048]{1,0:T(8,128)(2,1)S(1)}, bf16[16,2048]{1,0:T(8,128)(2,1)S(1)}, u32[]{:S(2)}, u32[]{:S(2)}) collective-permute-start(bf16[16,2048]{1,0:T(8,128)(2,1)S(1)} %get-tuple-element.80), channel_id=1, source_target_pairs={{0,2},{1,31},{2,4},{3,1},{4,6},{5,3},{6,8},{7,5},{8,10},{9,7},{10,... | collective-permute-start | bytes 196616 | tf_op jit(solution)/shard_map/ppermute | solution.py:204
  91.1 6.2 %collective-permute-start.16 = (bf16[8,2048]{1,0:T(8,128)(2,1)S(1)}, bf16[8,2048]{1,0:T(8,128)(2,1)S(1)}, u32[]{:S(2)}, u32[]{:S(2)}) collective-permute-start(bf16[8,2048]{1,0:T(8,128)(2,1)S(1)} %get-tuple-element.62), channel_id=1, source_target_pairs={{0,26},{1,7},{2,28},{3,9},{4,30},{5,11},{6,0},{7,13},{8,2},{9,15},... | collective-permute-start | bytes 98312 | tf_op jit(solution)/shard_map/ppermute | solution.py:204
  97.3 9.1 %collective-permute-start.32 = (bf16[32,2048]{1,0:T(8,128)(2,1)S(1)}, bf16[32,2048]{1,0:T(8,128)(2,1)S(1)}, u32[]{:S(2)}, u32[]{:S(2)}) collective-permute-start(bf16[32,2048]{1,0:T(8,128)(2,1)S(1)} %get-tuple-element.86), channel_id=1, source_target_pairs={{0,1},{1,0},{2,3},{3,2},{4,5},{5,4},{6,7},{7,6},{8,9},{9,8},{10,11... | collective-permute-start | bytes 393224 | tf_op jit(solution)/shard_map/ppermute | solution.py:207
  105.8 4.7 %collective-permute-start.18 = (bf16[32,2048]{1,0:T(8,128)(2,1)S(1)}, bf16[32,2048]{1,0:T(8,128)(2,1)S(1)}, u32[]{:S(2)}, u32[]{:S(2)}) collective-permute-start(bf16[32,2048]{1,0:T(8,128)(2,1)S(1)} %get-tuple-element.70), channel_id=1, source_target_pairs={{0,1},{1,0},{2,3},{3,2},{4,5},{5,4},{6,7},{7,6},{8,9},{9,8},{10,11... | collective-permute-start | bytes 393224 | tf_op jit(solution)/shard_map/ppermute | solution.py:207
  105.9 7.0 %collective-permute-start.17 = (bf16[32,2048]{1,0:T(8,128)(2,1)S(1)}, bf16[32,2048]{1,0:T(8,128)(2,1)S(1)}, u32[]{:S(2)}, u32[]{:S(2)}) collective-permute-start(bf16[32,2048]{1,0:T(8,128)(2,1)S(1)} %get-tuple-element.68), channel_id=1, source_target_pairs={{0,1},{1,0},{2,3},{3,2},{4,5},{5,4},{6,7},{7,6},{8,9},{9,8},{10,11... | collective-permute-start | bytes 393224 | tf_op jit(solution)/shard_map/ppermute | solution.py:207
  106.4 19.6 %collective-permute-start.33 = (bf16[32,2048]{1,0:T(8,128)(2,1)S(1)}, bf16[32,2048]{1,0:T(8,128)(2,1)S(1)}, u32[]{:S(2)}, u32[]{:S(2)}) collective-permute-start(bf16[32,2048]{1,0:T(8,128)(2,1)S(1)} %shard_map.82), channel_id=1, source_target_pairs={{0,10},{1,23},{2,12},{3,25},{4,14},{5,27},{6,16},{7,29},{8,18},{9,... | collective-permute-start | bytes 393224 | tf_op jit(solution)/shard_map/ppermute | solution.py:204
  110.5 18.5 %collective-permute-start.19 = (bf16[32,2048]{1,0:T(8,128)(2,1)S(1)}, bf16[32,2048]{1,0:T(8,128)(2,1)S(1)}, u32[]{:S(2)}, u32[]{:S(2)}) collective-permute-start(bf16[32,2048]{1,0:T(8,128)(2,1)S(1)} %shard_map.78), channel_id=1, source_target_pairs={{0,22},{1,11},{2,24},{3,13},{4,26},{5,15},{6,28},{7,17},{8,30},{9,... | collective-permute-start | bytes 393224 | tf_op jit(solution)/shard_map/ppermute | solution.py:204

commit v8 on v6

--- a/solution.py
+++ b/solution.py
@@ -236,6 +236,12 @@
     high2, low2 = swap(low), swap(high)
     steps = (*NEAR, 3)
 
+    def spread(blocks, sign):
+        moved = []
+        for b, d in zip(blocks, steps):
+            moved.append(shift(b, sign * d) if d else b)
+        return moved
+
     def hand(sources, sizes, flops):
         count = len(sources)
         weight = bf16(count * rows, sum(sizes))
@@ -247,7 +253,7 @@
             scratch=[pltpu.VMEM((count * rows, width + META), jnp.bfloat16)],
             flops=flops,
         )(place, *sources)
-        return [shift(b, d) if d else b for b, d in zip(blocks, steps)], (w_high, w_low)
+        return spread(blocks, 1), (w_high, w_low)
 
     def run(blocks, carried=()):
         slots = sum(b.shape[0] for b in blocks)
@@ -255,7 +261,7 @@
         for i, b in enumerate(carried):
             sizes[EARLY + i] += b.shape[0]
         experts_of = call(
-            functools.partial(experts, 256, len(blocks), len(carried)),
+            functools.partial(experts, hidden // 2, len(blocks), len(carried)),
             [bf16(n, width) for n in sizes],
             len(blocks) + len(carried) + 3,
             scratch=[pltpu.VMEM((slots, width), jnp.bfloat16), pltpu.VMEM((slots, width), jnp.float32)],
@@ -264,7 +270,7 @@
         return experts_of(*blocks, *carried, w_gate[0], w_up[0], w_down[0])
 
     def back(blocks):
-        return [shift(b, -d) if d else b for b, d in zip(blocks, steps)]
+        return spread(blocks, -1)
 
     heavy = 24 * 256 * width * hidden
     near, near_weights = hand((own, own2), [2 * cap] * 5, heavy)

time: 110 us -> 109 us (level)
  Pallas kernels: 16.8 us -> 14.3 us
  waiting for transfers between devices: 39.6 us -> 41.3 us
    pallas_call x2, Pallas kernels: 11.9 us -> 9.38 us  [run(): return experts_of(*blocks, *carried, w_gate[0], w_up[0], w_down[0])]
    ppermute x20, waiting for transfers between devices: 38.5 us -> 40.3 us  [shift(): return lax.ppermute(x, ('z', 'c'), pairs)]
  transfers between devices with their start and end apart: 25 -> 25, of which waited for: 8 -> 8; matrix products, arithmetic and copies ran while one was open for 0% -> 0% of each run, Pallas kernels for 13% -> 11%
where the time goes in v8:
time: 109 us; the launch traced here: 108 us
  starting transfers between devices  51.8 us (48%)
  waiting for transfers between devices  41.3 us (38%)
  Pallas kernels  14.3 us (13%)
    ppermute x20, starting transfers between devices, shift(): return lax.ppermute(x, ('z', 'c'), pairs)  50.6 us
    ppermute x20, waiting for transfers between devices, shift(): return lax.ppermute(x, ('z', 'c'), pairs)  40.3 us
    pallas_call x2, Pallas kernels, run(): return experts_of(*blocks, *carried, w_gate[0], w_up[0], w_down[0])  9.38 us
  transfers between devices with their start and end apart: 25, of which 8 were waited for; matrix products, arithmetic and copies ran while one was open for 0% of the time, Pallas kernels for 11%

profile of v8, /device:TPU:86, one launch (start us, length us, event | category | flops | bytes accessed | tf_op | source)
XLA Modules:
  0.0 107.7 jit_solution(17796531879120343549)
XLA Ops:
  0.0 1.5 %shard_map.73.refs_0_ = bf16[32,2176]{1,0:T(8,128)(2,1)S(1)} custom-call(bf16[32,2048]{1,0:T(8,128)(2,1)} %tok_hbm.1, f32[1,2048]{1,0:T(1,128)} %bitcast.20, s32[4,32]{1,0:T(4,128)} %bitcast.21, f32[4,32]{1,0:T(4,128)} %bitcast.22), custom_call_target="tpu_custom_call" | custom-call | flops 1048576 | bytes 1048576 | tf_op jit(solution)/shard_map/pallas_call | solution.py:219
  1.5 14.8 %collective-permute-start.8 = (bf16[32,2176]{1,0:T(8,128)(2,1)S(1)}, bf16[32,2176]{1,0:T(8,128)(2,1)S(1)}, u32[]{:S(2)}, u32[]{:S(2)}) collective-permute-start(bf16[32,2176]{1,0:T(8,128)(2,1)S(1)} %shard_map.73.refs_0_), channel_id=1, source_target_pairs={{0,22},{1,11},{2,24},{3,13},{4,26},{5,15},{6,28},{7,17},{8,30},{9,... | collective-permute-start | bytes 417800 | tf_op jit(solution)/shard_map/ppermute | solution.py:213
  16.3 0.0 collective-permute-start.7
  16.3 0.0 collective-permute-start
  16.3 0.0 slice-start.2
  16.3 0.0 slice-start.4
  16.4 0.1 pad_add_fusion.place_ref
  16.4 14.5 %collective-permute-done.8.refs_2_ = bf16[32,2176]{1,0:T(8,128)(2,1)S(1)} collective-permute-done((bf16[32,2176]{1,0:T(8,128)(2,1)S(1)}, bf16[32,2176]{1,0:T(8,128)(2,1)S(1)}, u32[]{:S(2)}, u32[]{:S(2)}) %collective-permute-start.8) | collective-permute-done | bytes 139296 | tf_op jit(solution)/shard_map/ppermute | solution.py:213
  31.0 0.0 collective-permute-start.9
  31.0 0.0 collective-permute-done.7.refs_0_
  31.0 0.5 collective-permute-start.10
  31.5 0.0 collective-permute-done.refs_1_
  31.5 0.9 shard_map.74
  32.4 0.1 collective-permute-start.1
  32.5 4.1 %collective-permute-start.2 = (bf16[16,2048]{1,0:T(8,128)(2,1)S(1)}, bf16[16,2048]{1,0:T(8,128)(2,1)S(1)}, u32[]{:S(2)}, u32[]{:S(2)}) collective-permute-start(bf16[16,2048]{1,0:T(8,128)(2,1)S(1)} %get-tuple-element.38), channel_id=1, source_target_pairs={{0,28},{1,5},{2,30},{3,7},{4,0},{5,9},{6,2},{7,11},{8,4},{9,13},{1... | collective-permute-start | bytes 196616 | tf_op jit(solution)/shard_map/ppermute | solution.py:213
  36.7 2.4 %collective-permute-start.3 = (bf16[16,2048]{1,0:T(8,128)(2,1)S(1)}, bf16[16,2048]{1,0:T(8,128)(2,1)S(1)}, u32[]{:S(2)}, u32[]{:S(2)}) collective-permute-start(bf16[16,2048]{1,0:T(8,128)(2,1)S(1)} %get-tuple-element.39), channel_id=1, source_target_pairs={{0,2},{1,31},{2,4},{3,1},{4,6},{5,3},{6,8},{7,5},{8,10},{9,7},{10,... | collective-permute-start | bytes 196616 | tf_op jit(solution)/shard_map/ppermute | solution.py:213
  39.1 0.0 collective-permute-done.9.refs_1_
  39.1 1.3 %collective-permute-start.4 = (bf16[16,2048]{1,0:T(8,128)(2,1)S(1)}, bf16[16,2048]{1,0:T(8,128)(2,1)S(1)}, u32[]{:S(2)}, u32[]{:S(2)}) collective-permute-start(bf16[16,2048]{1,0:T(8,128)(2,1)S(1)} %get-tuple-element.40), channel_id=1, source_target_pairs={{0,30},{1,3},{2,0},{3,5},{4,2},{5,7},{6,4},{7,9},{8,6},{9,11},{10,... | collective-permute-start | bytes 196616 | tf_op jit(solution)/shard_map/ppermute | solution.py:213
  40.4 0.0 collective-permute-done.10.refs_3_
  40.4 1.1 %shard_map.76 = (bf16[32,2048]{1,0:T(8,128)(2,1)S(1)}, bf16[32,2048]{1,0:T(8,128)(2,1)S(1)}, bf16[32,2048]{1,0:T(8,128)(2,1)S(1)}, bf16[32,2048]{1,0:T(8,128)(2,...) custom-call(s32[2]{0:T(128)S(1)} %pad_add_fusion.place_ref, ...), custom_call_target="tpu_custom_call" | custom-call | flops 268435456 | bytes 1048576 | tf_op jit(solution)/shard_map/pallas_call | solution.py:248
  41.6 1.0 collective-permute-start.15
  42.6 0.0 collective-permute-done.1.refs_0_
  42.6 1.5 %collective-permute-start.11 = (bf16[32,2048]{1,0:T(8,128)(2,1)S(1)}, bf16[32,2048]{1,0:T(8,128)(2,1)S(1)}, u32[]{:S(2)}, u32[]{:S(2)}) collective-permute-start(bf16[32,2048]{1,0:T(8,128)(2,1)S(1)} %get-tuple-element.44), channel_id=1, source_target_pairs={{0,4},{1,29},{2,6},{3,31},{4,8},{5,1},{6,10},{7,3},{8,12},{9,5},{1... | collective-permute-start | bytes 393224 | tf_op jit(solution)/shard_map/ppermute | solution.py:213
  44.0 0.0 collective-permute-done.2.refs_1_
  44.0 2.7 %collective-permute-start.12 = (bf16[32,2048]{1,0:T(8,128)(2,1)S(1)}, bf16[32,2048]{1,0:T(8,128)(2,1)S(1)}, u32[]{:S(2)}, u32[]{:S(2)}) collective-permute-start(bf16[32,2048]{1,0:T(8,128)(2,1)S(1)} %get-tuple-element.45), channel_id=1, source_target_pairs={{0,28},{1,5},{2,30},{3,7},{4,0},{5,9},{6,2},{7,11},{8,4},{9,13},{1... | collective-permute-start | bytes 393224 | tf_op jit(solution)/shard_map/ppermute | solution.py:213
  46.7 0.0 collective-permute-done.3.refs_2_
  46.7 3.2 %collective-permute-start.13 = (bf16[32,2048]{1,0:T(8,128)(2,1)S(1)}, bf16[32,2048]{1,0:T(8,128)(2,1)S(1)}, u32[]{:S(2)}, u32[]{:S(2)}) collective-permute-start(bf16[32,2048]{1,0:T(8,128)(2,1)S(1)} %get-tuple-element.46), channel_id=1, source_target_pairs={{0,2},{1,31},{2,4},{3,1},{4,6},{5,3},{6,8},{7,5},{8,10},{9,7},{10,... | collective-permute-start | bytes 393224 | tf_op jit(solution)/shard_map/ppermute | solution.py:213
  49.9 0.0 collective-permute-done.4.refs_3_
  49.9 0.0 collective-permute-start.14
  50.0 0.0 slice-done
  50.0 0.0 slice-done.2
  50.0 0.0 slice-done.4
  50.0 0.0 slice-done.1
  50.0 4.2 %shard_map.75 = (bf16[16,2048]{1,0:T(8,128)(2,1)S(1)}, bf16[16,2048]{1,0:T(8,128)(2,1)S(1)}, bf16[16,2048]{1,0:T(8,128)(2,1)S(1)}, bf16[16,2048]{1,0:T(8,128)(2,1)S(1)}, bf16[16,2048]{1,0:T(8,128)(2,1)S(1)}) custom-call(bf16[16,2048]{1,0:T(8,128)(2,1)S(1)} %collective-permute-done.1.refs_0_, bf16[16,2048]{1,0:T(8,128)(2,1)S(1)} %collective-permute-done.2.refs_1_, ...), custom_call_target="tpu_custom_call" | custom-call | flops 1761607680 | bytes 1048576 | tf_op jit(solution)/shard_map/pallas_call | solution.py:270
  54.2 0.0 collective-permute-done.15.refs_5_
  54.2 1.7 %collective-permute-start.5 = (bf16[16,2048]{1,0:T(8,128)(2,1)S(1)}, bf16[16,2048]{1,0:T(8,128)(2,1)S(1)}, u32[]{:S(2)}, u32[]{:S(2)}) collective-permute-start(bf16[16,2048]{1,0:T(8,128)(2,1)S(1)} %get-tuple-element.42), channel_id=1, source_target_pairs={{0,28},{1,5},{2,30},{3,7},{4,0},{5,9},{6,2},{7,11},{8,4},{9,13},{1... | collective-permute-start | bytes 196616 | tf_op jit(solution)/shard_map/ppermute | solution.py:213
  55.9 0.0 collective-permute-done.11.refs_0_
  55.9 0.0 collective-permute-done.12.refs_1_
  55.9 2.1 %collective-permute-done.13.refs_2_ = bf16[32,2048]{1,0:T(8,128)(2,1)S(1)} collective-permute-done((bf16[32,2048]{1,0:T(8,128)(2,1)S(1)}, bf16[32,2048]{1,0:T(8,128)(2,1)S(1)}, u32[]{:S(2)}, u32[]{:S(2)}) %collective-permute-start.13) | collective-permute-done | bytes 131104 | tf_op jit(solution)/shard_map/ppermute | solution.py:213
  58.0 0.9 collective-permute-done.14.refs_3_
  58.9 5.2 %shard_map.77 = (bf16[32,2048]{1,0:T(8,128)(2,1)S(1)}, bf16[32,2048]{1,0:T(8,128)(2,1)S(1)}, bf16[48,2048]{1,0:T(8,128)(2,1)S(1)}, bf16[48,2048]{1,0:T(8,128)(2,...) custom-call(bf16[32,2048]{1,0:T(8,128)(2,1)S(1)} %collective-permute-done.11.refs_0_, ...), custom_call_target="tpu_custom_call" | custom-call | flops 3875536896 | bytes 1048576 | tf_op jit(solution)/shard_map/pallas_call | solution.py:270
  64.1 1.6 %collective-permute-start.18 = (bf16[48,2048]{1,0:T(8,128)(2,1)S(1)}, bf16[48,2048]{1,0:T(8,128)(2,1)S(1)}, u32[]{:S(2)}, u32[]{:S(2)}) collective-permute-start(bf16[48,2048]{1,0:T(8,128)(2,1)S(1)} %get-tuple-element.55), channel_id=1, source_target_pairs={{0,30},{1,3},{2,0},{3,5},{4,2},{5,7},{6,4},{7,9},{8,6},{9,11},{10,... | collective-permute-start | bytes 589832 | tf_op jit(solution)/shard_map/ppermute | solution.py:213
  65.6 0.5 collective-permute-start.19
  66.2 0.0 collective-permute-start.6
  66.2 4.1 %collective-permute-start.16 = (bf16[32,2048]{1,0:T(8,128)(2,1)S(1)}, bf16[32,2048]{1,0:T(8,128)(2,1)S(1)}, u32[]{:S(2)}, u32[]{:S(2)}) collective-permute-start(bf16[32,2048]{1,0:T(8,128)(2,1)S(1)} %get-tuple-element.53), channel_id=1, source_target_pairs={{0,28},{1,5},{2,30},{3,7},{4,0},{5,9},{6,2},{7,11},{8,4},{9,13},{1... | collective-permute-start | bytes 393224 | tf_op jit(solution)/shard_map/ppermute | solution.py:213
  70.3 0.0 collective-permute-done.5.refs_0_
  70.3 0.0 collective-permute-start.17
  70.3 5.5 %collective-permute-done.6.refs_1_ = bf16[16,2048]{1,0:T(8,128)(2,1)S(1)} collective-permute-done((bf16[16,2048]{1,0:T(8,128)(2,1)S(1)}, bf16[16,2048]{1,0:T(8,128)(2,1)S(1)}, u32[]{:S(2)}, u32[]{:S(2)}) %collective-permute-start.6) | collective-permute-done | bytes 65568 | tf_op jit(solution)/shard_map/ppermute | solution.py:213
  75.9 4.6 %collective-permute-start.20 = (bf16[16,2048]{1,0:T(8,128)(2,1)S(1)}, bf16[16,2048]{1,0:T(8,128)(2,1)S(1)}, u32[]{:S(2)}, u32[]{:S(2)}) collective-permute-start(bf16[16,2048]{1,0:T(8,128)(2,1)S(1)} %get-tuple-element.58), channel_id=1, source_target_pairs={{0,26},{1,7},{2,28},{3,9},{4,30},{5,11},{6,0},{7,13},{8,2},{9,15},... | collective-permute-start | bytes 196616 | tf_op jit(solution)/shard_map/ppermute | solution.py:213
  80.4 1.9 %collective-permute-done.20.refs_7_ = bf16[16,2048]{1,0:T(8,128)(2,1)S(1)} collective-permute-done((bf16[16,2048]{1,0:T(8,128)(2,1)S(1)}, bf16[16,2048]{1,0:T(8,128)(2,1)S(1)}, u32[]{:S(2)}, u32[]{:S(2)}) %collective-permute-start.20) | collective-permute-done | bytes 65568 | tf_op jit(solution)/shard_map/ppermute | solution.py:213
  82.3 0.0 collective-permute-done.16.refs_2_
  82.4 0.0 collective-permute-done.17.refs_3_
  82.4 0.0 collective-permute-done.18.refs_4_
  82.4 0.0 collective-permute-done.19.refs_5_
  82.4 0.6 shard_map.78
  83.0 0.1 collective-permute-start.22
  83.1 0.5 collective-permute-start.21
  83.6 1.0 collective-permute-done.22.other
  84.7 5.5 %collective-permute-start.23 = (bf16[32,2048]{1,0:T(8,128)(2,1)S(1)}, bf16[32,2048]{1,0:T(8,128)(2,1)S(1)}, u32[]{:S(2)}, u32[]{:S(2)}) collective-permute-start(bf16[32,2048]{1,0:T(8,128)(2,1)S(1)} %get-tuple-element.67), channel_id=1, source_target_pairs={{0,22},{1,11},{2,24},{3,13},{4,26},{5,15},{6,28},{7,17},{8,30},{9,... | collective-permute-start | bytes 393224 | tf_op jit(solution)/shard_map/ppermute | solution.py:213
  90.2 1.4 %collective-permute-start.24 = (bf16[32,2048]{1,0:T(8,128)(2,1)S(1)}, bf16[32,2048]{1,0:T(8,128)(2,1)S(1)}, u32[]{:S(2)}, u32[]{:S(2)}) collective-permute-start(bf16[32,2048]{1,0:T(8,128)(2,1)S(1)} %get-tuple-element.68), channel_id=1, source_target_pairs={{0,10},{1,23},{2,12},{3,25},{4,14},{5,27},{6,16},{7,29},{8,18},{9,... | collective-permute-start | bytes 393224 | tf_op jit(solution)/shard_map/ppermute | solution.py:213
  91.6 0.0 collective-permute-done.21.other
  91.6 3.1 %collective-permute-done.23.one = bf16[32,2048]{1,0:T(8,128)(2,1)S(1)} collective-permute-done((bf16[32,2048]{1,0:T(8,128)(2,1)S(1)}, bf16[32,2048]{1,0:T(8,128)(2,1)S(1)}, u32[]{:S(2)}, u32[]{:S(2)}) %collective-permute-start.23) | collective-permute-done | bytes 131104 | tf_op jit(solution)/shard_map/ppermute | solution.py:213
  94.7 12.2 %collective-permute-done.24.two = bf16[32,2048]{1,0:T(8,128)(2,1)S(1)} collective-permute-done((bf16[32,2048]{1,0:T(8,128)(2,1)S(1)}, bf16[32,2048]{1,0:T(8,128)(2,1)S(1)}, u32[]{:S(2)}, u32[]{:S(2)}) %collective-permute-start.24) | collective-permute-done | bytes 131104 | tf_op jit(solution)/shard_map/ppermute | solution.py:213
  106.9 0.7 shard_map.80
  (10 shorter events, 0.1 us)
Async XLA Ops:
  1.5 29.5 %collective-permute-start.8 = (bf16[32,2176]{1,0:T(8,128)(2,1)S(1)}, bf16[32,2176]{1,0:T(8,128)(2,1)S(1)}, u32[]{:S(2)}, u32[]{:S(2)}) collective-permute-start(bf16[32,2176]{1,0:T(8,128)(2,1)S(1)} %shard_map.73.refs_0_), channel_id=1, source_target_pairs={{0,22},{1,11},{2,24},{3,13},{4,26},{5,15},{6,28},{7,17},{8,30},{9,... | collective-permute-start | bytes 417800 | tf_op jit(solution)/shard_map/ppermute | solution.py:213
  16.3 14.7 %collective-permute-start.7 = (bf16[32,2176]{1,0:T(8,128)(2,1)S(1)}, bf16[32,2176]{1,0:T(8,128)(2,1)S(1)}, u32[]{:S(2)}, u32[]{:S(2)}) collective-permute-start(bf16[32,2176]{1,0:T(8,128)(2,1)S(1)} %shard_map.73.refs_0_), channel_id=1, source_target_pairs={{0,10},{1,23},{2,12},{3,25},{4,14},{5,27},{6,16},{7,29},{8,18},{9,... | collective-permute-start | bytes 417800 | tf_op jit(solution)/shard_map/ppermute | solution.py:213
  16.3 15.2 %collective-permute-start = (bf16[32,2176]{1,0:T(8,128)(2,1)S(1)}, bf16[32,2176]{1,0:T(8,128)(2,1)S(1)}, u32[]{:S(2)}, u32[]{:S(2)}) collective-permute-start(bf16[32,2176]{1,0:T(8,128)(2,1)S(1)} %shard_map.73.refs_0_), channel_id=1, source_target_pairs={{0,1},{1,0},{2,3},{3,2},{4,5},{5,4},{6,7},{7,6},{8,9},{9,8},{10,11... | collective-permute-start | bytes 417800 | tf_op jit(solution)/shard_map/ppermute | solution.py:216
  16.3 33.6 %slice-start = ((s8[7340032]{0:T(1024)(128)(4,1)}), s8[4194304]{0:T(1024)(128)(4,1)S(1)}, s32[]{:S(2)}) async-start(s8[7340032]{0:T(1024)(128)(4,1)} %bitcast.8), calls=%async_computation | async-start | bytes 8388608
  16.3 33.6 %slice-start.2 = ((s8[7340032]{0:T(1024)(128)(4,1)}), s8[4194304]{0:T(1024)(128)(4,1)S(1)}, s32[]{:S(2)}) async-start(s8[7340032]{0:T(1024)(128)(4,1)} %bitcast.12), calls=%async_computation.2 | async-start | bytes 8388608
  16.3 33.6 %slice-start.4 = ((s8[7340032]{0:T(1024)(128)(4,1)}), s8[4194304]{0:T(1024)(128)(4,1)S(1)}, s32[]{:S(2)}) async-start(s8[7340032]{0:T(1024)(128)(4,1)} %bitcast.16), calls=%async_computation.4 | async-start | bytes 8388608
  16.4 33.5 %slice-start.1 = ((s8[7340032]{0:T(1024)(128)(4,1)}), s8[3145728]{0:T(1024)(128)(4,1)S(1)}, s32[]{:S(2)}) async-start(s8[7340032]{0:T(1024)(128)(4,1)} %bitcast.8), calls=%async_computation.1 | async-start | bytes 6291456
  16.4 33.6 %slice-start.3 = ((s8[7340032]{0:T(1024)(128)(4,1)}), s8[3145728]{0:T(1024)(128)(4,1)S(1)}, s32[]{:S(2)}) async-start(s8[7340032]{0:T(1024)(128)(4,1)} %bitcast.12), calls=%async_computation.3 | async-start | bytes 6291456
  16.4 33.6 %slice-start.5 = ((s8[7340032]{0:T(1024)(128)(4,1)}), s8[3145728]{0:T(1024)(128)(4,1)S(1)}, s32[]{:S(2)}) async-start(s8[7340032]{0:T(1024)(128)(4,1)} %bitcast.16), calls=%async_computation.5 | async-start | bytes 6291456
  31.0 8.1 %collective-permute-start.9 = (bf16[32,2176]{1,0:T(8,128)(2,1)S(1)}, bf16[32,2176]{1,0:T(8,128)(2,1)S(1)}, u32[]{:S(2)}, u32[]{:S(2)}) collective-permute-start(bf16[32,2176]{1,0:T(8,128)(2,1)S(1)} %collective-permute-done.8.refs_2_), channel_id=1, source_target_pairs={{0,1},{1,0},{2,3},{3,2},{4,5},{5,4},{6,7},{7,6},{8,9},{9,8},{10,11... | collective-permute-start | bytes 417800 | tf_op jit(solution)/shard_map/ppermute | solution.py:216
  31.0 9.5 %collective-permute-start.10 = (bf16[32,2176]{1,0:T(8,128)(2,1)S(1)}, bf16[32,2176]{1,0:T(8,128)(2,1)S(1)}, u32[]{:S(2)}, u32[]{:S(2)}) collective-permute-start(bf16[32,2176]{1,0:T(8,128)(2,1)S(1)} %collective-permute-done.7.refs_0_), channel_id=1, source_target_pairs={{0,1},{1,0},{2,3},{3,2},{4,5},{5,4},{6,7},{7,6},{8,9},{9,8},{10,11... | collective-permute-start | bytes 417800 | tf_op jit(solution)/shard_map/ppermute | solution.py:216
  32.4 10.2 %collective-permute-start.1 = (bf16[16,2048]{1,0:T(8,128)(2,1)S(1)}, bf16[16,2048]{1,0:T(8,128)(2,1)S(1)}, u32[]{:S(2)}, u32[]{:S(2)}) collective-permute-start(bf16[16,2048]{1,0:T(8,128)(2,1)S(1)} %get-tuple-element.37), channel_id=1, source_target_pairs={{0,4},{1,29},{2,6},{3,31},{4,8},{5,1},{6,10},{7,3},{8,12},{9,5},{1... | collective-permute-start | bytes 196616 | tf_op jit(solution)/shard_map/ppermute | solution.py:213
  32.5 11.5 %collective-permute-start.2 = (bf16[16,2048]{1,0:T(8,128)(2,1)S(1)}, bf16[16,2048]{1,0:T(8,128)(2,1)S(1)}, u32[]{:S(2)}, u32[]{:S(2)}) collective-permute-start(bf16[16,2048]{1,0:T(8,128)(2,1)S(1)} %get-tuple-element.38), channel_id=1, source_target_pairs={{0,28},{1,5},{2,30},{3,7},{4,0},{5,9},{6,2},{7,11},{8,4},{9,13},{1... | collective-permute-start | bytes 196616 | tf_op jit(solution)/shard_map/ppermute | solution.py:213
  36.7 10.1 %collective-permute-start.3 = (bf16[16,2048]{1,0:T(8,128)(2,1)S(1)}, bf16[16,2048]{1,0:T(8,128)(2,1)S(1)}, u32[]{:S(2)}, u32[]{:S(2)}) collective-permute-start(bf16[16,2048]{1,0:T(8,128)(2,1)S(1)} %get-tuple-element.39), channel_id=1, source_target_pairs={{0,2},{1,31},{2,4},{3,1},{4,6},{5,3},{6,8},{7,5},{8,10},{9,7},{10,... | collective-permute-start | bytes 196616 | tf_op jit(solution)/shard_map/ppermute | solution.py:213
  39.1 10.9 %collective-permute-start.4 = (bf16[16,2048]{1,0:T(8,128)(2,1)S(1)}, bf16[16,2048]{1,0:T(8,128)(2,1)S(1)}, u32[]{:S(2)}, u32[]{:S(2)}) collective-permute-start(bf16[16,2048]{1,0:T(8,128)(2,1)S(1)} %get-tuple-element.40), channel_id=1, source_target_pairs={{0,30},{1,3},{2,0},{3,5},{4,2},{5,7},{6,4},{7,9},{8,6},{9,11},{10,... | collective-permute-start | bytes 196616 | tf_op jit(solution)/shard_map/ppermute | solution.py:213
  41.6 12.7 %collective-permute-start.15 = (bf16[16,2048]{1,0:T(8,128)(2,1)S(1)}, bf16[16,2048]{1,0:T(8,128)(2,1)S(1)}, u32[]{:S(2)}, u32[]{:S(2)}) collective-permute-start(bf16[16,2048]{1,0:T(8,128)(2,1)S(1)} %get-tuple-element.49), channel_id=1, source_target_pairs={{0,6},{1,27},{2,8},{3,29},{4,10},{5,31},{6,12},{7,1},{8,14},{9,3},... | collective-permute-start | bytes 196616 | tf_op jit(solution)/shard_map/ppermute | solution.py:213
  42.6 13.3 %collective-permute-start.11 = (bf16[32,2048]{1,0:T(8,128)(2,1)S(1)}, bf16[32,2048]{1,0:T(8,128)(2,1)S(1)}, u32[]{:S(2)}, u32[]{:S(2)}) collective-permute-start(bf16[32,2048]{1,0:T(8,128)(2,1)S(1)} %get-tuple-element.44), channel_id=1, source_target_pairs={{0,4},{1,29},{2,6},{3,31},{4,8},{5,1},{6,10},{7,3},{8,12},{9,5},{1... | collective-permute-start | bytes 393224 | tf_op jit(solution)/shard_map/ppermute | solution.py:213
  44.0 11.9 %collective-permute-start.12 = (bf16[32,2048]{1,0:T(8,128)(2,1)S(1)}, bf16[32,2048]{1,0:T(8,128)(2,1)S(1)}, u32[]{:S(2)}, u32[]{:S(2)}) collective-permute-start(bf16[32,2048]{1,0:T(8,128)(2,1)S(1)} %get-tuple-element.45), channel_id=1, source_target_pairs={{0,28},{1,5},{2,30},{3,7},{4,0},{5,9},{6,2},{7,11},{8,4},{9,13},{1... | collective-permute-start | bytes 393224 | tf_op jit(solution)/shard_map/ppermute | solution.py:213
  46.7 11.3 %collective-permute-start.13 = (bf16[32,2048]{1,0:T(8,128)(2,1)S(1)}, bf16[32,2048]{1,0:T(8,128)(2,1)S(1)}, u32[]{:S(2)}, u32[]{:S(2)}) collective-permute-start(bf16[32,2048]{1,0:T(8,128)(2,1)S(1)} %get-tuple-element.46), channel_id=1, source_target_pairs={{0,2},{1,31},{2,4},{3,1},{4,6},{5,3},{6,8},{7,5},{8,10},{9,7},{10,... | collective-permute-start | bytes 393224 | tf_op jit(solution)/shard_map/ppermute | solution.py:213
  49.9 8.9 %collective-permute-start.14 = (bf16[32,2048]{1,0:T(8,128)(2,1)S(1)}, bf16[32,2048]{1,0:T(8,128)(2,1)S(1)}, u32[]{:S(2)}, u32[]{:S(2)}) collective-permute-start(bf16[32,2048]{1,0:T(8,128)(2,1)S(1)} %get-tuple-element.47), channel_id=1, source_target_pairs={{0,30},{1,3},{2,0},{3,5},{4,2},{5,7},{6,4},{7,9},{8,6},{9,11},{10,... | collective-permute-start | bytes 393224 | tf_op jit(solution)/shard_map/ppermute | solution.py:213
  54.2 16.1 %collective-permute-start.5 = (bf16[16,2048]{1,0:T(8,128)(2,1)S(1)}, bf16[16,2048]{1,0:T(8,128)(2,1)S(1)}, u32[]{:S(2)}, u32[]{:S(2)}) collective-permute-start(bf16[16,2048]{1,0:T(8,128)(2,1)S(1)} %get-tuple-element.42), channel_id=1, source_target_pairs={{0,28},{1,5},{2,30},{3,7},{4,0},{5,9},{6,2},{7,11},{8,4},{9,13},{1... | collective-permute-start | bytes 196616 | tf_op jit(solution)/shard_map/ppermute | solution.py:213
  64.1 18.3 %collective-permute-start.18 = (bf16[48,2048]{1,0:T(8,128)(2,1)S(1)}, bf16[48,2048]{1,0:T(8,128)(2,1)S(1)}, u32[]{:S(2)}, u32[]{:S(2)}) collective-permute-start(bf16[48,2048]{1,0:T(8,128)(2,1)S(1)} %get-tuple-element.55), channel_id=1, source_target_pairs={{0,30},{1,3},{2,0},{3,5},{4,2},{5,7},{6,4},{7,9},{8,6},{9,11},{10,... | collective-permute-start | bytes 589832 | tf_op jit(solution)/shard_map/ppermute | solution.py:213
  65.6 16.7 %collective-permute-start.19 = (bf16[48,2048]{1,0:T(8,128)(2,1)S(1)}, bf16[48,2048]{1,0:T(8,128)(2,1)S(1)}, u32[]{:S(2)}, u32[]{:S(2)}) collective-permute-start(bf16[48,2048]{1,0:T(8,128)(2,1)S(1)} %get-tuple-element.56), channel_id=1, source_target_pairs={{0,2},{1,31},{2,4},{3,1},{4,6},{5,3},{6,8},{7,5},{8,10},{9,7},{10,... | collective-permute-start | bytes 589832 | tf_op jit(solution)/shard_map/ppermute | solution.py:213
  66.2 9.7 %collective-permute-start.6 = (bf16[16,2048]{1,0:T(8,128)(2,1)S(1)}, bf16[16,2048]{1,0:T(8,128)(2,1)S(1)}, u32[]{:S(2)}, u32[]{:S(2)}) collective-permute-start(bf16[16,2048]{1,0:T(8,128)(2,1)S(1)} %get-tuple-element.43), channel_id=1, source_target_pairs={{0,4},{1,29},{2,6},{3,31},{4,8},{5,1},{6,10},{7,3},{8,12},{9,5},{1... | collective-permute-start | bytes 196616 | tf_op jit(solution)/shard_map/ppermute | solution.py:213
  66.2 16.2 %collective-permute-start.16 = (bf16[32,2048]{1,0:T(8,128)(2,1)S(1)}, bf16[32,2048]{1,0:T(8,128)(2,1)S(1)}, u32[]{:S(2)}, u32[]{:S(2)}) collective-permute-start(bf16[32,2048]{1,0:T(8,128)(2,1)S(1)} %get-tuple-element.53), channel_id=1, source_target_pairs={{0,28},{1,5},{2,30},{3,7},{4,0},{5,9},{6,2},{7,11},{8,4},{9,13},{1... | collective-permute-start | bytes 393224 | tf_op jit(solution)/shard_map/ppermute | solution.py:213
  70.3 12.0 %collective-permute-start.17 = (bf16[32,2048]{1,0:T(8,128)(2,1)S(1)}, bf16[32,2048]{1,0:T(8,128)(2,1)S(1)}, u32[]{:S(2)}, u32[]{:S(2)}) collective-permute-start(bf16[32,2048]{1,0:T(8,128)(2,1)S(1)} %get-tuple-element.54), channel_id=1, source_target_pairs={{0,4},{1,29},{2,6},{3,31},{4,8},{5,1},{6,10},{7,3},{8,12},{9,5},{1... | collective-permute-start | bytes 393224 | tf_op jit(solution)/shard_map/ppermute | solution.py:213
  75.9 6.5 %collective-permute-start.20 = (bf16[16,2048]{1,0:T(8,128)(2,1)S(1)}, bf16[16,2048]{1,0:T(8,128)(2,1)S(1)}, u32[]{:S(2)}, u32[]{:S(2)}) collective-permute-start(bf16[16,2048]{1,0:T(8,128)(2,1)S(1)} %get-tuple-element.58), channel_id=1, source_target_pairs={{0,26},{1,7},{2,28},{3,9},{4,30},{5,11},{6,0},{7,13},{8,2},{9,15},... | collective-permute-start | bytes 196616 | tf_op jit(solution)/shard_map/ppermute | solution.py:213
  83.0 1.7 %collective-permute-start.22 = (bf16[64,2048]{1,0:T(8,128)(2,1)S(1)}, bf16[64,2048]{1,0:T(8,128)(2,1)S(1)}, u32[]{:S(2)}, u32[]{:S(2)}) collective-permute-start(bf16[64,2048]{1,0:T(8,128)(2,1)S(1)} %get-tuple-element.66), channel_id=1, source_target_pairs={{0,1},{1,0},{2,3},{3,2},{4,5},{5,4},{6,7},{7,6},{8,9},{9,8},{10,11... | collective-permute-start | bytes 786440 | tf_op jit(solution)/shard_map/ppermute | solution.py:216
  83.1 8.5 %collective-permute-start.21 = (bf16[32,2048]{1,0:T(8,128)(2,1)S(1)}, bf16[32,2048]{1,0:T(8,128)(2,1)S(1)}, u32[]{:S(2)}, u32[]{:S(2)}) collective-permute-start(bf16[32,2048]{1,0:T(8,128)(2,1)S(1)} %get-tuple-element.64), channel_id=1, source_target_pairs={{0,1},{1,0},{2,3},{3,2},{4,5},{5,4},{6,7},{7,6},{8,9},{9,8},{10,11... | collective-permute-start | bytes 393224 | tf_op jit(solution)/shard_map/ppermute | solution.py:216
  84.7 10.0 %collective-permute-start.23 = (bf16[32,2048]{1,0:T(8,128)(2,1)S(1)}, bf16[32,2048]{1,0:T(8,128)(2,1)S(1)}, u32[]{:S(2)}, u32[]{:S(2)}) collective-permute-start(bf16[32,2048]{1,0:T(8,128)(2,1)S(1)} %get-tuple-element.67), channel_id=1, source_target_pairs={{0,22},{1,11},{2,24},{3,13},{4,26},{5,15},{6,28},{7,17},{8,30},{9,... | collective-permute-start | bytes 393224 | tf_op jit(solution)/shard_map/ppermute | solution.py:213
  90.2 16.8 %collective-permute-start.24 = (bf16[32,2048]{1,0:T(8,128)(2,1)S(1)}, bf16[32,2048]{1,0:T(8,128)(2,1)S(1)}, u32[]{:S(2)}, u32[]{:S(2)}) collective-permute-start(bf16[32,2048]{1,0:T(8,128)(2,1)S(1)} %get-tuple-element.68), channel_id=1, source_target_pairs={{0,10},{1,23},{2,12},{3,25},{4,14},{5,27},{6,16},{7,29},{8,18},{9,... | collective-permute-start | bytes 393224 | tf_op jit(solution)/shard_map/ppermute | solution.py:213

commit v9 on v8

--- a/solution.py
+++ b/solution.py
@@ -10,7 +10,7 @@
 
 HOP = 5
 NEAR = (2, -2, 1, -1, 0)
-EARLY = 2
+EARLY = 0
 GRP_EP = ("grp", "z", "c")
 META = 128
 LIMIT = 16 << 20
@@ -125,28 +125,19 @@
         at += b.shape[0]
 
 
-def experts(tile, count, held, *refs):
+def experts(count, held, *refs):
     blocks, carried, refs = refs[:count], refs[count : count + held], refs[count + held :]
     (gate_ref, up_ref, down_ref), refs = refs[:3], refs[3:]
-    outs, (x_ref, total_ref) = refs[:count], refs[count:]
+    outs, x_ref = refs[:count], refs[count]
     gather(blocks, x_ref)
-    hidden = gate_ref.shape[1]
-    total_ref[...] = jnp.zeros_like(total_ref)
-
-    @pl.loop(0, hidden // tile)
-    def _(i):
-        cols = pl.ds(pl.multiple_of(i * tile, tile), tile)
-        x = x_ref[...]
-        gate = jnp.minimum(jnp.dot(x, gate_ref[:, cols], preferred_element_type=jnp.float32), 7.0)
-        upper = jnp.clip(
-            jnp.dot(x, up_ref[:, cols], preferred_element_type=jnp.float32), -7.0, 7.0
-        )
-        active = (gate * jax.nn.sigmoid(1.702 * gate) * (upper + 1.0)).astype(jnp.bfloat16)
-        total_ref[...] += jnp.dot(active, down_ref[cols, :], preferred_element_type=jnp.float32)
-
+    x = x_ref[...]
+    gate = jnp.minimum(jnp.dot(x, gate_ref[...], preferred_element_type=jnp.float32), 7.0)
+    upper = jnp.clip(jnp.dot(x, up_ref[...], preferred_element_type=jnp.float32), -7.0, 7.0)
+    active = (gate * jax.nn.sigmoid(1.702 * gate) * (upper + 1.0)).astype(jnp.bfloat16)
+    total = jnp.dot(active, down_ref[...], preferred_element_type=jnp.float32).astype(jnp.bfloat16)
     at = 0
     for i, (b, o) in enumerate(zip(blocks, outs)):
-        o[: b.shape[0]] = total_ref[at : at + b.shape[0], :].astype(jnp.bfloat16)
+        o[: b.shape[0]] = total[at : at + b.shape[0]]
         if EARLY <= i < EARLY + held:
             o[b.shape[0] :] = carried[i - EARLY][...]
         at += b.shape[0]
@@ -156,7 +147,7 @@
     early, blocks, refs = refs[:EARLY], refs[EARLY : EARLY + 6], refs[EARLY + 6 :]
     (high_ref, low_ref, near_high, near_low), refs = refs[:4], refs[4:]
     far_mine, far_other, mine, other, x_ref, near_ref = refs
-    at, near_at, small = 0, 0, early[0].shape[0]
+    at, near_at, small = 0, 0, near_ref.shape[0] // len(NEAR)
     for e in early:
         near_ref[near_at : near_at + small, :] = e[...]
         near_at += small
@@ -261,10 +252,10 @@
         for i, b in enumerate(carried):
             sizes[EARLY + i] += b.shape[0]
         experts_of = call(
-            functools.partial(experts, hidden // 2, len(blocks), len(carried)),
+            functools.partial(experts, len(blocks), len(carried)),
             [bf16(n, width) for n in sizes],
             len(blocks) + len(carried) + 3,
-            scratch=[pltpu.VMEM((slots, width), jnp.bfloat16), pltpu.VMEM((slots, width), jnp.float32)],
+            scratch=[pltpu.VMEM((slots, width), jnp.bfloat16)],
             flops=6 * slots * width * hidden,
         )
         return experts_of(*blocks, *carried, w_gate[0], w_up[0], w_down[0])

time: 109 us -> 106 us (0.972); the launches traced: 108 us -> 106 us
  starting transfers between devices: 51.8 us -> 45.7 us
  waiting for transfers between devices: 41.3 us -> 46.9 us
  Pallas kernels: 14.3 us -> 13 us
    ppermute x20 -> x18, starting transfers between devices: 50.6 us -> 44.6 us  [shift(): return lax.ppermute(x, ('z', 'c'), pairs)]
    ppermute x20 -> x18, waiting for transfers between devices: 40.3 us -> 45.9 us  [shift(): return lax.ppermute(x, ('z', 'c'), pairs)]
    pallas_call x2, Pallas kernels: 9.38 us -> 8.14 us  [run(): return experts_of(*blocks, *carried, w_gate[0], w_up[0], w_down[0])]
  transfers between devices with their start and end apart: 25 -> 23, of which waited for: 8 -> 8; matrix products, arithmetic and copies ran while one was open for 0% -> 0% of each run, Pallas kernels for 11% -> 6%
where the time goes in v9:
time: 106 us
  waiting for transfers between devices  46.9 us (44%)
  starting transfers between devices  45.7 us (43%)
  Pallas kernels  13 us (12%)
    ppermute x18, waiting for transfers between devices, shift(): return lax.ppermute(x, ('z', 'c'), pairs)  45.9 us
    ppermute x18, starting transfers between devices, shift(): return lax.ppermute(x, ('z', 'c'), pairs)  44.6 us
    pallas_call x2, Pallas kernels, run(): return experts_of(*blocks, *carried, w_gate[0], w_up[0], w_down[0])  8.14 us
  transfers between devices with their start and end apart: 23, of which 8 were waited for; matrix products, arithmetic and copies ran while one was open for 0% of the time, Pallas kernels for 6%

profile of v9, /device:TPU:86, one launch (start us, length us, event | category | flops | bytes accessed | tf_op | source)
XLA Modules:
  0.0 106.0 jit_solution(17818322729025039538)
XLA Ops:
  0.0 1.5 %shard_map.73.refs_0_ = bf16[32,2176]{1,0:T(8,128)(2,1)S(1)} custom-call(bf16[32,2048]{1,0:T(8,128)(2,1)} %tok_hbm.1, f32[1,2048]{1,0:T(1,128)} %bitcast.20, s32[4,32]{1,0:T(4,128)} %bitcast.21, f32[4,32]{1,0:T(4,128)} %bitcast.22), custom_call_target="tpu_custom_call" | custom-call | flops 1048576 | bytes 1048576 | tf_op jit(solution)/shard_map/pallas_call | solution.py:210
  1.5 14.8 %collective-permute-start.1 = (bf16[32,2176]{1,0:T(8,128)(2,1)S(1)}, bf16[32,2176]{1,0:T(8,128)(2,1)S(1)}, u32[]{:S(2)}, u32[]{:S(2)}) collective-permute-start(bf16[32,2176]{1,0:T(8,128)(2,1)S(1)} %shard_map.73.refs_0_), channel_id=1, source_target_pairs={{0,22},{1,11},{2,24},{3,13},{4,26},{5,15},{6,28},{7,17},{8,30},{9,... | collective-permute-start | bytes 417800 | tf_op jit(solution)/shard_map/ppermute | solution.py:204
  16.3 0.0 collective-permute-start
  16.3 0.0 collective-permute-start.9
  16.3 0.0 slice-start
  16.3 0.0 slice-start.2
  16.3 0.0 slice-start.4
  16.4 0.1 pad_add_fusion.place_ref
  16.4 0.0 slice-start.1
  16.4 14.5 %collective-permute-done.1.refs_2_ = bf16[32,2176]{1,0:T(8,128)(2,1)S(1)} collective-permute-done((bf16[32,2176]{1,0:T(8,128)(2,1)S(1)}, bf16[32,2176]{1,0:T(8,128)(2,1)S(1)}, u32[]{:S(2)}, u32[]{:S(2)}) %collective-permute-start.1) | collective-permute-done | bytes 139296 | tf_op jit(solution)/shard_map/ppermute | solution.py:204
  31.0 0.0 collective-permute-start.2
  31.0 0.0 collective-permute-done.refs_0_
  31.0 0.5 collective-permute-start.3
  31.5 0.0 collective-permute-done.9.refs_1_
  31.5 0.9 shard_map.75
  32.4 0.1 collective-permute-start.10
  32.5 4.1 %collective-permute-start.11 = (bf16[16,2048]{1,0:T(8,128)(2,1)S(1)}, bf16[16,2048]{1,0:T(8,128)(2,1)S(1)}, u32[]{:S(2)}, u32[]{:S(2)}) collective-permute-start(bf16[16,2048]{1,0:T(8,128)(2,1)S(1)} %get-tuple-element.44), channel_id=1, source_target_pairs={{0,28},{1,5},{2,30},{3,7},{4,0},{5,9},{6,2},{7,11},{8,4},{9,13},{1... | collective-permute-start | bytes 196616 | tf_op jit(solution)/shard_map/ppermute | solution.py:204
  36.7 2.4 %collective-permute-start.12 = (bf16[16,2048]{1,0:T(8,128)(2,1)S(1)}, bf16[16,2048]{1,0:T(8,128)(2,1)S(1)}, u32[]{:S(2)}, u32[]{:S(2)}) collective-permute-start(bf16[16,2048]{1,0:T(8,128)(2,1)S(1)} %get-tuple-element.45), channel_id=1, source_target_pairs={{0,2},{1,31},{2,4},{3,1},{4,6},{5,3},{6,8},{7,5},{8,10},{9,7},{10,... | collective-permute-start | bytes 196616 | tf_op jit(solution)/shard_map/ppermute | solution.py:204
  39.1 0.0 collective-permute-done.2.refs_1_
  39.1 1.3 %collective-permute-start.13 = (bf16[16,2048]{1,0:T(8,128)(2,1)S(1)}, bf16[16,2048]{1,0:T(8,128)(2,1)S(1)}, u32[]{:S(2)}, u32[]{:S(2)}) collective-permute-start(bf16[16,2048]{1,0:T(8,128)(2,1)S(1)} %get-tuple-element.46), channel_id=1, source_target_pairs={{0,30},{1,3},{2,0},{3,5},{4,2},{5,7},{6,4},{7,9},{8,6},{9,11},{10,... | collective-permute-start | bytes 196616 | tf_op jit(solution)/shard_map/ppermute | solution.py:204
  40.4 0.0 collective-permute-done.3.refs_3_
  40.4 1.1 %shard_map.74 = (bf16[32,2048]{1,0:T(8,128)(2,1)S(1)}, bf16[32,2048]{1,0:T(8,128)(2,1)S(1)}, bf16[32,2048]{1,0:T(8,128)(2,1)S(1)}, bf16[32,2048]{1,0:T(8,128)(2,...) custom-call(s32[2]{0:T(128)S(1)} %pad_add_fusion.place_ref, ...), custom_call_target="tpu_custom_call" | custom-call | flops 268435456 | bytes 1048576 | tf_op jit(solution)/shard_map/pallas_call | solution.py:239
  41.6 1.0 collective-permute-start.8
  42.6 0.0 collective-permute-done.10.refs_0_
  42.6 1.5 %collective-permute-start.4 = (bf16[32,2048]{1,0:T(8,128)(2,1)S(1)}, bf16[32,2048]{1,0:T(8,128)(2,1)S(1)}, u32[]{:S(2)}, u32[]{:S(2)}) collective-permute-start(bf16[32,2048]{1,0:T(8,128)(2,1)S(1)} %get-tuple-element.37), channel_id=1, source_target_pairs={{0,4},{1,29},{2,6},{3,31},{4,8},{5,1},{6,10},{7,3},{8,12},{9,5},{1... | collective-permute-start | bytes 393224 | tf_op jit(solution)/shard_map/ppermute | solution.py:204
  44.0 0.0 collective-permute-done.11.refs_1_
  44.0 2.7 %collective-permute-start.5 = (bf16[32,2048]{1,0:T(8,128)(2,1)S(1)}, bf16[32,2048]{1,0:T(8,128)(2,1)S(1)}, u32[]{:S(2)}, u32[]{:S(2)}) collective-permute-start(bf16[32,2048]{1,0:T(8,128)(2,1)S(1)} %get-tuple-element.38), channel_id=1, source_target_pairs={{0,28},{1,5},{2,30},{3,7},{4,0},{5,9},{6,2},{7,11},{8,4},{9,13},{1... | collective-permute-start | bytes 393224 | tf_op jit(solution)/shard_map/ppermute | solution.py:204
  46.7 0.0 collective-permute-done.12.refs_2_
  46.7 3.2 %collective-permute-start.6 = (bf16[32,2048]{1,0:T(8,128)(2,1)S(1)}, bf16[32,2048]{1,0:T(8,128)(2,1)S(1)}, u32[]{:S(2)}, u32[]{:S(2)}) collective-permute-start(bf16[32,2048]{1,0:T(8,128)(2,1)S(1)} %get-tuple-element.39), channel_id=1, source_target_pairs={{0,2},{1,31},{2,4},{3,1},{4,6},{5,3},{6,8},{7,5},{8,10},{9,7},{10,... | collective-permute-start | bytes 393224 | tf_op jit(solution)/shard_map/ppermute | solution.py:204
  49.9 0.0 collective-permute-done.13.refs_3_
  49.9 0.0 collective-permute-start.7
  50.0 0.0 slice-done
  50.0 0.0 slice-done.2
  50.0 0.0 slice-done.4
  50.0 0.0 slice-done.1
  50.0 0.0 slice-done.3
  50.0 0.0 slice-done.5
  50.0 4.0 %shard_map.76 = (bf16[16,2048]{1,0:T(8,128)(2,1)S(1)}, bf16[16,2048]{1,0:T(8,128)(2,1)S(1)}, bf16[16,2048]{1,0:T(8,128)(2,1)S(1)}, bf16[16,2048]{1,0:T(8,128)(2,1)S(1)}, bf16[16,2048]{1,0:T(8,128)(2,1)S(1)}) custom-call(bf16[16,2048]{1,0:T(8,128)(2,1)S(1)} %collective-permute-done.10.refs_0_, bf16[16,2048]{1,0:T(8,128)(2,1)S(1)} %collective-permute-done.11.refs_1_, ...), custom_call_target="tpu_custom_call" | custom-call | flops 1761607680 | bytes 1048576 | tf_op jit(solution)/shard_map/pallas_call | solution.py:261
  54.0 0.0 collective-permute-done.8.refs_5_
  54.0 0.0 collective-permute-done.4.refs_0_
  54.0 0.5 collective-permute-done.5.refs_1_
  54.5 3.5 %collective-permute-done.6.refs_2_ = bf16[32,2048]{1,0:T(8,128)(2,1)S(1)} collective-permute-done((bf16[32,2048]{1,0:T(8,128)(2,1)S(1)}, bf16[32,2048]{1,0:T(8,128)(2,1)S(1)}, u32[]{:S(2)}, u32[]{:S(2)}) %collective-permute-start.6) | collective-permute-done | bytes 131104 | tf_op jit(solution)/shard_map/ppermute | solution.py:204
  58.0 0.9 collective-permute-done.7.refs_3_
  58.9 4.2 %shard_map.77 = (bf16[48,2048]{1,0:T(8,128)(2,1)S(1)}, bf16[48,2048]{1,0:T(8,128)(2,1)S(1)}, bf16[48,2048]{1,0:T(8,128)(2,1)S(1)}, bf16[48,2048]{1,0:T(8,128)(2,...) custom-call(bf16[32,2048]{1,0:T(8,128)(2,1)S(1)} %collective-permute-done.4.refs_0_, ...), custom_call_target="tpu_custom_call" | custom-call | flops 3875536896 | bytes 1048576 | tf_op jit(solution)/shard_map/pallas_call | solution.py:261
  63.1 0.6 collective-permute-start.14
  63.6 2.4 %collective-permute-start.15 = (bf16[48,2048]{1,0:T(8,128)(2,1)S(1)}, bf16[48,2048]{1,0:T(8,128)(2,1)S(1)}, u32[]{:S(2)}, u32[]{:S(2)}) collective-permute-start(bf16[48,2048]{1,0:T(8,128)(2,1)S(1)} %get-tuple-element.54), channel_id=1, source_target_pairs={{0,4},{1,29},{2,6},{3,31},{4,8},{5,1},{6,10},{7,3},{8,12},{9,5},{1... | collective-permute-start | bytes 589832 | tf_op jit(solution)/shard_map/ppermute | solution.py:204
  66.1 2.7 %collective-permute-start.16 = (bf16[48,2048]{1,0:T(8,128)(2,1)S(1)}, bf16[48,2048]{1,0:T(8,128)(2,1)S(1)}, u32[]{:S(2)}, u32[]{:S(2)}) collective-permute-start(bf16[48,2048]{1,0:T(8,128)(2,1)S(1)} %get-tuple-element.55), channel_id=1, source_target_pairs={{0,30},{1,3},{2,0},{3,5},{4,2},{5,7},{6,4},{7,9},{8,6},{9,11},{10,... | collective-permute-start | bytes 589832 | tf_op jit(solution)/shard_map/ppermute | solution.py:204
  68.8 0.0 collective-permute-start.17
  68.8 0.8 collective-permute-start.18
  69.5 11.3 %collective-permute-done.18.refs_5_ = bf16[16,2048]{1,0:T(8,128)(2,1)S(1)} collective-permute-done((bf16[16,2048]{1,0:T(8,128)(2,1)S(1)}, bf16[16,2048]{1,0:T(8,128)(2,1)S(1)}, u32[]{:S(2)}, u32[]{:S(2)}) %collective-permute-start.18) | collective-permute-done | bytes 65568 | tf_op jit(solution)/shard_map/ppermute | solution.py:204
  80.8 0.0 collective-permute-done.14.refs_0_
  80.8 0.0 collective-permute-done.15.refs_1_
  80.8 0.0 collective-permute-done.16.refs_2_
  80.8 0.0 collective-permute-done.17.refs_3_
  80.8 0.6 shard_map.78
  81.4 0.1 collective-permute-start.20
  81.6 0.5 collective-permute-start.19
  82.0 1.0 collective-permute-done.20.other
  83.1 5.7 %collective-permute-start.21 = (bf16[32,2048]{1,0:T(8,128)(2,1)S(1)}, bf16[32,2048]{1,0:T(8,128)(2,1)S(1)}, u32[]{:S(2)}, u32[]{:S(2)}) collective-permute-start(bf16[32,2048]{1,0:T(8,128)(2,1)S(1)} %get-tuple-element.67), channel_id=1, source_target_pairs={{0,22},{1,11},{2,24},{3,13},{4,26},{5,15},{6,28},{7,17},{8,30},{9,... | collective-permute-start | bytes 393224 | tf_op jit(solution)/shard_map/ppermute | solution.py:204
  88.8 1.3 %collective-permute-start.22 = (bf16[32,2048]{1,0:T(8,128)(2,1)S(1)}, bf16[32,2048]{1,0:T(8,128)(2,1)S(1)}, u32[]{:S(2)}, u32[]{:S(2)}) collective-permute-start(bf16[32,2048]{1,0:T(8,128)(2,1)S(1)} %get-tuple-element.68), channel_id=1, source_target_pairs={{0,10},{1,23},{2,12},{3,25},{4,14},{5,27},{6,16},{7,29},{8,18},{9,... | collective-permute-start | bytes 393224 | tf_op jit(solution)/shard_map/ppermute | solution.py:204
  90.1 0.0 collective-permute-done.19.other
  90.1 14.4 %collective-permute-done.21.one = bf16[32,2048]{1,0:T(8,128)(2,1)S(1)} collective-permute-done((bf16[32,2048]{1,0:T(8,128)(2,1)S(1)}, bf16[32,2048]{1,0:T(8,128)(2,1)S(1)}, u32[]{:S(2)}, u32[]{:S(2)}) %collective-permute-start.21) | collective-permute-done | bytes 131104 | tf_op jit(solution)/shard_map/ppermute | solution.py:204
  104.4 0.8 collective-permute-done.22.two
  105.3 0.7 shard_map.80
  (6 shorter events, 0.1 us)
Async XLA Ops:
  1.5 29.5 %collective-permute-start.1 = (bf16[32,2176]{1,0:T(8,128)(2,1)S(1)}, bf16[32,2176]{1,0:T(8,128)(2,1)S(1)}, u32[]{:S(2)}, u32[]{:S(2)}) collective-permute-start(bf16[32,2176]{1,0:T(8,128)(2,1)S(1)} %shard_map.73.refs_0_), channel_id=1, source_target_pairs={{0,22},{1,11},{2,24},{3,13},{4,26},{5,15},{6,28},{7,17},{8,30},{9,... | collective-permute-start | bytes 417800 | tf_op jit(solution)/shard_map/ppermute | solution.py:204
  16.3 14.7 %collective-permute-start = (bf16[32,2176]{1,0:T(8,128)(2,1)S(1)}, bf16[32,2176]{1,0:T(8,128)(2,1)S(1)}, u32[]{:S(2)}, u32[]{:S(2)}) collective-permute-start(bf16[32,2176]{1,0:T(8,128)(2,1)S(1)} %shard_map.73.refs_0_), channel_id=1, source_target_pairs={{0,10},{1,23},{2,12},{3,25},{4,14},{5,27},{6,16},{7,29},{8,18},{9,... | collective-permute-start | bytes 417800 | tf_op jit(solution)/shard_map/ppermute | solution.py:204
  16.3 15.2 %collective-permute-start.9 = (bf16[32,2176]{1,0:T(8,128)(2,1)S(1)}, bf16[32,2176]{1,0:T(8,128)(2,1)S(1)}, u32[]{:S(2)}, u32[]{:S(2)}) collective-permute-start(bf16[32,2176]{1,0:T(8,128)(2,1)S(1)} %shard_map.73.refs_0_), channel_id=1, source_target_pairs={{0,1},{1,0},{2,3},{3,2},{4,5},{5,4},{6,7},{7,6},{8,9},{9,8},{10,11... | collective-permute-start | bytes 417800 | tf_op jit(solution)/shard_map/ppermute | solution.py:207
  16.3 33.6 %slice-start = ((s8[7340032]{0:T(1024)(128)(4,1)}), s8[4194304]{0:T(1024)(128)(4,1)S(1)}, s32[]{:S(2)}) async-start(s8[7340032]{0:T(1024)(128)(4,1)} %bitcast.8), calls=%async_computation | async-start | bytes 8388608
  16.3 33.6 %slice-start.2 = ((s8[7340032]{0:T(1024)(128)(4,1)}), s8[4194304]{0:T(1024)(128)(4,1)S(1)}, s32[]{:S(2)}) async-start(s8[7340032]{0:T(1024)(128)(4,1)} %bitcast.12), calls=%async_computation.2 | async-start | bytes 8388608
  16.3 33.6 %slice-start.4 = ((s8[7340032]{0:T(1024)(128)(4,1)}), s8[4194304]{0:T(1024)(128)(4,1)S(1)}, s32[]{:S(2)}) async-start(s8[7340032]{0:T(1024)(128)(4,1)} %bitcast.16), calls=%async_computation.4 | async-start | bytes 8388608
  16.4 33.5 %slice-start.1 = ((s8[7340032]{0:T(1024)(128)(4,1)}), s8[3145728]{0:T(1024)(128)(4,1)S(1)}, s32[]{:S(2)}) async-start(s8[7340032]{0:T(1024)(128)(4,1)} %bitcast.8), calls=%async_computation.1 | async-start | bytes 6291456
  16.4 33.6 %slice-start.3 = ((s8[7340032]{0:T(1024)(128)(4,1)}), s8[3145728]{0:T(1024)(128)(4,1)S(1)}, s32[]{:S(2)}) async-start(s8[7340032]{0:T(1024)(128)(4,1)} %bitcast.12), calls=%async_computation.3 | async-start | bytes 6291456
  16.4 33.6 %slice-start.5 = ((s8[7340032]{0:T(1024)(128)(4,1)}), s8[3145728]{0:T(1024)(128)(4,1)S(1)}, s32[]{:S(2)}) async-start(s8[7340032]{0:T(1024)(128)(4,1)} %bitcast.16), calls=%async_computation.5 | async-start | bytes 6291456
  31.0 8.1 %collective-permute-start.2 = (bf16[32,2176]{1,0:T(8,128)(2,1)S(1)}, bf16[32,2176]{1,0:T(8,128)(2,1)S(1)}, u32[]{:S(2)}, u32[]{:S(2)}) collective-permute-start(bf16[32,2176]{1,0:T(8,128)(2,1)S(1)} %collective-permute-done.1.refs_2_), channel_id=1, source_target_pairs={{0,1},{1,0},{2,3},{3,2},{4,5},{5,4},{6,7},{7,6},{8,9},{9,8},{10,11... | collective-permute-start | bytes 417800 | tf_op jit(solution)/shard_map/ppermute | solution.py:207
  31.0 9.5 %collective-permute-start.3 = (bf16[32,2176]{1,0:T(8,128)(2,1)S(1)}, bf16[32,2176]{1,0:T(8,128)(2,1)S(1)}, u32[]{:S(2)}, u32[]{:S(2)}) collective-permute-start(bf16[32,2176]{1,0:T(8,128)(2,1)S(1)} %collective-permute-done.refs_0_), channel_id=1, source_target_pairs={{0,1},{1,0},{2,3},{3,2},{4,5},{5,4},{6,7},{7,6},{8,9},{9,8},{10,11... | collective-permute-start | bytes 417800 | tf_op jit(solution)/shard_map/ppermute | solution.py:207
  32.4 10.2 %collective-permute-start.10 = (bf16[16,2048]{1,0:T(8,128)(2,1)S(1)}, bf16[16,2048]{1,0:T(8,128)(2,1)S(1)}, u32[]{:S(2)}, u32[]{:S(2)}) collective-permute-start(bf16[16,2048]{1,0:T(8,128)(2,1)S(1)} %get-tuple-element.43), channel_id=1, source_target_pairs={{0,4},{1,29},{2,6},{3,31},{4,8},{5,1},{6,10},{7,3},{8,12},{9,5},{1... | collective-permute-start | bytes 196616 | tf_op jit(solution)/shard_map/ppermute | solution.py:204
  32.5 11.5 %collective-permute-start.11 = (bf16[16,2048]{1,0:T(8,128)(2,1)S(1)}, bf16[16,2048]{1,0:T(8,128)(2,1)S(1)}, u32[]{:S(2)}, u32[]{:S(2)}) collective-permute-start(bf16[16,2048]{1,0:T(8,128)(2,1)S(1)} %get-tuple-element.44), channel_id=1, source_target_pairs={{0,28},{1,5},{2,30},{3,7},{4,0},{5,9},{6,2},{7,11},{8,4},{9,13},{1... | collective-permute-start | bytes 196616 | tf_op jit(solution)/shard_map/ppermute | solution.py:204
  36.7 10.1 %collective-permute-start.12 = (bf16[16,2048]{1,0:T(8,128)(2,1)S(1)}, bf16[16,2048]{1,0:T(8,128)(2,1)S(1)}, u32[]{:S(2)}, u32[]{:S(2)}) collective-permute-start(bf16[16,2048]{1,0:T(8,128)(2,1)S(1)} %get-tuple-element.45), channel_id=1, source_target_pairs={{0,2},{1,31},{2,4},{3,1},{4,6},{5,3},{6,8},{7,5},{8,10},{9,7},{10,... | collective-permute-start | bytes 196616 | tf_op jit(solution)/shard_map/ppermute | solution.py:204
  39.1 10.9 %collective-permute-start.13 = (bf16[16,2048]{1,0:T(8,128)(2,1)S(1)}, bf16[16,2048]{1,0:T(8,128)(2,1)S(1)}, u32[]{:S(2)}, u32[]{:S(2)}) collective-permute-start(bf16[16,2048]{1,0:T(8,128)(2,1)S(1)} %get-tuple-element.46), channel_id=1, source_target_pairs={{0,30},{1,3},{2,0},{3,5},{4,2},{5,7},{6,4},{7,9},{8,6},{9,11},{10,... | collective-permute-start | bytes 196616 | tf_op jit(solution)/shard_map/ppermute | solution.py:204
  41.6 12.4 %collective-permute-start.8 = (bf16[16,2048]{1,0:T(8,128)(2,1)S(1)}, bf16[16,2048]{1,0:T(8,128)(2,1)S(1)}, u32[]{:S(2)}, u32[]{:S(2)}) collective-permute-start(bf16[16,2048]{1,0:T(8,128)(2,1)S(1)} %get-tuple-element.42), channel_id=1, source_target_pairs={{0,6},{1,27},{2,8},{3,29},{4,10},{5,31},{6,12},{7,1},{8,14},{9,3},... | collective-permute-start | bytes 196616 | tf_op jit(solution)/shard_map/ppermute | solution.py:204
  42.6 11.4 %collective-permute-start.4 = (bf16[32,2048]{1,0:T(8,128)(2,1)S(1)}, bf16[32,2048]{1,0:T(8,128)(2,1)S(1)}, u32[]{:S(2)}, u32[]{:S(2)}) collective-permute-start(bf16[32,2048]{1,0:T(8,128)(2,1)S(1)} %get-tuple-element.37), channel_id=1, source_target_pairs={{0,4},{1,29},{2,6},{3,31},{4,8},{5,1},{6,10},{7,3},{8,12},{9,5},{1... | collective-permute-start | bytes 393224 | tf_op jit(solution)/shard_map/ppermute | solution.py:204
  44.0 10.4 %collective-permute-start.5 = (bf16[32,2048]{1,0:T(8,128)(2,1)S(1)}, bf16[32,2048]{1,0:T(8,128)(2,1)S(1)}, u32[]{:S(2)}, u32[]{:S(2)}) collective-permute-start(bf16[32,2048]{1,0:T(8,128)(2,1)S(1)} %get-tuple-element.38), channel_id=1, source_target_pairs={{0,28},{1,5},{2,30},{3,7},{4,0},{5,9},{6,2},{7,11},{8,4},{9,13},{1... | collective-permute-start | bytes 393224 | tf_op jit(solution)/shard_map/ppermute | solution.py:204
  46.7 11.3 %collective-permute-start.6 = (bf16[32,2048]{1,0:T(8,128)(2,1)S(1)}, bf16[32,2048]{1,0:T(8,128)(2,1)S(1)}, u32[]{:S(2)}, u32[]{:S(2)}) collective-permute-start(bf16[32,2048]{1,0:T(8,128)(2,1)S(1)} %get-tuple-element.39), channel_id=1, source_target_pairs={{0,2},{1,31},{2,4},{3,1},{4,6},{5,3},{6,8},{7,5},{8,10},{9,7},{10,... | collective-permute-start | bytes 393224 | tf_op jit(solution)/shard_map/ppermute | solution.py:204
  49.9 8.9 %collective-permute-start.7 = (bf16[32,2048]{1,0:T(8,128)(2,1)S(1)}, bf16[32,2048]{1,0:T(8,128)(2,1)S(1)}, u32[]{:S(2)}, u32[]{:S(2)}) collective-permute-start(bf16[32,2048]{1,0:T(8,128)(2,1)S(1)} %get-tuple-element.40), channel_id=1, source_target_pairs={{0,30},{1,3},{2,0},{3,5},{4,2},{5,7},{6,4},{7,9},{8,6},{9,11},{10,... | collective-permute-start | bytes 393224 | tf_op jit(solution)/shard_map/ppermute | solution.py:204
  63.1 17.8 %collective-permute-start.14 = (bf16[48,2048]{1,0:T(8,128)(2,1)S(1)}, bf16[48,2048]{1,0:T(8,128)(2,1)S(1)}, u32[]{:S(2)}, u32[]{:S(2)}) collective-permute-start(bf16[48,2048]{1,0:T(8,128)(2,1)S(1)} %get-tuple-element.53), channel_id=1, source_target_pairs={{0,28},{1,5},{2,30},{3,7},{4,0},{5,9},{6,2},{7,11},{8,4},{9,13},{1... | collective-permute-start | bytes 589832 | tf_op jit(solution)/shard_map/ppermute | solution.py:204
  63.6 17.2 %collective-permute-start.15 = (bf16[48,2048]{1,0:T(8,128)(2,1)S(1)}, bf16[48,2048]{1,0:T(8,128)(2,1)S(1)}, u32[]{:S(2)}, u32[]{:S(2)}) collective-permute-start(bf16[48,2048]{1,0:T(8,128)(2,1)S(1)} %get-tuple-element.54), channel_id=1, source_target_pairs={{0,4},{1,29},{2,6},{3,31},{4,8},{5,1},{6,10},{7,3},{8,12},{9,5},{1... | collective-permute-start | bytes 589832 | tf_op jit(solution)/shard_map/ppermute | solution.py:204
  66.1 14.7 %collective-permute-start.16 = (bf16[48,2048]{1,0:T(8,128)(2,1)S(1)}, bf16[48,2048]{1,0:T(8,128)(2,1)S(1)}, u32[]{:S(2)}, u32[]{:S(2)}) collective-permute-start(bf16[48,2048]{1,0:T(8,128)(2,1)S(1)} %get-tuple-element.55), channel_id=1, source_target_pairs={{0,30},{1,3},{2,0},{3,5},{4,2},{5,7},{6,4},{7,9},{8,6},{9,11},{10,... | collective-permute-start | bytes 589832 | tf_op jit(solution)/shard_map/ppermute | solution.py:204
  68.8 12.0 %collective-permute-start.17 = (bf16[48,2048]{1,0:T(8,128)(2,1)S(1)}, bf16[48,2048]{1,0:T(8,128)(2,1)S(1)}, u32[]{:S(2)}, u32[]{:S(2)}) collective-permute-start(bf16[48,2048]{1,0:T(8,128)(2,1)S(1)} %get-tuple-element.56), channel_id=1, source_target_pairs={{0,2},{1,31},{2,4},{3,1},{4,6},{5,3},{6,8},{7,5},{8,10},{9,7},{10,... | collective-permute-start | bytes 589832 | tf_op jit(solution)/shard_map/ppermute | solution.py:204
  68.8 12.0 %collective-permute-start.18 = (bf16[16,2048]{1,0:T(8,128)(2,1)S(1)}, bf16[16,2048]{1,0:T(8,128)(2,1)S(1)}, u32[]{:S(2)}, u32[]{:S(2)}) collective-permute-start(bf16[16,2048]{1,0:T(8,128)(2,1)S(1)} %get-tuple-element.58), channel_id=1, source_target_pairs={{0,26},{1,7},{2,28},{3,9},{4,30},{5,11},{6,0},{7,13},{8,2},{9,15},... | collective-permute-start | bytes 196616 | tf_op jit(solution)/shard_map/ppermute | solution.py:204
  81.4 1.7 %collective-permute-start.20 = (bf16[64,2048]{1,0:T(8,128)(2,1)S(1)}, bf16[64,2048]{1,0:T(8,128)(2,1)S(1)}, u32[]{:S(2)}, u32[]{:S(2)}) collective-permute-start(bf16[64,2048]{1,0:T(8,128)(2,1)S(1)} %get-tuple-element.66), channel_id=1, source_target_pairs={{0,1},{1,0},{2,3},{3,2},{4,5},{5,4},{6,7},{7,6},{8,9},{9,8},{10,11... | collective-permute-start | bytes 786440 | tf_op jit(solution)/shard_map/ppermute | solution.py:207
  81.6 8.5 %collective-permute-start.19 = (bf16[32,2048]{1,0:T(8,128)(2,1)S(1)}, bf16[32,2048]{1,0:T(8,128)(2,1)S(1)}, u32[]{:S(2)}, u32[]{:S(2)}) collective-permute-start(bf16[32,2048]{1,0:T(8,128)(2,1)S(1)} %get-tuple-element.64), channel_id=1, source_target_pairs={{0,1},{1,0},{2,3},{3,2},{4,5},{5,4},{6,7},{7,6},{8,9},{9,8},{10,11... | collective-permute-start | bytes 393224 | tf_op jit(solution)/shard_map/ppermute | solution.py:207
  83.1 21.3 %collective-permute-start.21 = (bf16[32,2048]{1,0:T(8,128)(2,1)S(1)}, bf16[32,2048]{1,0:T(8,128)(2,1)S(1)}, u32[]{:S(2)}, u32[]{:S(2)}) collective-permute-start(bf16[32,2048]{1,0:T(8,128)(2,1)S(1)} %get-tuple-element.67), channel_id=1, source_target_pairs={{0,22},{1,11},{2,24},{3,13},{4,26},{5,15},{6,28},{7,17},{8,30},{9,... | collective-permute-start | bytes 393224 | tf_op jit(solution)/shard_map/ppermute | solution.py:204
  88.8 16.5 %collective-permute-start.22 = (bf16[32,2048]{1,0:T(8,128)(2,1)S(1)}, bf16[32,2048]{1,0:T(8,128)(2,1)S(1)}, u32[]{:S(2)}, u32[]{:S(2)}) collective-permute-start(bf16[32,2048]{1,0:T(8,128)(2,1)S(1)} %get-tuple-element.68), channel_id=1, source_target_pairs={{0,10},{1,23},{2,12},{3,25},{4,14},{5,27},{6,16},{7,29},{8,18},{9,... | collective-permute-start | bytes 393224 | tf_op jit(solution)/shard_map/ppermute | solution.py:204
